TPU v7x, 32 devices: a whole 2x2x4 slice. The times are simulated.
32 devices in a mesh: ep: 8 (over z, core), tp: 4 (over y, x).
Axes of the slice: x: 2, y: 2, z: 4, core: 2. Of those that a mesh axis runs over, the one named last changes fastest.
Arguments:
- first_batch_queries: bfloat16 [2048, 1024], P('ep', 'tp'), may hold values from -6 to 6
- first_batch_keys: bfloat16 [2048, 1024], P('ep', 'tp'), may hold values from -6 to 6
- first_batch_values: bfloat16 [2048, 2048], P('ep', 'tp'), may hold values from -6 to 6
- output_gate_preactivation: bfloat16 [2048, 2048], P('ep', 'tp'), may hold values from -6 to 6
- decay_preactivation: bfloat16 [2048, 1024], P('ep', 'tp'), may hold values from -6 to 6
- channel_decay_bias: float32 [1024], P('tp')
- added_log_decay: float32 [16, 2048], P('tp', 'ep'), may hold values from -0.7 to 0
- head_norm_gain: float32 [2048], P('tp'), may hold values from 0.1 to 1.9
- attention_output_weight: bfloat16 [2048, 2048], P(None, 'tp'), may hold values from -0.125 to 0.125
- second_batch_rows: bfloat16 [768, 2048], P('ep'), may hold values from -6 to 6
- expert_norm_gain: float32 [2048], replicated, may hold values from 0.1 to 1.9
- routed_expert_index: int32 [768, 4], P('ep'), may hold values from 0 to 7, all different within a row; in each aligned block of 96 rows (0 to 95, 96 to 191, ...) at most 72 rows name the same one
- router_chosen_scores: float32 [768, 4], P('ep'), may hold values from 0.1 to 1
- expert_gate_weight: bfloat16 [8, 2048, 4096], P('ep', None, 'tp'), may hold values from -0.125 to 0.125
- expert_up_weight: bfloat16 [8, 2048, 4096], P('ep', None, 'tp'), may hold values from -0.125 to 0.125
- expert_down_weight: bfloat16 [8, 4096, 2048], P('ep', None, 'tp'), may hold values from -0.09375 to 0.09375
- shared_gate_weight: bfloat16 [2048, 1024], P(None, 'tp'), may hold values from -0.125 to 0.125
- shared_up_weight: bfloat16 [2048, 1024], P(None, 'tp'), may hold values from -0.125 to 0.125
- shared_down_weight: bfloat16 [1024, 2048], P(None, 'tp'), may hold values from -0.1875 to 0.1875
Outputs:
- token_mixed: bfloat16 [2048, 2048], P('ep', 'tp')
- channel_mixed: bfloat16 [768, 2048], P('ep', 'tp')
Inputs may be any that keep to these rules, and one draw needn't show every extreme that they name: `routed_expert_index`: in each aligned block of 96 rows (the rows of one index of ep) no expert is named by more than 72 rows, a bound that some block reaches; a row names 4 different experts.
All inputs are finite; a program needn't handle non-finite values.
Results may differ from a plain program's by a relative error of at most 0.018.
Values may be sent and summed in bfloat16 or wider, within the bound.
No kernel may reach another device: no remote copies, remote signals or barrier semaphores. Data moves between devices by JAX's collectives and lax.ppermute only.
A program may use at most 64 MiB of HBM per device.

v0:
```python
import math

import jax
import jax.numpy as jnp
import numpy as np
from jax import lax
from jax.experimental import pallas as pl
from jax.experimental.pallas import tpu as pltpu
from jax.sharding import PartitionSpec as P


BLOCK = 64
epsilon = 1e-06
temper = 16.0
routed_scale = 2.5
highest = lax.Precision.HIGHEST
f32 = jnp.float32
bf16 = jnp.bfloat16
AXES = ("ep", "tp")


class Places:
    def __init__(self):
        self.ep, self.tp = lax.axis_size("ep"), lax.axis_size("tp")
        self.side = math.isqrt(self.tp)
        self.chips = self.ep // 2
        assert self.side * self.side == self.tp and self.chips * 2 == self.ep

    def pairs(self, move):
        n = self.side
        out = []
        for e in range(self.ep):
            for j in range(self.tp):
                z, c, y, x = move(e // 2, e % 2, j // n, j % n)
                if 0 <= z < self.chips:
                    out.append((e * self.tp + j, (z * 2 + c) * self.tp + (y % n) * n + x % n))
        return out

    def send(self, value, move):
        return lax.ppermute(value, AXES, self.pairs(move))

    def along_z(self, value, k):
        return self.send(value, lambda z, c, y, x: ((z + k) % self.chips, c, y, x))

    def up_z(self, value, k):
        return self.send(value, lambda z, c, y, x: (z + k, c, y, x))

    def to_sibling(self, value):
        return self.send(value, lambda z, c, y, x: (z, 1 - c, y, x))

    def along_u(self, value, k):
        return self.send(value, lambda z, c, y, x: (z, c, y, x + k) if c == 0 else (z, c, y + k, x))

    def along_v(self, value, k):
        return self.send(value, lambda z, c, y, x: (z, c, y + k, x) if c == 0 else (z, c, y, x + k))

    def along_tp(self, value, dy, dx):
        return self.send(value, lambda z, c, y, x: (z, c, y + dy, x + dx))


def dot(a, b, precision=None):
    return jnp.dot(a, b, preferred_element_type=f32, precision=precision)


def dot_nt(a, b):
    return lax.dot_general(a, b, (((1,), (1,)), ((), ())), preferred_element_type=f32)


def dot_tn(a, b, precision=None):
    return lax.dot_general(
        a, b, (((0,), (0,)), ((), ())), preferred_element_type=f32, precision=precision
    )


def hold(values):
    return lax.optimization_barrier(values)


def silu(value):
    return value / (1.0 + jnp.exp(-value))


def whole(count):
    return [pl.BlockSpec(memory_space=pltpu.VMEM)] * count


def column(n, core, x, y, du, dv):
    if core == 0:
        return (y + dv) % n * n + (x + du) % n
    return (y + du) % n * n + (x + dv) % n


class Index:
    def __init__(self, places):
        n = places.side
        table = [
            [z, c, (x + y) % n, z * 2 + c]
            + [column(n, c, x, y, -i, k) for k in range(n) for i in range(n)]
            + [(y - dy) % n * n + (x - dx) % n for dy in range(n) for dx in range(n)]
            for z in range(places.chips)
            for c in range(2)
            for y in range(n)
            for x in range(n)
        ]
        here = lax.axis_index("ep") * places.tp + lax.axis_index("tp")
        self.vector = lax.dynamic_index_in_dim(
            jnp.asarray(np.array(table, np.int32)), here, 0, keepdims=False
        )
        self.z, self.c, self.part, self.e = range(4)
        self.held, self.given = 4, 4 + n
        self.tp = 4 + n * n

    def block(self, place, count=1):
        return lambda i, s: (s[place + i], 0)


def call(body, outs, operands, flops, smem=0):
    specs = [pl.BlockSpec(memory_space=pltpu.SMEM)] * smem + whole(len(operands) - smem)
    return pl.pallas_call(
        body,
        out_shape=outs,
        in_specs=specs,
        out_specs=jax.tree.map(lambda _: pl.BlockSpec(memory_space=pltpu.VMEM), outs),
        cost_estimate=pl.CostEstimate(flops=flops, transcendentals=0, bytes_accessed=0),
    )(*operands)


def local_attention(q, k, v, decay_pre, bias, added):
    heads, rows = added.shape
    dk, dv = q.shape[1] // heads, v.shape[1] // heads
    blocks = rows // BLOCK
    group = min(max(1, 128 // dk), heads)
    lanes = group * dk

    def body(q_ref, k_ref, v_ref, d_ref, bias_ref, added_ref, o_ref, qd_ref, pack_ref):
        spread = (
            lax.broadcasted_iota(jnp.int32, (heads, heads * dk), 1) // dk
            == lax.broadcasted_iota(jnp.int32, (heads, heads * dk), 0)
        ).astype(f32)
        logits = d_ref[...].astype(f32) + bias_ref[...]
        base = jnp.minimum(logits, 0.0) - jnp.log1p(jnp.exp(-jnp.abs(logits)))
        decay = base / temper + dot_tn(added_ref[...], spread, highest)
        row = lax.broadcasted_iota(jnp.int32, (BLOCK, BLOCK), 0)
        col = lax.broadcasted_iota(jnp.int32, (BLOCK, BLOCK), 1)
        lower = row >= col
        lower_f = lower.astype(f32)
        lane = lax.broadcasted_iota(jnp.int32, (1, lanes), 1)
        masks = [(lane // dk == g).astype(f32) for g in range(group)]
        states = [None] * heads
        lead = jnp.zeros((1, heads * dk), f32)
        for b in range(blocks):
            span = slice(b * BLOCK, (b + 1) * BLOCK)
            running = dot(lower_f, decay[span], highest)
            total = running[BLOCK - 1 : BLOCK, :]
            grow = jnp.exp(running)
            q_dec = q_ref[span, :].astype(f32) * grow
            keys = k_ref[span, :].astype(f32)
            k_up = (keys * jnp.exp(-running)).astype(bf16)
            k_end = (keys * jnp.exp(total - running)).astype(bf16)
            qd_ref[span, :] = (q_dec * jnp.exp(lead)).astype(bf16)
            shrink = jnp.exp(total)
            for h in range(heads):
                at = slice(h // group * lanes, h // group * lanes + lanes)
                q_h = (q_dec[:, at] * masks[h % group]).astype(bf16)
                v_h = v_ref[span, h * dv : (h + 1) * dv]
                scores = jnp.where(lower, dot_nt(q_h, k_up[:, at]), 0.0).astype(bf16)
                value = dot(scores, v_h)
                if b:
                    value = value + dot_nt(q_h, states[h].astype(bf16))
                o_ref[span, h * dv : (h + 1) * dv] = value
                update = dot_tn(v_h, k_end[:, at])
                states[h] = update if b == 0 else states[h] * shrink[:, at] + update
            lead = lead + total
        for h0 in range(0, heads, group):
            packed = states[h0]
            for g in range(1, group):
                packed = jnp.where(lane // dk == g, states[h0 + g], packed)
            pack_ref[0:dv, h0 * dk : h0 * dk + lanes] = packed.astype(bf16)
        pack_ref[dv : dv + 8, :] = jnp.broadcast_to(jnp.exp(lead), (8, heads * dk)).astype(bf16)

    outs = (
        jax.ShapeDtypeStruct((rows, heads * dv), f32),
        jax.ShapeDtypeStruct((rows, heads * dk), bf16),
        jax.ShapeDtypeStruct((dv + 8, heads * dk), bf16),
    )
    return call(body, outs, (q, k, v, decay_pre, bias[None, :], added), 1 << 25)


def finish_attention(
    index, local, qd, states, gate_pre, gain, heads, normed, shared_gate, shared_up
):
    rows = local.shape[0]
    dv, dk = local.shape[1] // heads, qd.shape[1] // heads
    group = min(max(1, 128 // dk), heads)
    lanes = group * dk
    tokens, hidden = normed.shape[0], shared_gate.shape[1]
    sharing = local.shape[1] // hidden
    part = tokens // sharing

    def body(s_ref, local_ref, qd_ref, gate_ref, gain_ref, normed_ref, sg_ref, su_ref, *refs):
        out_ref = refs[-1]
        first = s_ref[index.c] == 0
        between = jnp.ones((1, heads * dk), f32)
        incoming = jnp.zeros((dv, heads * dk), f32)
        sib = refs[0][...].astype(f32)
        for hop in range(1, (len(refs) - 2) // 2 + 1):
            mine, other = refs[2 * hop - 1][...].astype(f32), refs[2 * hop][...].astype(f32)
            inside = s_ref[index.z] >= hop
            early, late = jnp.where(first, mine, other), jnp.where(first, other, mine)
            decay = late[dv : dv + 1]
            got = early[0:dv] * decay + late[0:dv]
            incoming = incoming + jnp.where(inside, between * got, 0.0)
            between = jnp.where(inside, between * (early[dv : dv + 1] * decay), between)
        incoming = jnp.where(first, incoming, incoming * sib[dv : dv + 1] + sib[0:dv]).astype(bf16)
        lane = lax.broadcasted_iota(jnp.int32, (1, lanes), 1)
        for h in range(heads):
            at = slice(h // group * lanes, h // group * lanes + lanes)
            vs = slice(h * dv, (h + 1) * dv)
            mask = lane // dk == h % group
            q_h = jnp.where(mask, qd_ref[:, at], jnp.zeros((), bf16))
            value = local_ref[:, vs] + dot_nt(q_h, incoming[:, at])
            mean_square = jnp.mean(value * value, axis=1, keepdims=True)
            value = value * lax.rsqrt(mean_square + epsilon) * gain_ref[:, vs]
            out_ref[0:rows, vs] = (value * silu(gate_ref[:, vs].astype(f32))).astype(bf16)
        features = normed_ref[...]
        shared = (silu(dot(features, sg_ref[...])) * dot(features, su_ref[...])).astype(bf16)
        for i in range(sharing):
            out_ref[rows : rows + part, i * hidden : (i + 1) * hidden] = shared[
                i * part : (i + 1) * part
            ]

    out = jax.ShapeDtypeStruct((rows + part, local.shape[1]), bf16)
    operands = (index.vector, local, qd, gate_pre, gain[None, :], normed, shared_gate, shared_up)
    return call(body, out, operands + tuple(states), 1 << 27, smem=1)


def project(index, gathered, attention_weight, shared_weight, tokens):
    count = len(gathered)
    folded, width = gathered[0].shape
    hidden, columns = shared_weight.shape[0] // count, shared_weight.shape[1]
    sharing = width // hidden
    part = tokens // sharing
    rows = folded - part

    def body(s_ref, *refs):
        weight_ref, shared_ref, mixed_ref, out_ref, sum_ref = refs[count:]
        for i in range(count):

            @pl.when(pl.program_id(0) == i)
            def _():
                ref = refs[i]
                mixed = dot(ref[0:rows, :], weight_ref[...])
                units = jnp.concatenate(
                    [ref[rows:, q * hidden : (q + 1) * hidden] for q in range(sharing)], axis=0
                )
                shared = dot(units, shared_ref[...])
                if i:
                    mixed, shared = mixed + sum_ref[...], shared + out_ref[...]
                if i < count - 1:
                    sum_ref[...] = mixed
                else:
                    mixed_ref[...] = mixed.astype(bf16)
                out_ref[...] = shared

    fixed = lambda i, s: (0, 0)
    return pl.pallas_call(
        body,
        out_shape=(
            jax.ShapeDtypeStruct((rows, columns), bf16),
            jax.ShapeDtypeStruct((tokens, columns), f32),
        ),
        grid_spec=pltpu.PrefetchScalarGridSpec(
            num_scalar_prefetch=1,
            grid=(count,),
            in_specs=[pl.BlockSpec((folded, width), fixed)] * count
            + [
                pl.BlockSpec((width, columns), index.block(index.tp)),
                pl.BlockSpec((hidden, columns), index.block(index.tp)),
            ],
            out_specs=(pl.BlockSpec((rows, columns), fixed), pl.BlockSpec((tokens, columns), fixed)),
            scratch_shapes=[pltpu.VMEM((rows, columns), f32)],
        ),
        cost_estimate=pl.CostEstimate(
            flops=2 * folded * width * columns * count, transcendentals=0, bytes_accessed=0
        ),
    )(index.vector, *gathered, attention_weight, shared_weight)


def prepare_rows(places, parts, rows, gain, index, scores, experts):
    tokens, width = rows.shape
    top = index.shape[1]
    piece = width // parts
    pad = -(-tokens // 128) * 128
    extra = -(-experts // 8) * 8

    def body(s_ref, rows_ref, gain_ref, index_ref, score_ref, normed_ref, packed_ref):
        value = rows_ref[...].astype(f32)
        mean_square = jnp.mean(value * value, axis=1, keepdims=True)
        normed = (value * lax.rsqrt(mean_square + epsilon) * gain_ref[...]).astype(bf16)
        normed_ref[...] = normed
        for q in range(parts):

            @pl.when(s_ref[places.part] == q)
            def _():
                packed_ref[0:tokens, :] = normed[:, q * piece : (q + 1) * piece]

        scores = score_ref[...]
        weights = routed_scale * scores / jnp.sum(scores, axis=0, keepdims=True)
        expert = lax.broadcasted_iota(jnp.int32, (extra, tokens), 0)
        named = jnp.zeros((extra, tokens), f32)
        weight = jnp.zeros((extra, tokens), f32)
        for k in range(top):
            hit = index_ref[k : k + 1, :] == expert
            named = jnp.where(hit, 1.0, named)
            weight = jnp.where(hit, weights[k : k + 1, :], weight)
        strict = (
            lax.broadcasted_iota(jnp.int32, (tokens, tokens), 0)
            < lax.broadcasted_iota(jnp.int32, (tokens, tokens), 1)
        ).astype(bf16)
        ranks = jnp.where(named > 0, dot(named.astype(bf16), strict), -1.0)
        packed_ref[tokens : tokens + extra, :] = jnp.full((extra, piece), -1.0, bf16)
        packed_ref[tokens : tokens + extra, 0:tokens] = ranks.astype(bf16)
        packed_ref[tokens : tokens + extra, pad : pad + tokens] = weight.astype(bf16)

    outs = (
        jax.ShapeDtypeStruct((tokens, width), bf16),
        jax.ShapeDtypeStruct((tokens + extra, piece), bf16),
    )
    operands = (places.vector, rows, gain[None, :], index.T, scores.T)
    return call(body, outs, operands, 1 << 22, smem=1)


def group_of(sources, capacity):
    group = 1
    while group < sources and group * capacity % 16:
        group *= 2
    return group


def expert_up(index, own, far, capacity, gate_weight, up_weight):
    parts = len(far[0])
    tokens, width = own[0].shape
    packed_rows, piece = own[1].shape
    extra = packed_rows - tokens
    pad = -(-tokens // 128) * 128
    sources = 1 + len(far)
    slots = sources * capacity
    group = group_of(sources, capacity)
    hidden = gate_weight.shape[1]
    step = min(256, hidden)
    flat = list(own) + [p for pieces in far for p in pieces]

    def body(s_ref, *refs):
        row_refs = refs[: len(flat)]
        gate_ref, up_ref, out_ref, info_ref, rows_ref, section_ref = refs[len(flat) :]

        @pl.when(pl.program_id(0) == 0)
        def _():
            expert = lax.broadcasted_iota(jnp.int32, (extra, 2 * pad), 0) == s_ref[index.e]
            if pad > tokens:
                for s in range(sources):
                    rows_ref[s * pad + tokens : (s + 1) * pad, :] = jnp.zeros(
                        (pad - tokens, width), bf16
                    )
            rows_ref[0:tokens, :] = row_refs[0][...]
            for q in range(parts):

                @pl.when(s_ref[index.part] == q)
                def _():
                    for s in range(1, sources):
                        for i in range(parts):
                            to = (q - i) % parts
                            rows_ref[
                                s * pad : s * pad + tokens, to * piece : (to + 1) * piece
                            ] = row_refs[2 + (s - 1) * parts + i][0:tokens, :]

            for s0 in range(0, sources, group):
                targets = []
                for s in range(s0, s0 + group):
                    table_ref = row_refs[2 + (s - 1) * parts if s else 1]
                    table = table_ref[tokens : tokens + extra, 0 : 2 * pad].astype(f32)
                    mine = jnp.sum(jnp.where(expert, table, 0.0), axis=0, keepdims=True)
                    info_ref[s : s + 1, :] = mine
                    rank = mine[:, 0:pad]
                    targets.append(jnp.where(rank >= 0, rank + (s - s0) * capacity, -1.0))
                target = jnp.concatenate(targets, axis=1) if group > 1 else targets[0]
                slot = lax.broadcasted_iota(jnp.int32, (group * capacity, group * pad), 0)
                picks = (slot.astype(f32) == target).astype(bf16)
                section_ref[s0 * capacity : (s0 + group) * capacity, :] = dot(
                    picks, rows_ref[s0 * pad : (s0 + group) * pad, :]
                ).astype(bf16)

        section = section_ref[...]
        gate_value = dot(section, gate_ref[...])
        up_value = dot(section, up_ref[...])
        out_ref[...] = (silu(gate_value) * up_value).astype(bf16)

    weight_spec = pl.BlockSpec((width, step), lambda i: (0, i))
    return pl.pallas_call(
        body,
        grid=(hidden // step,),
        out_shape=(
            jax.ShapeDtypeStruct((slots, hidden), bf16),
            jax.ShapeDtypeStruct((sources, 2 * pad), f32),
        ),
        in_specs=[pl.BlockSpec(memory_space=pltpu.SMEM)]
        + whole(len(flat))
        + [weight_spec, weight_spec],
        out_specs=(
            pl.BlockSpec((slots, step), lambda i: (0, i)),
            pl.BlockSpec((sources, 2 * pad), lambda i: (0, 0)),
        ),
        scratch_shapes=[
            pltpu.VMEM((sources * pad, width), bf16),
            pltpu.VMEM((slots, width), bf16),
        ],
        cost_estimate=pl.CostEstimate(
            flops=4 * slots * width * hidden, transcendentals=0, bytes_accessed=0
        ),
    )(index.vector, *flat, gate_weight, up_weight)


def take_block(index, weight, place, hidden):
    columns = weight.shape[1]

    def body(s_ref, in_ref, out_ref):
        out_ref[...] = in_ref[...]

    return pl.pallas_call(
        body,
        out_shape=jax.ShapeDtypeStruct((hidden, columns), weight.dtype),
        grid_spec=pltpu.PrefetchScalarGridSpec(
            num_scalar_prefetch=1,
            grid=(4,),
            in_specs=[pl.BlockSpec((hidden // 4, columns), lambda i, s: (s[place] * 4 + i, 0))],
            out_specs=pl.BlockSpec((hidden // 4, columns), lambda i, s: (i, 0)),
        ),
        cost_estimate=pl.CostEstimate(flops=1 << 20, transcendentals=0, bytes_accessed=0),
    )(index.vector, weight)


def down_first(index, hiddens, weight, traded):
    hidden, columns = hiddens[0].shape[1], weight.shape[1]
    chunks, partners = len(hiddens), len(traded)
    fixed = lambda i, s: (0, 0)

    def body(s_ref, *refs):
        weights = refs[chunks : chunks + 1 + partners]
        outs = refs[chunks + 1 + partners :]
        for w in range(1 + partners):
            for h in range(chunks):
                outs[w * chunks + h][...] = dot(refs[h][...], weights[w][...])

    outs = pl.pallas_call(
        body,
        out_shape=[
            jax.ShapeDtypeStruct((h.shape[0], columns), f32)
            for _ in range(1 + partners)
            for h in hiddens
        ],
        grid_spec=pltpu.PrefetchScalarGridSpec(
            num_scalar_prefetch=1,
            grid=(1,),
            in_specs=[pl.BlockSpec(h.shape, fixed) for h in hiddens]
            + [pl.BlockSpec((hidden, columns), index.block(index.held))]
            + [pl.BlockSpec((hidden, columns), fixed)] * partners,
            out_specs=[
                pl.BlockSpec((h.shape[0], columns), fixed)
                for _ in range(1 + partners)
                for h in hiddens
            ],
        ),
        cost_estimate=pl.CostEstimate(
            flops=2 * sum(h.shape[0] for h in hiddens) * hidden * columns * (1 + partners),
            transcendentals=0,
            bytes_accessed=0,
        ),
    )(index.vector, *hiddens, weight, *traded)
    return [outs[w * chunks : (w + 1) * chunks] for w in range(1 + partners)]


def down_partner(first, hiddens, weights):
    count = len(hiddens)

    def body(first_ref, *refs):
        total = first_ref[...]
        for i in range(count):
            total = total + dot(refs[i][...], refs[count + i][...])
        refs[-1][...] = total.astype(bf16)

    out = jax.ShapeDtypeStruct(first.shape, bf16)
    flops = 2 * first.size * hiddens[0].shape[1] * count
    return call(body, out, (first, *hiddens, *weights), flops)


def down_own(index, firsts, gathered, weight):
    count, chunks = len(gathered), len(firsts)
    hidden, columns = gathered[0][0].shape[1], weight.shape[1]
    fixed = lambda i, s: (0, 0)

    def body(s_ref, *refs):
        hidden_refs = refs[chunks : chunks + count * chunks]
        weight_ref = refs[chunks + count * chunks]
        outs = refs[chunks + count * chunks + 1 :]
        for i in range(count):

            @pl.when(pl.program_id(0) == i)
            def _():
                for h in range(chunks):
                    before = outs[h][...] if i else refs[h][...]
                    outs[h][...] = before + dot(hidden_refs[i * chunks + h][...], weight_ref[...])

    flat = [h for pieces in gathered for h in pieces]
    return pl.pallas_call(
        body,
        out_shape=[jax.ShapeDtypeStruct(f.shape, f32) for f in firsts],
        grid_spec=pltpu.PrefetchScalarGridSpec(
            num_scalar_prefetch=1,
            grid=(count,),
            in_specs=[pl.BlockSpec(f.shape, fixed) for f in firsts]
            + [pl.BlockSpec(h.shape, fixed) for h in flat]
            + [pl.BlockSpec((hidden, columns), index.block(index.held + 1))],
            out_specs=[pl.BlockSpec(f.shape, fixed) for f in firsts],
        ),
        cost_estimate=pl.CostEstimate(
            flops=2 * sum(h.shape[0] for h in flat) * hidden * columns,
            transcendentals=0,
            bytes_accessed=0,
        ),
    )(index.vector, *firsts, *flat, weight)


def combine(own, back, info, tokens, capacity, out_type):
    slots, columns = own.shape
    sources = slots // capacity
    pad = info.shape[1] // 2
    group = group_of(sources, capacity)

    def body(own_ref, info_ref, *refs):
        out_ref = refs[-1]
        for s0 in range(0, sources, group):
            span = slice(s0 * capacity, (s0 + group) * capacity)
            value = own_ref[span, :]
            for ref in refs[:-1]:
                value = value + ref[span, :].astype(f32)
            value = value.astype(bf16)
            for s in range(s0, s0 + group):
                rank = info_ref[s : s + 1, 0:pad]
                target = jnp.where(rank >= 0, rank + (s - s0) * capacity, -1.0)
                slot = lax.broadcasted_iota(jnp.int32, (group * capacity, pad), 0).astype(f32)
                places = jnp.where(slot == target, info_ref[s : s + 1, pad : 2 * pad], 0.0)
                out_ref[s] = dot_tn(places.astype(bf16), value)[0:tokens].astype(out_type)

    out = jax.ShapeDtypeStruct((sources, tokens, columns), out_type)
    return call(body, out, (own, info, *back), 1 << 26)


def local(
    first_batch_queries,
    first_batch_keys,
    first_batch_values,
    output_gate_preactivation,
    decay_preactivation,
    channel_decay_bias,
    added_log_decay,
    head_norm_gain,
    attention_output_weight,
    second_batch_rows,
    expert_norm_gain,
    routed_expert_index,
    router_chosen_scores,
    expert_gate_weight,
    expert_up_weight,
    expert_down_weight,
    shared_gate_weight,
    shared_up_weight,
    shared_down_weight,
):
    at = Places()
    index = Index(at)
    n, chips, experts = at.side, at.chips, at.ep
    heads = added_log_decay.shape[0]
    tokens, top_count = routed_expert_index.shape
    capacity = tokens * top_count * 3 // (2 * experts)
    gate_weight, up_weight, down_weight = (
        expert_gate_weight[0],
        expert_up_weight[0],
        expert_down_weight[0],
    )
    hidden = gate_weight.shape[1]

    def down_block(k, i):
        return take_block(index, down_weight, index.given + (k - 1) * n + i, hidden)

    normed, packed = prepare_rows(
        index,
        n,
        second_batch_rows,
        expert_norm_gain,
        routed_expert_index,
        router_chosen_scores,
        experts,
    )
    far = [at.along_z(packed, k) for k in range(1, chips)]
    early = [down_block(k, 0) for k in range(1, n)]
    o_local, q_device, own_state = local_attention(
        first_batch_queries,
        first_batch_keys,
        first_batch_values,
        decay_preactivation,
        channel_decay_bias,
        added_log_decay,
    )
    far, own_state, early = hold((far, own_state, early))
    traded = [[at.along_v(early[k - 1], k)] for k in range(1, n)]
    arrived = [at.up_z(own_state, hop) for hop in range(1, chips)]
    far = [[a] + [at.along_u(a, i) for i in range(1, n)] for a in far]
    late = [[down_block(k, i) for i in range(1, n)] for k in range(1, n)]
    far, arrived, late = hold((far, arrived, late))
    states = [at.to_sibling(own_state)]
    for state in arrived:
        states += [state, at.to_sibling(state)]
    for k in range(1, n):
        traded[k - 1] += [at.along_v(block, k) for block in late[k - 1]]
    ups = [expert_up(index, (normed, packed), far, capacity, gate_weight, up_weight)]
    other = (
        (at.to_sibling(normed), at.to_sibling(packed)),
        [[at.to_sibling(p) for p in pieces] for pieces in far],
    )
    gathered_first = [at.along_u(ups[0][0], i) for i in range(1, n)]
    _, other = hold((ups[0][0], other))
    ups.append(expert_up(index, *other, capacity, gate_weight, up_weight))
    hiddens = [up[0] for up in ups]
    gathered_second = [at.along_u(hiddens[1], i) for i in range(1, n)]
    both = finish_attention(
        index,
        o_local,
        q_device,
        states,
        output_gate_preactivation,
        head_norm_gain,
        heads,
        normed,
        shared_gate_weight,
        shared_up_weight,
    )
    firsts = down_first(index, hiddens, down_weight, [t[0] for t in traded])

    def partials(chunk, gathered):
        return [
            down_partner(firsts[k][chunk], gathered, traded[k - 1][1:]) for k in range(1, n)
        ]

    partial = partials(0, gathered_first)
    back = [[at.along_v(partial[k - 1], -k) for k in range(1, n)]]
    gathered_second, both, _ = hold((gathered_second, both, partial))
    partial = partials(1, gathered_second)
    back.append([at.along_v(partial[k - 1], -k) for k in range(1, n)])
    gathered = [list(pair) for pair in zip(gathered_first, gathered_second)]
    owns = down_own(index, firsts[0], gathered, down_weight)
    here, there = [
        combine(owns[chunk], back[chunk], ups[chunk][1], tokens, capacity, (f32, bf16)[chunk])
        for chunk in range(2)
    ]
    there, to_send = hold((there, both))
    from_sibling = at.to_sibling(there)
    chip_sum = here + from_sibling.astype(f32)
    routed_total = chip_sum[0]
    for k in range(1, chips):
        routed_total = routed_total + at.along_z(chip_sum[k].astype(bf16), -k).astype(f32)

    mixed = [
        both if dy == 0 and dx == 0 else at.along_tp(to_send, dy, dx)
        for dy in range(n)
        for dx in range(n)
    ]
    token_mixed, shared_total = project(
        index, mixed, attention_output_weight, shared_down_weight, tokens
    )
    channel_mixed = (routed_total + shared_total).astype(bf16)
    return (token_mixed, channel_mixed)


def solution(mesh):
    placed = (
        P("ep", "tp"),
        P("ep", "tp"),
        P("ep", "tp"),
        P("ep", "tp"),
        P("ep", "tp"),
        P("tp"),
        P("tp", "ep"),
        P("tp"),
        P(None, "tp"),
        P("ep", None),
        P(),
        P("ep", None),
        P("ep", None),
        P("ep", None, "tp"),
        P("ep", None, "tp"),
        P("ep", None, "tp"),
        P(None, "tp"),
        P(None, "tp"),
        P(None, "tp"),
    )

    return jax.shard_map(
        local, mesh=mesh, in_specs=placed, out_specs=(P("ep", "tp"), P("ep", "tp")), check_vma=False
    )
```

profile of v0, /device:TPU:0, one launch (start us, length us, event | category | flops | bytes accessed | tf_op | source)
XLA Modules:
  0.0 129.2 jit_solution(8633258783968478676)
XLA Ops:
  0.6 1.3 dynamic-slice_bitcast_fusion.s_ref
  1.9 2.0 %shard_map.203 = (bf16[96,2048]{1,0:T(8,128)(2,1)}, bf16[104,1024]{1,0:T(8,128)(2,1)}) custom-call(s32[12]{0:T(128)} %dynamic-slice_bitcast_fusion.s_ref, bf16[96,2048]{1,0:T(8,128)(2,1)} %rows_ref.1, f32[1,2048]{1,0:T(1,128)} %bitcast.36, s32[4,96]{1,0:T(4,128)} %bitcast.37, f32[4,96]{1,0:T(4,128)} %bitcast.38), custom_call_target="tpu_custom_call" | custom-call | flops 4194304 | tf_op jit(solution)/shard_map/pallas_call | solution.py:119
  4.0 3.1 %collective-permute-start = (bf16[104,1024]{1,0:T(8,128)(2,1)}, bf16[104,1024]{1,0:T(8,128)(2,1)S(1)}, u32[]{:S(2)}, u32[]{:S(2)}) collective-permute-start(bf16[104,1024]{1,0:T(8,128)(2,1)} %get-tuple-element.47.refs_1_), channel_id=1, source_target_pairs={{0,8},{1,9},{2,10},{3,11},{4,12},{5,13},{6,14},{7,15},{8,16},{9,17... | collective-permute-start | bytes 638984 | tf_op jit(solution)/shard_map/ppermute | solution.py:40
  7.0 2.6 %collective-permute-start.1 = (bf16[104,1024]{1,0:T(8,128)(2,1)}, bf16[104,1024]{1,0:T(8,128)(2,1)S(1)}, u32[]{:S(2)}, u32[]{:S(2)}) collective-permute-start(bf16[104,1024]{1,0:T(8,128)(2,1)} %get-tuple-element.47.refs_1_), channel_id=1, source_target_pairs={{0,16},{1,17},{2,18},{3,19},{4,20},{5,21},{6,22},{7,23},{8,24},{9,... | collective-permute-start | bytes 638984 | tf_op jit(solution)/shard_map/ppermute | solution.py:40
  9.6 1.3 %collective-permute-start.2 = (bf16[104,1024]{1,0:T(8,128)(2,1)}, bf16[104,1024]{1,0:T(8,128)(2,1)S(1)}, u32[]{:S(2)}, u32[]{:S(2)}) collective-permute-start(bf16[104,1024]{1,0:T(8,128)(2,1)} %get-tuple-element.47.refs_1_), channel_id=1, source_target_pairs={{0,24},{1,25},{2,26},{3,27},{4,28},{5,29},{6,30},{7,31},{8,0},{9,1... | collective-permute-start | bytes 638984 | tf_op jit(solution)/shard_map/ppermute | solution.py:40
  11.0 4.0 %shard_map.205 = bf16[1024,512]{1,0:T(8,128)(2,1)} custom-call(s32[12]{0:T(128)} %dynamic-slice_bitcast_fusion.s_ref, bf16[4096,512]{1,0:T(8,128)(2,1)} %bitcast.28), custom_call_target="tpu_custom_call" | custom-call | flops 1048576 | tf_op jit(solution)/shard_map/pallas_call | solution.py:429
  15.0 5.2 %shard_map.204 = (f32[256,512]{1,0:T(8,128)}, bf16[256,256]{1,0:T(8,128)(2,1)}, bf16[136,256]{1,0:T(8,128)(2,1)}) custom-call(bf16[256,256]{1,0:T(8,128)(2,1)} %q_ref.1, bf16[256,256]{1,0:T(8,128)(2,1)} %k_ref.1, bf16[256,512]{1,0:T(8,128)(2,1)} %v_ref.1, bf16[256,256]{1,0:T(8,128)(2,1)} %d_ref.1, f32[1,256]{1,0:T(1,128)} %bitcast.40, f32[4,256]{1,0:T(4,128)} %added_ref.1), custom_call_target="tpu_custom_call" | custom-call | flops 33554432 | tf_op jit(solution)/shard_map/pallas_call | solution.py:119
  20.2 3.5 %collective-permute-done.1.refs_4_ = bf16[104,1024]{1,0:T(8,128)(2,1)S(1)} collective-permute-done((bf16[104,1024]{1,0:T(8,128)(2,1)}, bf16[104,1024]{1,0:T(8,128)(2,1)S(1)}, u32[]{:S(2)}, u32[]{:S(2)}) %collective-permute-start.1) | collective-permute-done | bytes 213024 | tf_op jit(solution)/shard_map/ppermute | solution.py:40
  23.8 6.9 %collective-permute-start.6 = (bf16[136,256]{1,0:T(8,128)(2,1)}, bf16[136,256]{1,0:T(8,128)(2,1)S(1)}, u32[]{:S(2)}, u32[]{:S(2)}) collective-permute-start(bf16[136,256]{1,0:T(8,128)(2,1)} %get-tuple-element.52), channel_id=1, source_target_pairs={{0,8},{1,9},{2,10},{3,11},{4,12},{5,13},{6,14},{7,15},{8,16},{9,17... | collective-permute-start | bytes 208904 | tf_op jit(solution)/shard_map/ppermute | solution.py:40
  30.7 3.5 %collective-permute-start.7 = (bf16[136,256]{1,0:T(8,128)(2,1)}, bf16[136,256]{1,0:T(8,128)(2,1)S(1)}, u32[]{:S(2)}, u32[]{:S(2)}) collective-permute-start(bf16[136,256]{1,0:T(8,128)(2,1)} %get-tuple-element.52), channel_id=1, source_target_pairs={{0,16},{1,17},{2,18},{3,19},{4,20},{5,21},{6,22},{7,23},{8,24},{9,... | collective-permute-start | bytes 208904 | tf_op jit(solution)/shard_map/ppermute | solution.py:40
  34.2 1.9 %collective-permute-start.8 = (bf16[136,256]{1,0:T(8,128)(2,1)}, bf16[136,256]{1,0:T(8,128)(2,1)}, u32[]{:S(2)}, u32[]{:S(2)}) collective-permute-start(bf16[136,256]{1,0:T(8,128)(2,1)} %get-tuple-element.52), channel_id=1, source_target_pairs={{0,24},{1,25},{2,26},{3,27},{4,28},{5,29},{6,30},{7,31}} | collective-permute-start | bytes 208904 | tf_op jit(solution)/shard_map/ppermute | solution.py:40
  36.1 1.5 %collective-permute-start.3 = (bf16[104,1024]{1,0:T(8,128)(2,1)S(1)}, bf16[104,1024]{1,0:T(8,128)(2,1)S(1)}, u32[]{:S(2)}, u32[]{:S(2)}) collective-permute-start(bf16[104,1024]{1,0:T(8,128)(2,1)S(1)} %collective-permute-done.refs_2_), channel_id=1, source_target_pairs={{0,1},{1,0},{2,3},{3,2},{4,6},{5,7},{6,4},{7,5},{8,9},{9,8},{10,11... | collective-permute-start | bytes 638984 | tf_op jit(solution)/shard_map/ppermute | solution.py:40
  37.6 0.5 collective-permute-start.4
  38.2 1.5 %collective-permute-start.5 = (bf16[104,1024]{1,0:T(8,128)(2,1)S(1)}, bf16[104,1024]{1,0:T(8,128)(2,1)S(1)}, u32[]{:S(2)}, u32[]{:S(2)}) collective-permute-start(bf16[104,1024]{1,0:T(8,128)(2,1)S(1)} %collective-permute-done.2.refs_6_), channel_id=1, source_target_pairs={{0,1},{1,0},{2,3},{3,2},{4,6},{5,7},{6,4},{7,5},{8,9},{9,8},{10,11... | collective-permute-start | bytes 638984 | tf_op jit(solution)/shard_map/ppermute | solution.py:40
  39.8 0.5 collective-permute-start.10
  40.3 4.0 %shard_map.206 = bf16[1024,512]{1,0:T(8,128)(2,1)} custom-call(s32[12]{0:T(128)} %dynamic-slice_bitcast_fusion.s_ref, bf16[4096,512]{1,0:T(8,128)(2,1)} %bitcast.29), custom_call_target="tpu_custom_call" | custom-call | flops 1048576 | tf_op jit(solution)/shard_map/pallas_call | solution.py:429
  44.3 2.2 %collective-permute-done.5.refs_7_ = bf16[104,1024]{1,0:T(8,128)(2,1)S(1)} collective-permute-done((bf16[104,1024]{1,0:T(8,128)(2,1)S(1)}, bf16[104,1024]{1,0:T(8,128)(2,1)S(1)}, u32[]{:S(2)}, u32[]{:S(2)}) %collective-permute-start.5) | collective-permute-done | bytes 213024 | tf_op jit(solution)/shard_map/ppermute | solution.py:40
  46.6 0.5 collective-permute-start.12
  47.1 1.6 %collective-permute-start.22 = (bf16[1024,512]{1,0:T(8,128)(2,1)}, bf16[1024,512]{1,0:T(8,128)(2,1)}, u32[]{:S(2)}, u32[]{:S(2)}) collective-permute-start(bf16[1024,512]{1,0:T(8,128)(2,1)} %shard_map.205), channel_id=1, source_target_pairs={{0,2},{1,3},{2,0},{3,1},{4,5},{5,4},{6,7},{7,6},{8,10},{9,11},{10,... | collective-permute-start | bytes 3145736 | tf_op jit(solution)/shard_map/ppermute | solution.py:40
  48.7 0.5 collective-permute-start.24
  49.2 0.5 collective-permute-start.15
  49.7 0.2 copy-done.21
  49.9 0.5 collective-permute-start.16
  50.4 0.2 copy-done.22
  50.6 7.7 %shard_map.207 = (bf16[288,1024]{1,0:T(8,128)(2,1)}, f32[4,256]{1,0:T(4,128)}) custom-call(s32[12]{0:T(128)} %dynamic-slice_bitcast_fusion.s_ref, bf16[96,2048]{1,0:T(8,128)(2,1)} %get-tuple-element.46.refs_0_.normed_ref, bf16[104,1024]{1,0:T(8,128)(2,1)} %get-tuple-element.47.refs_1_, bf16[104,1024]{1,0:T(8,128)(2,1)} %copy-done.14, ...), custom_call_target="tpu_custom_call" | custom-call | flops 2415919104 | tf_op jit(solution)/shard_map/pallas_call | solution.py:399
  58.4 0.7 copy-done.23
  59.1 1.5 %collective-permute-start.23 = (bf16[288,1024]{1,0:T(8,128)(2,1)}, bf16[288,1024]{1,0:T(8,128)(2,1)S(1)}, u32[]{:S(2)}, u32[]{:S(2)}) collective-permute-start(bf16[288,1024]{1,0:T(8,128)(2,1)} %get-tuple-element.59.refs_0_), channel_id=1, source_target_pairs={{0,1},{1,0},{2,3},{3,2},{4,6},{5,7},{6,4},{7,5},{8,9},{9,8},{10,11... | collective-permute-start | bytes 1769480 | tf_op jit(solution)/shard_map/ppermute | solution.py:40
  60.6 7.7 %shard_map.208 = (bf16[288,1024]{1,0:T(8,128)(2,1)}, f32[4,256]{1,0:T(4,128)}) custom-call(s32[12]{0:T(128)} %dynamic-slice_bitcast_fusion.s_ref, bf16[96,2048]{1,0:T(8,128)(2,1)} %copy-done.5, bf16[104,1024]{1,0:T(8,128)(2,1)} %copy-done.19, bf16[104,1024]{1,0:T(8,128)(2,1)} %copy-done.20, bf16[104,1024]{1,0:T(8,128)(2,1)} %copy-done.21, ...), custom_call_target="tpu_custom_call" | custom-call | flops 2415919104 | tf_op jit(solution)/shard_map/pallas_call | solution.py:399
  68.3 0.5 collective-permute-start.17
  68.8 1.3 collective-permute-done.18.refs_0_
  70.1 0.2 collective-permute-start.19
  70.2 1.1 collective-permute-done.19.refs_2_
  71.3 0.2 collective-permute-start.20
  71.5 1.1 collective-permute-done.20.refs_4_
  72.6 0.2 collective-permute-start.21
  72.8 1.3 %collective-permute-done.21.refs_6_ = bf16[136,256]{1,0:T(8,128)(2,1)S(1)} collective-permute-done((bf16[136,256]{1,0:T(8,128)(2,1)}, bf16[136,256]{1,0:T(8,128)(2,1)S(1)}, u32[]{:S(2)}, u32[]{:S(2)}) %collective-permute-start.21) | collective-permute-done | bytes 69664 | tf_op jit(solution)/shard_map/ppermute | solution.py:40
  74.1 0.6 copy-done.29
  74.7 3.5 %shard_map.209.refs_0_ = bf16[304,512]{1,0:T(8,128)(2,1)} custom-call(s32[12]{0:T(128)} %dynamic-slice_bitcast_fusion.s_ref, f32[256,512]{1,0:T(8,128)} %get-tuple-element.69.local_ref, bf16[256,256]{1,0:T(8,128)(2,1)} %get-tuple-element.70.qd_ref, bf16[256,512]{1,0:T(8,128)(2,1)} %gate_ref.1, f32[1,512]{1,0:T(1,128)} %bitcast.39, ...), custom_call_target="tpu_custom_call" | custom-call | flops 134217728 | tf_op jit(solution)/shard_map/pallas_call | solution.py:119
  78.2 4.8 %shard_map.210 = (f32[288,512]{1,0:T(8,128)}, f32[288,512]{1,0:T(8,128)}, f32[288,512]{1,0:T(8,128)}, f32[288,512]{1,0:T(8,128)}) custom-call(s32[12]{0:T(128)} %dynamic-slice_bitcast_fusion.s_ref, bf16[288,1024]{1,0:T(8,128)(2,1)} %get-tuple-element.59.refs_0_, bf16[288,1024]{1,0:T(8,128)(2,1)} %get-tuple-element.68.refs_1_, bf16[4096,512]{1,0:T(8,128)(2,1)} %bitcast.30, ...), custom_call_target="tpu_custom_call" | custom-call | flops 1207959552 | tf_op jit(solution)/shard_map/pallas_call | solution.py:454
  83.0 1.4 %collective-permute-done.24.refs_1_ = bf16[1024,512]{1,0:T(8,128)(2,1)S(1)} collective-permute-done((bf16[1024,512]{1,0:T(8,128)(2,1)}, bf16[1024,512]{1,0:T(8,128)(2,1)S(1)}, u32[]{:S(2)}, u32[]{:S(2)}) %collective-permute-start.24) | collective-permute-done | bytes 1048608 | tf_op jit(solution)/shard_map/ppermute | solution.py:40
  84.4 1.0 copy-done
  85.5 2.8 %shard_map.211 = bf16[288,512]{1,0:T(8,128)(2,1)} custom-call(f32[288,512]{1,0:T(8,128)} %get-tuple-element.75.first_ref, bf16[288,1024]{1,0:T(8,128)(2,1)} %copy-done.1, bf16[1024,512]{1,0:T(8,128)(2,1)} %copy-done), custom_call_target="tpu_custom_call" | custom-call | flops 301989888 | tf_op jit(solution)/shard_map/pallas_call | solution.py:119
  88.2 0.8 copy-done.2
  89.1 2.8 %shard_map.213 = bf16[288,512]{1,0:T(8,128)(2,1)} custom-call(f32[288,512]{1,0:T(8,128)} %get-tuple-element.83.first_ref, bf16[288,1024]{1,0:T(8,128)(2,1)} %copy-done.2, bf16[1024,512]{1,0:T(8,128)(2,1)} %copy-done), custom_call_target="tpu_custom_call" | custom-call | flops 301989888 | tf_op jit(solution)/shard_map/pallas_call | solution.py:119
  91.8 1.5 %collective-permute-start.25 = (bf16[288,512]{1,0:T(8,128)(2,1)}, bf16[288,512]{1,0:T(8,128)(2,1)S(1)}, u32[]{:S(2)}, u32[]{:S(2)}) collective-permute-start(bf16[288,512]{1,0:T(8,128)(2,1)} %shard_map.213), channel_id=1, source_target_pairs={{0,2},{1,3},{2,0},{3,1},{4,5},{5,4},{6,7},{7,6},{8,10},{9,11},{10,... | collective-permute-start | bytes 884744 | tf_op jit(solution)/shard_map/ppermute | solution.py:40
  93.4 4.2 %shard_map.212 = (f32[288,512]{1,0:T(8,128)}, f32[288,512]{1,0:T(8,128)}) custom-call(s32[12]{0:T(128)} %dynamic-slice_bitcast_fusion.s_ref, f32[288,512]{1,0:T(8,128)} %get-tuple-element.78.refs_0_, f32[288,512]{1,0:T(8,128)} %get-tuple-element.79.refs_1_, bf16[288,1024]{1,0:T(8,128)(2,1)} %copy-done.1, bf16[288,1024]{1,0:T(8,128)(2,1)} %copy-done.2, ...), custom_call_target="tpu_custom_call" | custom-call | flops 603979776 | tf_op jit(solution)/shard_map/pallas_call | solution.py:514
  97.6 1.2 collective-permute-done.25.refs_0_
  98.8 0.7 copy-done.11
  99.5 2.2 %shard_map.214 = bf16[4,96,512]{2,1,0:T(8,128)(2,1)} custom-call(f32[288,512]{1,0:T(8,128)} %get-tuple-element.81.own_ref, f32[4,256]{1,0:T(4,128)} %get-tuple-element.82.info_ref, bf16[288,512]{1,0:T(8,128)(2,1)} %copy-done.11), custom_call_target="tpu_custom_call" | custom-call | flops 67108864 | tf_op jit(solution)/shard_map/pallas_call | solution.py:119
  101.8 1.5 %collective-permute-start.29 = (bf16[288,512]{1,0:T(8,128)(2,1)S(1)}, bf16[288,512]{1,0:T(8,128)(2,1)S(1)}, u32[]{:S(2)}, u32[]{:S(2)}) collective-permute-start(bf16[288,512]{1,0:T(8,128)(2,1)S(1)} %copy-done.9), channel_id=1, source_target_pairs={{0,2},{1,3},{2,0},{3,1},{4,5},{5,4},{6,7},{7,6},{8,10},{9,11},{10,... | collective-permute-start | bytes 884744 | tf_op jit(solution)/shard_map/ppermute | solution.py:40
  103.3 1.5 %collective-permute-start.26 = (bf16[304,512]{1,0:T(8,128)(2,1)S(1)}, bf16[304,512]{1,0:T(8,128)(2,1)S(1)}, u32[]{:S(2)}, u32[]{:S(2)}) collective-permute-start(bf16[304,512]{1,0:T(8,128)(2,1)S(1)} %copy-done.4), channel_id=1, source_target_pairs={{0,1},{1,0},{2,3},{3,2},{4,5},{5,4},{6,7},{7,6},{8,9},{9,8},{10,11... | collective-permute-start | bytes 933896 | tf_op jit(solution)/shard_map/ppermute | solution.py:40
  104.8 0.5 collective-permute-start.27
  105.3 1.5 %collective-permute-start.28 = (bf16[304,512]{1,0:T(8,128)(2,1)S(1)}, bf16[304,512]{1,0:T(8,128)(2,1)S(1)}, u32[]{:S(2)}, u32[]{:S(2)}) collective-permute-start(bf16[304,512]{1,0:T(8,128)(2,1)S(1)} %copy-done.4), channel_id=1, source_target_pairs={{0,3},{1,2},{2,1},{3,0},{4,7},{5,6},{6,5},{7,4},{8,11},{9,10},{10,... | collective-permute-start | bytes 933896 | tf_op jit(solution)/shard_map/ppermute | solution.py:40
  106.8 3.9 %collective-permute-done.29.refs_0_ = bf16[288,512]{1,0:T(8,128)(2,1)S(1)} collective-permute-done((bf16[288,512]{1,0:T(8,128)(2,1)S(1)}, bf16[288,512]{1,0:T(8,128)(2,1)S(1)}, u32[]{:S(2)}, u32[]{:S(2)}) %collective-permute-start.29) | collective-permute-done | bytes 294944 | tf_op jit(solution)/shard_map/ppermute | solution.py:40
  110.6 0.7 copy-done.10
  111.3 2.4 %shard_map.216 = f32[4,96,512]{2,1,0:T(8,128)} custom-call(f32[288,512]{1,0:T(8,128)} %get-tuple-element.86.own_ref, f32[4,256]{1,0:T(4,128)} %get-tuple-element.87.info_ref, bf16[288,512]{1,0:T(8,128)(2,1)} %copy-done.10), custom_call_target="tpu_custom_call" | custom-call | flops 67108864 | tf_op jit(solution)/shard_map/pallas_call | solution.py:119
  113.8 1.3 fusion.5
  115.1 0.5 collective-permute-start.32
  115.7 3.4 %collective-permute-start.31 = (bf16[96,512]{1,0:T(8,128)(2,1)S(1)}, bf16[96,512]{1,0:T(8,128)(2,1)S(1)}, u32[]{:S(2)}, u32[]{:S(2)}) collective-permute-start(bf16[96,512]{1,0:T(8,128)(2,1)S(1)} %get-tuple-element.92), channel_id=1, source_target_pairs={{0,24},{1,25},{2,26},{3,27},{4,28},{5,29},{6,30},{7,31},{8,0},{9,1... | collective-permute-start | bytes 294920 | tf_op jit(solution)/shard_map/ppermute | solution.py:40
  119.0 1.9 %collective-permute-done.27.refs_2_ = bf16[304,512]{1,0:T(8,128)(2,1)S(1)} collective-permute-done((bf16[304,512]{1,0:T(8,128)(2,1)S(1)}, bf16[304,512]{1,0:T(8,128)(2,1)S(1)}, u32[]{:S(2)}, u32[]{:S(2)}) %collective-permute-start.27) | collective-permute-done | bytes 311328 | tf_op jit(solution)/shard_map/ppermute | solution.py:40
  120.9 0.7 copy-done.7
  121.6 0.7 copy-done.8
  122.3 5.2 %shard_map.215 = (bf16[256,512]{1,0:T(8,128)(2,1)}, f32[96,512]{1,0:T(8,128)}) custom-call(s32[12]{0:T(128)} %dynamic-slice_bitcast_fusion.s_ref, bf16[304,512]{1,0:T(8,128)(2,1)} %shard_map.209.refs_0_, bf16[304,512]{1,0:T(8,128)(2,1)} %copy-done.6, bf16[304,512]{1,0:T(8,128)(2,1)} %copy-done.7, bf16[304,512]{1,0:T(8,128)(2,1)} %copy-done.8, ...), custom_call_target="tpu_custom_call" | custom-call | flops 637534208 | tf_op jit(solution)/shard_map/pallas_call | solution.py:266
  127.5 1.6 %fusion.4 = bf16[96,512]{1,0:T(8,128)(2,1)} fusion(f32[96,512]{1,0:T(8,128)} %get-tuple-element.89, f32[4,96,512]{2,1,0:T(8,128)S(1)} %get-tuple-element.91, bf16[96,512]{1,0:T(8,128)(2,1)S(1)} %collective-permute-done.33, bf16[96,512]{1,0:T(8,128)(2,1)S(1)} %collective-permute-done.32, bf16[96,512]{1,0:T(8,128)(2,1)S(1)} %collective-permute-done.31), kind=kLoop, calls=%fused_computation.6 | loop fusion | flops 393216 | bytes 786432 | tf_op jit(solution)/shard_map/convert_element_type | solution.py:680
  (84 shorter events, 0.3 us)
Async XLA Ops:
  4.0 35.7 %copy-start.3 = (bf16[96,2048]{1,0:T(8,128)(2,1)S(1)}, bf16[96,2048]{1,0:T(8,128)(2,1)}, u32[]{:S(2)}) copy-start(bf16[96,2048]{1,0:T(8,128)(2,1)} %get-tuple-element.46.refs_0_.normed_ref) | copy-start | bytes 1179652
  4.0 35.8 %copy-start.12 = (bf16[104,1024]{1,0:T(8,128)(2,1)S(1)}, bf16[104,1024]{1,0:T(8,128)(2,1)}, u32[]{:S(2)}) copy-start(bf16[104,1024]{1,0:T(8,128)(2,1)} %get-tuple-element.47.refs_1_) | copy-start | bytes 638980
  4.0 16.3 %collective-permute-start = (bf16[104,1024]{1,0:T(8,128)(2,1)}, bf16[104,1024]{1,0:T(8,128)(2,1)S(1)}, u32[]{:S(2)}, u32[]{:S(2)}) collective-permute-start(bf16[104,1024]{1,0:T(8,128)(2,1)} %get-tuple-element.47.refs_1_), channel_id=1, source_target_pairs={{0,8},{1,9},{2,10},{3,11},{4,12},{5,13},{6,14},{7,15},{8,16},{9,17... | collective-permute-start | bytes 638984 | tf_op jit(solution)/shard_map/ppermute | solution.py:40
  7.0 16.8 %collective-permute-start.1 = (bf16[104,1024]{1,0:T(8,128)(2,1)}, bf16[104,1024]{1,0:T(8,128)(2,1)S(1)}, u32[]{:S(2)}, u32[]{:S(2)}) collective-permute-start(bf16[104,1024]{1,0:T(8,128)(2,1)} %get-tuple-element.47.refs_1_), channel_id=1, source_target_pairs={{0,16},{1,17},{2,18},{3,19},{4,20},{5,21},{6,22},{7,23},{8,24},{9,... | collective-permute-start | bytes 638984 | tf_op jit(solution)/shard_map/ppermute | solution.py:40
  9.6 14.2 %collective-permute-start.2 = (bf16[104,1024]{1,0:T(8,128)(2,1)}, bf16[104,1024]{1,0:T(8,128)(2,1)S(1)}, u32[]{:S(2)}, u32[]{:S(2)}) collective-permute-start(bf16[104,1024]{1,0:T(8,128)(2,1)} %get-tuple-element.47.refs_1_), channel_id=1, source_target_pairs={{0,24},{1,25},{2,26},{3,27},{4,28},{5,29},{6,30},{7,31},{8,0},{9,1... | collective-permute-start | bytes 638984 | tf_op jit(solution)/shard_map/ppermute | solution.py:40
  20.2 30.4 %copy-start.14 = (bf16[104,1024]{1,0:T(8,128)(2,1)}, bf16[104,1024]{1,0:T(8,128)(2,1)S(1)}, u32[]{:S(2)}) copy-start(bf16[104,1024]{1,0:T(8,128)(2,1)S(1)} %collective-permute-done.refs_2_) | copy-start | bytes 638980
  23.8 26.8 %copy-start.15 = (bf16[104,1024]{1,0:T(8,128)(2,1)}, bf16[104,1024]{1,0:T(8,128)(2,1)S(1)}, u32[]{:S(2)}) copy-start(bf16[104,1024]{1,0:T(8,128)(2,1)S(1)} %collective-permute-done.1.refs_4_) | copy-start | bytes 638980
  23.8 26.8 %copy-start.13 = (bf16[104,1024]{1,0:T(8,128)(2,1)}, bf16[104,1024]{1,0:T(8,128)(2,1)S(1)}, u32[]{:S(2)}) copy-start(bf16[104,1024]{1,0:T(8,128)(2,1)S(1)} %collective-permute-done.2.refs_6_) | copy-start | bytes 638980
  23.8 14.4 %collective-permute-start.6 = (bf16[136,256]{1,0:T(8,128)(2,1)}, bf16[136,256]{1,0:T(8,128)(2,1)S(1)}, u32[]{:S(2)}, u32[]{:S(2)}) collective-permute-start(bf16[136,256]{1,0:T(8,128)(2,1)} %get-tuple-element.52), channel_id=1, source_target_pairs={{0,8},{1,9},{2,10},{3,11},{4,12},{5,13},{6,14},{7,15},{8,16},{9,17... | collective-permute-start | bytes 208904 | tf_op jit(solution)/shard_map/ppermute | solution.py:40
  30.7 8.9 %collective-permute-start.7 = (bf16[136,256]{1,0:T(8,128)(2,1)}, bf16[136,256]{1,0:T(8,128)(2,1)S(1)}, u32[]{:S(2)}, u32[]{:S(2)}) collective-permute-start(bf16[136,256]{1,0:T(8,128)(2,1)} %get-tuple-element.52), channel_id=1, source_target_pairs={{0,16},{1,17},{2,18},{3,19},{4,20},{5,21},{6,22},{7,23},{8,24},{9,... | collective-permute-start | bytes 208904 | tf_op jit(solution)/shard_map/ppermute | solution.py:40
  34.2 5.5 %collective-permute-start.8 = (bf16[136,256]{1,0:T(8,128)(2,1)}, bf16[136,256]{1,0:T(8,128)(2,1)}, u32[]{:S(2)}, u32[]{:S(2)}) collective-permute-start(bf16[136,256]{1,0:T(8,128)(2,1)} %get-tuple-element.52), channel_id=1, source_target_pairs={{0,24},{1,25},{2,26},{3,27},{4,28},{5,29},{6,30},{7,31}} | collective-permute-start | bytes 208904 | tf_op jit(solution)/shard_map/ppermute | solution.py:40
  36.1 8.2 %collective-permute-start.3 = (bf16[104,1024]{1,0:T(8,128)(2,1)S(1)}, bf16[104,1024]{1,0:T(8,128)(2,1)S(1)}, u32[]{:S(2)}, u32[]{:S(2)}) collective-permute-start(bf16[104,1024]{1,0:T(8,128)(2,1)S(1)} %collective-permute-done.refs_2_), channel_id=1, source_target_pairs={{0,1},{1,0},{2,3},{3,2},{4,6},{5,7},{6,4},{7,5},{8,9},{9,8},{10,11... | collective-permute-start | bytes 638984 | tf_op jit(solution)/shard_map/ppermute | solution.py:40
  37.6 6.7 %collective-permute-start.4 = (bf16[104,1024]{1,0:T(8,128)(2,1)S(1)}, bf16[104,1024]{1,0:T(8,128)(2,1)S(1)}, u32[]{:S(2)}, u32[]{:S(2)}) collective-permute-start(bf16[104,1024]{1,0:T(8,128)(2,1)S(1)} %collective-permute-done.1.refs_4_), channel_id=1, source_target_pairs={{0,1},{1,0},{2,3},{3,2},{4,6},{5,7},{6,4},{7,5},{8,9},{9,8},{10,11... | collective-permute-start | bytes 638984 | tf_op jit(solution)/shard_map/ppermute | solution.py:40
  38.2 31.9 %copy-start.24 = (bf16[136,256]{1,0:T(8,128)(2,1)}, bf16[136,256]{1,0:T(8,128)(2,1)S(1)}, u32[]{:S(2)}) copy-start(bf16[136,256]{1,0:T(8,128)(2,1)S(1)} %collective-permute-done.6.refs_1_) | copy-start | bytes 208900
  38.2 8.4 %collective-permute-start.5 = (bf16[104,1024]{1,0:T(8,128)(2,1)S(1)}, bf16[104,1024]{1,0:T(8,128)(2,1)S(1)}, u32[]{:S(2)}, u32[]{:S(2)}) collective-permute-start(bf16[104,1024]{1,0:T(8,128)(2,1)S(1)} %collective-permute-done.2.refs_6_), channel_id=1, source_target_pairs={{0,1},{1,0},{2,3},{3,2},{4,6},{5,7},{6,4},{7,5},{8,9},{9,8},{10,11... | collective-permute-start | bytes 638984 | tf_op jit(solution)/shard_map/ppermute | solution.py:40
  39.7 31.7 %copy-start.25 = (bf16[136,256]{1,0:T(8,128)(2,1)}, bf16[136,256]{1,0:T(8,128)(2,1)S(1)}, u32[]{:S(2)}) copy-start(bf16[136,256]{1,0:T(8,128)(2,1)S(1)} %collective-permute-done.7.refs_3_) | copy-start | bytes 208900
  39.7 9.0 %collective-permute-start.9 = (bf16[96,2048]{1,0:T(8,128)(2,1)S(1)}, bf16[96,2048]{1,0:T(8,128)(2,1)S(1)}, u32[]{:S(2)}, u32[]{:S(2)}) collective-permute-start(bf16[96,2048]{1,0:T(8,128)(2,1)S(1)} %copy-done.3), channel_id=1, source_target_pairs={{0,4},{1,5},{2,6},{3,7},{4,0},{5,1},{6,2},{7,3},{8,12},{9,13},{10,... | collective-permute-start | bytes 1179656 | tf_op jit(solution)/shard_map/ppermute | solution.py:40
  39.8 7.3 %collective-permute-start.10 = (bf16[104,1024]{1,0:T(8,128)(2,1)S(1)}, bf16[104,1024]{1,0:T(8,128)(2,1)S(1)}, u32[]{:S(2)}, u32[]{:S(2)}) collective-permute-start(bf16[104,1024]{1,0:T(8,128)(2,1)S(1)} %copy-done.12), channel_id=1, source_target_pairs={{0,4},{1,5},{2,6},{3,7},{4,0},{5,1},{6,2},{7,3},{8,12},{9,13},{10,... | collective-permute-start | bytes 638984 | tf_op jit(solution)/shard_map/ppermute | solution.py:40
  44.3 6.3 %copy-start.17 = (bf16[104,1024]{1,0:T(8,128)(2,1)}, bf16[104,1024]{1,0:T(8,128)(2,1)S(1)}, u32[]{:S(2)}) copy-start(bf16[104,1024]{1,0:T(8,128)(2,1)S(1)} %collective-permute-done.3.refs_3_) | copy-start | bytes 638980
  44.3 6.3 %copy-start.18 = (bf16[104,1024]{1,0:T(8,128)(2,1)}, bf16[104,1024]{1,0:T(8,128)(2,1)S(1)}, u32[]{:S(2)}) copy-start(bf16[104,1024]{1,0:T(8,128)(2,1)S(1)} %collective-permute-done.4.refs_5_) | copy-start | bytes 638980
  46.6 4.1 %copy-start.16 = (bf16[104,1024]{1,0:T(8,128)(2,1)}, bf16[104,1024]{1,0:T(8,128)(2,1)S(1)}, u32[]{:S(2)}) copy-start(bf16[104,1024]{1,0:T(8,128)(2,1)S(1)} %collective-permute-done.5.refs_7_) | copy-start | bytes 638980
  46.6 2.6 %collective-permute-start.11 = (bf16[104,1024]{1,0:T(8,128)(2,1)S(1)}, bf16[104,1024]{1,0:T(8,128)(2,1)S(1)}, u32[]{:S(2)}, u32[]{:S(2)}) collective-permute-start(bf16[104,1024]{1,0:T(8,128)(2,1)S(1)} %collective-permute-done.refs_2_), channel_id=1, source_target_pairs={{0,4},{1,5},{2,6},{3,7},{4,0},{5,1},{6,2},{7,3},{8,12},{9,13},{10,... | collective-permute-start | bytes 638984 | tf_op jit(solution)/shard_map/ppermute | solution.py:40
  46.6 2.6 %collective-permute-start.12 = (bf16[104,1024]{1,0:T(8,128)(2,1)S(1)}, bf16[104,1024]{1,0:T(8,128)(2,1)S(1)}, u32[]{:S(2)}, u32[]{:S(2)}) collective-permute-start(bf16[104,1024]{1,0:T(8,128)(2,1)S(1)} %collective-permute-done.3.refs_3_), channel_id=1, source_target_pairs={{0,4},{1,5},{2,6},{3,7},{4,0},{5,1},{6,2},{7,3},{8,12},{9,13},{10,... | collective-permute-start | bytes 638984 | tf_op jit(solution)/shard_map/ppermute | solution.py:40
  47.1 2.6 %collective-permute-start.13 = (bf16[104,1024]{1,0:T(8,128)(2,1)S(1)}, bf16[104,1024]{1,0:T(8,128)(2,1)S(1)}, u32[]{:S(2)}, u32[]{:S(2)}) collective-permute-start(bf16[104,1024]{1,0:T(8,128)(2,1)S(1)} %collective-permute-done.1.refs_4_), channel_id=1, source_target_pairs={{0,4},{1,5},{2,6},{3,7},{4,0},{5,1},{6,2},{7,3},{8,12},{9,13},{10,... | collective-permute-start | bytes 638984 | tf_op jit(solution)/shard_map/ppermute | solution.py:40
  47.1 11.3 %copy-start.19 = (bf16[104,1024]{1,0:T(8,128)(2,1)}, bf16[104,1024]{1,0:T(8,128)(2,1)S(1)}, u32[]{:S(2)}) copy-start(bf16[104,1024]{1,0:T(8,128)(2,1)S(1)} %collective-permute-done.10.refs_1_) | copy-start | bytes 638980
  47.1 31.2 %collective-permute-start.22 = (bf16[1024,512]{1,0:T(8,128)(2,1)}, bf16[1024,512]{1,0:T(8,128)(2,1)}, u32[]{:S(2)}, u32[]{:S(2)}) collective-permute-start(bf16[1024,512]{1,0:T(8,128)(2,1)} %shard_map.205), channel_id=1, source_target_pairs={{0,2},{1,3},{2,0},{3,1},{4,5},{5,4},{6,7},{7,6},{8,10},{9,11},{10,... | collective-permute-start | bytes 3145736 | tf_op jit(solution)/shard_map/ppermute | solution.py:40
  48.7 9.7 %copy-start.5 = (bf16[96,2048]{1,0:T(8,128)(2,1)}, bf16[96,2048]{1,0:T(8,128)(2,1)S(1)}, u32[]{:S(2)}) copy-start(bf16[96,2048]{1,0:T(8,128)(2,1)S(1)} %collective-permute-done.9.refs_0_) | copy-start | bytes 1179652
  48.7 35.8 %collective-permute-start.24 = (bf16[1024,512]{1,0:T(8,128)(2,1)}, bf16[1024,512]{1,0:T(8,128)(2,1)S(1)}, u32[]{:S(2)}, u32[]{:S(2)}) collective-permute-start(bf16[1024,512]{1,0:T(8,128)(2,1)} %shard_map.206), channel_id=1, source_target_pairs={{0,2},{1,3},{2,0},{3,1},{4,5},{5,4},{6,7},{7,6},{8,10},{9,11},{10,... | collective-permute-start | bytes 3145736 | tf_op jit(solution)/shard_map/ppermute | solution.py:40
  49.2 9.2 %copy-start.20 = (bf16[104,1024]{1,0:T(8,128)(2,1)}, bf16[104,1024]{1,0:T(8,128)(2,1)S(1)}, u32[]{:S(2)}) copy-start(bf16[104,1024]{1,0:T(8,128)(2,1)S(1)} %collective-permute-done.11.refs_2_) | copy-start | bytes 638980
  49.2 9.2 %collective-permute-start.14 = (bf16[104,1024]{1,0:T(8,128)(2,1)S(1)}, bf16[104,1024]{1,0:T(8,128)(2,1)S(1)}, u32[]{:S(2)}, u32[]{:S(2)}) collective-permute-start(bf16[104,1024]{1,0:T(8,128)(2,1)S(1)} %collective-permute-done.4.refs_5_), channel_id=1, source_target_pairs={{0,4},{1,5},{2,6},{3,7},{4,0},{5,1},{6,2},{7,3},{8,12},{9,13},{10,... | collective-permute-start | bytes 638984 | tf_op jit(solution)/shard_map/ppermute | solution.py:40
  49.2 0.7 copy-start.21
  49.2 11.4 %collective-permute-start.15 = (bf16[104,1024]{1,0:T(8,128)(2,1)S(1)}, bf16[104,1024]{1,0:T(8,128)(2,1)}, u32[]{:S(2)}, u32[]{:S(2)}) collective-permute-start(bf16[104,1024]{1,0:T(8,128)(2,1)S(1)} %collective-permute-done.2.refs_6_), channel_id=1, source_target_pairs={{0,4},{1,5},{2,6},{3,7},{4,0},{5,1},{6,2},{7,3},{8,12},{9,13},{10,... | collective-permute-start | bytes 638984 | tf_op jit(solution)/shard_map/ppermute | solution.py:40
  49.9 0.7 copy-start.22
  49.9 10.7 %collective-permute-start.16 = (bf16[104,1024]{1,0:T(8,128)(2,1)S(1)}, bf16[104,1024]{1,0:T(8,128)(2,1)}, u32[]{:S(2)}, u32[]{:S(2)}) collective-permute-start(bf16[104,1024]{1,0:T(8,128)(2,1)S(1)} %collective-permute-done.5.refs_7_), channel_id=1, source_target_pairs={{0,4},{1,5},{2,6},{3,7},{4,0},{5,1},{6,2},{7,3},{8,12},{9,13},{10,... | collective-permute-start | bytes 638984 | tf_op jit(solution)/shard_map/ppermute | solution.py:40
  58.4 0.7 copy-start.23
  59.1 9.7 %copy-start.30 = (bf16[136,256]{1,0:T(8,128)(2,1)S(1)}, bf16[136,256]{1,0:T(8,128)(2,1)}, u32[]{:S(2)}) copy-start(bf16[136,256]{1,0:T(8,128)(2,1)} %get-tuple-element.52) | copy-start | bytes 208900
  59.1 23.9 %collective-permute-start.23 = (bf16[288,1024]{1,0:T(8,128)(2,1)}, bf16[288,1024]{1,0:T(8,128)(2,1)S(1)}, u32[]{:S(2)}, u32[]{:S(2)}) collective-permute-start(bf16[288,1024]{1,0:T(8,128)(2,1)} %get-tuple-element.59.refs_0_), channel_id=1, source_target_pairs={{0,1},{1,0},{2,3},{3,2},{4,6},{5,7},{6,4},{7,5},{8,9},{9,8},{10,11... | collective-permute-start | bytes 1769480 | tf_op jit(solution)/shard_map/ppermute | solution.py:40
  68.3 20.0 %collective-permute-start.17 = (bf16[288,1024]{1,0:T(8,128)(2,1)}, bf16[288,1024]{1,0:T(8,128)(2,1)S(1)}, u32[]{:S(2)}, u32[]{:S(2)}) collective-permute-start(bf16[288,1024]{1,0:T(8,128)(2,1)} %get-tuple-element.68.refs_1_), channel_id=1, source_target_pairs={{0,1},{1,0},{2,3},{3,2},{4,6},{5,7},{6,4},{7,5},{8,9},{9,8},{10,11... | collective-permute-start | bytes 1769480 | tf_op jit(solution)/shard_map/ppermute | solution.py:40
  68.8 1.3 collective-permute-start.18
  70.1 4.0 %copy-start.26 = (bf16[136,256]{1,0:T(8,128)(2,1)}, bf16[136,256]{1,0:T(8,128)(2,1)S(1)}, u32[]{:S(2)}) copy-start(bf16[136,256]{1,0:T(8,128)(2,1)S(1)} %collective-permute-done.18.refs_0_) | copy-start | bytes 208900
  70.1 1.3 collective-permute-start.19
  71.3 2.7 %copy-start.27 = (bf16[136,256]{1,0:T(8,128)(2,1)}, bf16[136,256]{1,0:T(8,128)(2,1)S(1)}, u32[]{:S(2)}) copy-start(bf16[136,256]{1,0:T(8,128)(2,1)S(1)} %collective-permute-done.19.refs_2_) | copy-start | bytes 208900
  71.3 1.3 collective-permute-start.20
  72.6 1.5 %copy-start.28 = (bf16[136,256]{1,0:T(8,128)(2,1)}, bf16[136,256]{1,0:T(8,128)(2,1)S(1)}, u32[]{:S(2)}) copy-start(bf16[136,256]{1,0:T(8,128)(2,1)S(1)} %collective-permute-done.20.refs_4_) | copy-start | bytes 208900
  72.6 1.5 %collective-permute-start.21 = (bf16[136,256]{1,0:T(8,128)(2,1)}, bf16[136,256]{1,0:T(8,128)(2,1)S(1)}, u32[]{:S(2)}, u32[]{:S(2)}) collective-permute-start(bf16[136,256]{1,0:T(8,128)(2,1)} %collective-permute-done.8.refs_5_), channel_id=1, source_target_pairs={{0,4},{1,5},{2,6},{3,7},{4,0},{5,1},{6,2},{7,3},{8,12},{9,13},{10,... | collective-permute-start | bytes 208904 | tf_op jit(solution)/shard_map/ppermute | solution.py:40
  83.0 1.4 %copy-start.1 = (bf16[288,1024]{1,0:T(8,128)(2,1)}, bf16[288,1024]{1,0:T(8,128)(2,1)S(1)}, u32[]{:S(2)}) copy-start(bf16[288,1024]{1,0:T(8,128)(2,1)S(1)} %collective-permute-done.23.refs_0_.refs_2_) | copy-start | bytes 1769476
  84.4 1.0 copy-start
  88.2 0.8 copy-start.2
  91.8 9.9 %copy-start.9 = (bf16[288,512]{1,0:T(8,128)(2,1)S(1)}, bf16[288,512]{1,0:T(8,128)(2,1)}, u32[]{:S(2)}) copy-start(bf16[288,512]{1,0:T(8,128)(2,1)} %shard_map.211) | copy-start | bytes 884740
  91.8 11.4 %copy-start.4 = (bf16[304,512]{1,0:T(8,128)(2,1)S(1)}, bf16[304,512]{1,0:T(8,128)(2,1)}, u32[]{:S(2)}) copy-start(bf16[304,512]{1,0:T(8,128)(2,1)} %shard_map.209.refs_0_) | copy-start | bytes 933892
  91.8 6.9 %collective-permute-start.25 = (bf16[288,512]{1,0:T(8,128)(2,1)}, bf16[288,512]{1,0:T(8,128)(2,1)S(1)}, u32[]{:S(2)}, u32[]{:S(2)}) collective-permute-start(bf16[288,512]{1,0:T(8,128)(2,1)} %shard_map.213), channel_id=1, source_target_pairs={{0,2},{1,3},{2,0},{3,1},{4,5},{5,4},{6,7},{7,6},{8,10},{9,11},{10,... | collective-permute-start | bytes 884744 | tf_op jit(solution)/shard_map/ppermute | solution.py:40
  98.8 0.7 copy-start.11
  101.8 12.0 %collective-permute-start.30 = (bf16[4,96,512]{2,1,0:T(8,128)(2,1)}, bf16[4,96,512]{2,1,0:T(8,128)(2,1)S(1)}, u32[]{:S(2)}, u32[]{:S(2)}) collective-permute-start(bf16[4,96,512]{2,1,0:T(8,128)(2,1)} %shard_map.214), channel_id=1, source_target_pairs={{0,4},{1,5},{2,6},{3,7},{4,0},{5,1},{6,2},{7,3},{8,12},{9,13},{10,... | collective-permute-start | bytes 1179656 | tf_op jit(solution)/shard_map/ppermute | solution.py:40
  101.8 8.9 %collective-permute-start.29 = (bf16[288,512]{1,0:T(8,128)(2,1)S(1)}, bf16[288,512]{1,0:T(8,128)(2,1)S(1)}, u32[]{:S(2)}, u32[]{:S(2)}) collective-permute-start(bf16[288,512]{1,0:T(8,128)(2,1)S(1)} %copy-done.9), channel_id=1, source_target_pairs={{0,2},{1,3},{2,0},{3,1},{4,5},{5,4},{6,7},{7,6},{8,10},{9,11},{10,... | collective-permute-start | bytes 884744 | tf_op jit(solution)/shard_map/ppermute | solution.py:40
  103.3 12.4 %collective-permute-start.26 = (bf16[304,512]{1,0:T(8,128)(2,1)S(1)}, bf16[304,512]{1,0:T(8,128)(2,1)S(1)}, u32[]{:S(2)}, u32[]{:S(2)}) collective-permute-start(bf16[304,512]{1,0:T(8,128)(2,1)S(1)} %copy-done.4), channel_id=1, source_target_pairs={{0,1},{1,0},{2,3},{3,2},{4,5},{5,4},{6,7},{7,6},{8,9},{9,8},{10,11... | collective-permute-start | bytes 933896 | tf_op jit(solution)/shard_map/ppermute | solution.py:40
  104.8 16.1 %collective-permute-start.27 = (bf16[304,512]{1,0:T(8,128)(2,1)S(1)}, bf16[304,512]{1,0:T(8,128)(2,1)S(1)}, u32[]{:S(2)}, u32[]{:S(2)}) collective-permute-start(bf16[304,512]{1,0:T(8,128)(2,1)S(1)} %copy-done.4), channel_id=1, source_target_pairs={{0,2},{1,3},{2,0},{3,1},{4,6},{5,7},{6,4},{7,5},{8,10},{9,11},{10,... | collective-permute-start | bytes 933896 | tf_op jit(solution)/shard_map/ppermute | solution.py:40
  105.3 15.6 %collective-permute-start.28 = (bf16[304,512]{1,0:T(8,128)(2,1)S(1)}, bf16[304,512]{1,0:T(8,128)(2,1)S(1)}, u32[]{:S(2)}, u32[]{:S(2)}) collective-permute-start(bf16[304,512]{1,0:T(8,128)(2,1)S(1)} %copy-done.4), channel_id=1, source_target_pairs={{0,3},{1,2},{2,1},{3,0},{4,7},{5,6},{6,5},{7,4},{8,11},{9,10},{10,... | collective-permute-start | bytes 933896 | tf_op jit(solution)/shard_map/ppermute | solution.py:40
  110.6 0.7 copy-start.10
  115.1 12.4 %collective-permute-start.33 = (bf16[96,512]{1,0:T(8,128)(2,1)S(1)}, bf16[96,512]{1,0:T(8,128)(2,1)S(1)}, u32[]{:S(2)}, u32[]{:S(2)}) collective-permute-start(bf16[96,512]{1,0:T(8,128)(2,1)S(1)} %get-tuple-element.93), channel_id=1, source_target_pairs={{0,8},{1,9},{2,10},{3,11},{4,12},{5,13},{6,14},{7,15},{8,16},{9,17... | collective-permute-start | bytes 294920 | tf_op jit(solution)/shard_map/ppermute | solution.py:40
  115.1 12.4 %collective-permute-start.32 = (bf16[96,512]{1,0:T(8,128)(2,1)S(1)}, bf16[96,512]{1,0:T(8,128)(2,1)S(1)}, u32[]{:S(2)}, u32[]{:S(2)}) collective-permute-start(bf16[96,512]{1,0:T(8,128)(2,1)S(1)} %get-tuple-element.94), channel_id=1, source_target_pairs={{0,16},{1,17},{2,18},{3,19},{4,20},{5,21},{6,22},{7,23},{8,24},{9,... | collective-permute-start | bytes 294920 | tf_op jit(solution)/shard_map/ppermute | solution.py:40
  115.7 5.2 %copy-start.6 = (bf16[304,512]{1,0:T(8,128)(2,1)}, bf16[304,512]{1,0:T(8,128)(2,1)S(1)}, u32[]{:S(2)}) copy-start(bf16[304,512]{1,0:T(8,128)(2,1)S(1)} %collective-permute-done.26.refs_1_) | copy-start | bytes 933892
  115.7 11.9 %collective-permute-start.31 = (bf16[96,512]{1,0:T(8,128)(2,1)S(1)}, bf16[96,512]{1,0:T(8,128)(2,1)S(1)}, u32[]{:S(2)}, u32[]{:S(2)}) collective-permute-start(bf16[96,512]{1,0:T(8,128)(2,1)S(1)} %get-tuple-element.92), channel_id=1, source_target_pairs={{0,24},{1,25},{2,26},{3,27},{4,28},{5,29},{6,30},{7,31},{8,0},{9,1... | collective-permute-start | bytes 294920 | tf_op jit(solution)/shard_map/ppermute | solution.py:40
  120.9 0.7 copy-start.7
  121.6 0.7 copy-start.8
  (1 other events, 0.6 us)
where the time goes:
time: 130 us; the launch traced here: 129 us
  Pallas kernels  58.7 us (45%)
  starting transfers between devices  39.9 us (31%)
  waiting for transfers between devices  18.9 us (15%)
  local copies, waits for them, and re-layouts  7.83 us (6%)
  other arithmetic  2.9 us (2%)
    ppermute x34, starting transfers between devices, send(): return lax.ppermute(value, AXES, self.pairs(move))  39.9 us
    pallas_call x7, Pallas kernels, call(): pl.pallas_call(body, out_shape=outs, in_specs=specs, out_specs=jax.tree.m...  21 us
    ppermute x34, waiting for transfers between devices, send(): return lax.ppermute(value, AXES, self.pairs(move))  18.9 us
    pallas_call x2, Pallas kernels, expert_up(): pl.pallas_call(body, grid=(hidden // step,), out_shape=(jax.ShapeDtypeStr...  15.4 us
    pallas_call x2, Pallas kernels, take_block(): pl.pallas_call(body, out_shape=jax.ShapeDtypeStruct((hidden, columns), we...  8.08 us
    unnamed x62, local copies, waits for them, and re-layouts  6.53 us
    pallas_call x1, Pallas kernels, project(): pl.pallas_call(body, out_shape=(jax.ShapeDtypeStruct((rows, columns), bf1...  5.19 us
    pallas_call x1, Pallas kernels, down_first(): pl.pallas_call(body, out_shape=[jax.ShapeDtypeStruct((h.shape[0], columns...  4.78 us
  transfers between devices with their start and end apart: 34, of which 10 were waited for; matrix products, arithmetic and copies ran while one was open for 1% of the time, Pallas kernels for 40%

commit v1 on v0

--- a/solution.py
+++ b/solution.py
@@ -78,10 +78,6 @@
 
 def silu(value):
     return value / (1.0 + jnp.exp(-value))
-
-
-def whole(count):
-    return [pl.BlockSpec(memory_space=pltpu.VMEM)] * count
 
 
 def column(n, core, x, y, du, dv):
@@ -110,19 +106,25 @@
         self.held, self.given = 4, 4 + n
         self.tp = 4 + n * n
 
-    def block(self, place, count=1):
-        return lambda i, s: (s[place + i], 0)
-
-
-def call(body, outs, operands, flops, smem=0):
-    specs = [pl.BlockSpec(memory_space=pltpu.SMEM)] * smem + whole(len(operands) - smem)
+    def rows(self, s_ref, place, ref, size):
+        start = pl.multiple_of(s_ref[place] * size, size)
+        return ref[pl.ds(start, size), :]
+
+
+def call(body, outs, operands, flops, smem=0, scratch=()):
+    specs = [pl.BlockSpec(memory_space=pltpu.SMEM)] * smem
+    specs += [pl.BlockSpec(memory_space=pltpu.VMEM)] * (len(operands) - smem)
+    given = list(operands[:smem])
+    given += [pltpu.with_memory_space_constraint(v, pltpu.VMEM) for v in operands[smem:]]
     return pl.pallas_call(
         body,
-        out_shape=outs,
+        out_shape=jax.tree.map(lambda o: pltpu.VMEM(o.shape, o.dtype), outs),
         in_specs=specs,
         out_specs=jax.tree.map(lambda _: pl.BlockSpec(memory_space=pltpu.VMEM), outs),
+        scratch_shapes=list(scratch),
+        compiler_params=pltpu.CompilerParams(vmem_limit_bytes=12 << 20),
         cost_estimate=pl.CostEstimate(flops=flops, transcendentals=0, bytes_accessed=0),
-    )(*operands)
+    )(*given)
 
 
 def local_attention(q, k, v, decay_pre, bias, added):
@@ -243,47 +245,24 @@
     rows = folded - part
 
     def body(s_ref, *refs):
-        weight_ref, shared_ref, mixed_ref, out_ref, sum_ref = refs[count:]
+        weight_ref, shared_ref, mixed_ref, out_ref = refs[count:]
+        mixed = shared = 0.0
         for i in range(count):
-
-            @pl.when(pl.program_id(0) == i)
-            def _():
-                ref = refs[i]
-                mixed = dot(ref[0:rows, :], weight_ref[...])
-                units = jnp.concatenate(
-                    [ref[rows:, q * hidden : (q + 1) * hidden] for q in range(sharing)], axis=0
-                )
-                shared = dot(units, shared_ref[...])
-                if i:
-                    mixed, shared = mixed + sum_ref[...], shared + out_ref[...]
-                if i < count - 1:
-                    sum_ref[...] = mixed
-                else:
-                    mixed_ref[...] = mixed.astype(bf16)
-                out_ref[...] = shared
-
-    fixed = lambda i, s: (0, 0)
-    return pl.pallas_call(
-        body,
-        out_shape=(
-            jax.ShapeDtypeStruct((rows, columns), bf16),
-            jax.ShapeDtypeStruct((tokens, columns), f32),
-        ),
-        grid_spec=pltpu.PrefetchScalarGridSpec(
-            num_scalar_prefetch=1,
-            grid=(count,),
-            in_specs=[pl.BlockSpec((folded, width), fixed)] * count
-            + [
-                pl.BlockSpec((width, columns), index.block(index.tp)),
-                pl.BlockSpec((hidden, columns), index.block(index.tp)),
-            ],
-            out_specs=(pl.BlockSpec((rows, columns), fixed), pl.BlockSpec((tokens, columns), fixed)),
-            scratch_shapes=[pltpu.VMEM((rows, columns), f32)],
-        ),
-        cost_estimate=pl.CostEstimate(
-            flops=2 * folded * width * columns * count, transcendentals=0, bytes_accessed=0
-        ),
-    )(index.vector, *gathered, attention_weight, shared_weight)
+            ref = refs[i]
+            mixed = mixed + dot(ref[0:rows, :], index.rows(s_ref, index.tp + i, weight_ref, width))
+            units = jnp.concatenate(
+                [ref[rows:, q * hidden : (q + 1) * hidden] for q in range(sharing)], axis=0
+            )
+            shared = shared + dot(units, index.rows(s_ref, index.tp + i, shared_ref, hidden))
+        mixed_ref[...] = mixed.astype(bf16)
+        out_ref[...] = shared
+
+    outs = (
+        jax.ShapeDtypeStruct((rows, columns), bf16),
+        jax.ShapeDtypeStruct((tokens, columns), f32),
+    )
+    operands = (index.vector, *gathered, attention_weight, shared_weight)
+    return call(body, outs, operands, 2 * folded * width * columns * count, smem=1)
 
 
 def prepare_rows(places, parts, rows, gain, index, scores, experts):
@@ -353,129 +332,77 @@
     def body(s_ref, *refs):
         row_refs = refs[: len(flat)]
         gate_ref, up_ref, out_ref, info_ref, rows_ref, section_ref = refs[len(flat) :]
-
-        @pl.when(pl.program_id(0) == 0)
-        def _():
-            expert = lax.broadcasted_iota(jnp.int32, (extra, 2 * pad), 0) == s_ref[index.e]
-            if pad > tokens:
-                for s in range(sources):
-                    rows_ref[s * pad + tokens : (s + 1) * pad, :] = jnp.zeros(
-                        (pad - tokens, width), bf16
-                    )
-            rows_ref[0:tokens, :] = row_refs[0][...]
-            for q in range(parts):
-
-                @pl.when(s_ref[index.part] == q)
-                def _():
-                    for s in range(1, sources):
-                        for i in range(parts):
-                            to = (q - i) % parts
-                            rows_ref[
-                                s * pad : s * pad + tokens, to * piece : (to + 1) * piece
-                            ] = row_refs[2 + (s - 1) * parts + i][0:tokens, :]
-
-            for s0 in range(0, sources, group):
-                targets = []
-                for s in range(s0, s0 + group):
-                    table_ref = row_refs[2 + (s - 1) * parts if s else 1]
-                    table = table_ref[tokens : tokens + extra, 0 : 2 * pad].astype(f32)
-                    mine = jnp.sum(jnp.where(expert, table, 0.0), axis=0, keepdims=True)
-                    info_ref[s : s + 1, :] = mine
-                    rank = mine[:, 0:pad]
-                    targets.append(jnp.where(rank >= 0, rank + (s - s0) * capacity, -1.0))
-                target = jnp.concatenate(targets, axis=1) if group > 1 else targets[0]
-                slot = lax.broadcasted_iota(jnp.int32, (group * capacity, group * pad), 0)
-                picks = (slot.astype(f32) == target).astype(bf16)
-                section_ref[s0 * capacity : (s0 + group) * capacity, :] = dot(
-                    picks, rows_ref[s0 * pad : (s0 + group) * pad, :]
-                ).astype(bf16)
-
-        section = section_ref[...]
-        gate_value = dot(section, gate_ref[...])
-        up_value = dot(section, up_ref[...])
-        out_ref[...] = (silu(gate_value) * up_value).astype(bf16)
-
-    weight_spec = pl.BlockSpec((width, step), lambda i: (0, i))
-    return pl.pallas_call(
-        body,
-        grid=(hidden // step,),
-        out_shape=(
-            jax.ShapeDtypeStruct((slots, hidden), bf16),
-            jax.ShapeDtypeStruct((sources, 2 * pad), f32),
-        ),
-        in_specs=[pl.BlockSpec(memory_space=pltpu.SMEM)]
-        + whole(len(flat))
-        + [weight_spec, weight_spec],
-        out_specs=(
-            pl.BlockSpec((slots, step), lambda i: (0, i)),
-            pl.BlockSpec((sources, 2 * pad), lambda i: (0, 0)),
-        ),
-        scratch_shapes=[
-            pltpu.VMEM((sources * pad, width), bf16),
-            pltpu.VMEM((slots, width), bf16),
-        ],
-        cost_estimate=pl.CostEstimate(
-            flops=4 * slots * width * hidden, transcendentals=0, bytes_accessed=0
-        ),
-    )(index.vector, *flat, gate_weight, up_weight)
+        expert = lax.broadcasted_iota(jnp.int32, (extra, 2 * pad), 0) == s_ref[index.e]
+        if pad > tokens:
+            for s in range(sources):
+                rows_ref[s * pad + tokens : (s + 1) * pad, :] = jnp.zeros((pad - tokens, width), bf16)
+        rows_ref[0:tokens, :] = row_refs[0][...]
+        for q in range(parts):
+
+            @pl.when(s_ref[index.part] == q)
+            def _():
+                for s in range(1, sources):
+                    for i in range(parts):
+                        to = (q - i) % parts
+                        rows_ref[s * pad : s * pad + tokens, to * piece : (to + 1) * piece] = (
+                            row_refs[2 + (s - 1) * parts + i][0:tokens, :]
+                        )
+
+        for s0 in range(0, sources, group):
+            targets = []
+            for s in range(s0, s0 + group):
+                table_ref = row_refs[2 + (s - 1) * parts if s else 1]
+                table = table_ref[tokens : tokens + extra, 0 : 2 * pad].astype(f32)
+                mine = jnp.sum(jnp.where(expert, table, 0.0), axis=0, keepdims=True)
+                info_ref[s : s + 1, :] = mine
+                rank = mine[:, 0:pad]
+                targets.append(jnp.where(rank >= 0, rank + (s - s0) * capacity, -1.0))
+            target = jnp.concatenate(targets, axis=1) if group > 1 else targets[0]
+            slot = lax.broadcasted_iota(jnp.int32, (group * capacity, group * pad), 0)
+            picks = (slot.astype(f32) == target).astype(bf16)
+            section_ref[s0 * capacity : (s0 + group) * capacity, :] = dot(
+                picks, rows_ref[s0 * pad : (s0 + group) * pad, :]
+            ).astype(bf16)
+        for h in range(0, hidden, step):
+            section = section_ref[...]
+            gate_value = dot(section, gate_ref[:, h : h + step])
+            up_value = dot(section, up_ref[:, h : h + step])
+            out_ref[:, h : h + step] = (silu(gate_value) * up_value).astype(bf16)
+
+    outs = (
+        jax.ShapeDtypeStruct((slots, hidden), bf16),
+        jax.ShapeDtypeStruct((sources, 2 * pad), f32),
+    )
+    scratch = (pltpu.VMEM((sources * pad, width), bf16), pltpu.VMEM((slots, width), bf16))
+    operands = (index.vector, *flat, gate_weight, up_weight)
+    return call(body, outs, operands, 4 * slots * width * hidden, smem=1, scratch=scratch)
 
 
 def take_block(index, weight, place, hidden):
-    columns = weight.shape[1]
-
     def body(s_ref, in_ref, out_ref):
-        out_ref[...] = in_ref[...]
-
-    return pl.pallas_call(
-        body,
-        out_shape=jax.ShapeDtypeStruct((hidden, columns), weight.dtype),
-        grid_spec=pltpu.PrefetchScalarGridSpec(
-            num_scalar_prefetch=1,
-            grid=(4,),
-            in_specs=[pl.BlockSpec((hidden // 4, columns), lambda i, s: (s[place] * 4 + i, 0))],
-            out_specs=pl.BlockSpec((hidden // 4, columns), lambda i, s: (i, 0)),
-        ),
-        cost_estimate=pl.CostEstimate(flops=1 << 20, transcendentals=0, bytes_accessed=0),
-    )(index.vector, weight)
+        out_ref[...] = index.rows(s_ref, place, in_ref, hidden)
+
+    out = jax.ShapeDtypeStruct((hidden, weight.shape[1]), weight.dtype)
+    return call(body, out, (index.vector, weight), 1 << 20, smem=1)
 
 
 def down_first(index, hiddens, weight, traded):
     hidden, columns = hiddens[0].shape[1], weight.shape[1]
     chunks, partners = len(hiddens), len(traded)
-    fixed = lambda i, s: (0, 0)
 
     def body(s_ref, *refs):
-        weights = refs[chunks : chunks + 1 + partners]
         outs = refs[chunks + 1 + partners :]
-        for w in range(1 + partners):
+        weights = [index.rows(s_ref, index.held, refs[chunks], hidden)]
+        weights += [ref[...] for ref in refs[chunks + 1 : chunks + 1 + partners]]
+        for w, weight in enumerate(weights):
             for h in range(chunks):
-                outs[w * chunks + h][...] = dot(refs[h][...], weights[w][...])
-
-    outs = pl.pallas_call(
-        body,
-        out_shape=[
-            jax.ShapeDtypeStruct((h.shape[0], columns), f32)
-            for _ in range(1 + partners)
-            for h in hiddens
-        ],
-        grid_spec=pltpu.PrefetchScalarGridSpec(
-            num_scalar_prefetch=1,
-            grid=(1,),
-            in_specs=[pl.BlockSpec(h.shape, fixed) for h in hiddens]
-            + [pl.BlockSpec((hidden, columns), index.block(index.held))]
-            + [pl.BlockSpec((hidden, columns), fixed)] * partners,
-            out_specs=[
-                pl.BlockSpec((h.shape[0], columns), fixed)
-                for _ in range(1 + partners)
-                for h in hiddens
-            ],
-        ),
-        cost_estimate=pl.CostEstimate(
-            flops=2 * sum(h.shape[0] for h in hiddens) * hidden * columns * (1 + partners),
-            transcendentals=0,
-            bytes_accessed=0,
-        ),
-    )(index.vector, *hiddens, weight, *traded)
+                outs[w * chunks + h][...] = dot(refs[h][...], weight)
+
+    shapes = [
+        jax.ShapeDtypeStruct((h.shape[0], columns), f32) for _ in range(1 + partners) for h in hiddens
+    ]
+    flops = 2 * sum(h.shape[0] for h in hiddens) * hidden * columns * (1 + partners)
+    outs = call(body, shapes, (index.vector, *hiddens, weight, *traded), flops, smem=1)
     return [outs[w * chunks : (w + 1) * chunks] for w in range(1 + partners)]
 
 
@@ -496,38 +423,22 @@
 def down_own(index, firsts, gathered, weight):
     count, chunks = len(gathered), len(firsts)
     hidden, columns = gathered[0][0].shape[1], weight.shape[1]
-    fixed = lambda i, s: (0, 0)
 
     def body(s_ref, *refs):
         hidden_refs = refs[chunks : chunks + count * chunks]
         weight_ref = refs[chunks + count * chunks]
         outs = refs[chunks + count * chunks + 1 :]
-        for i in range(count):
-
-            @pl.when(pl.program_id(0) == i)
-            def _():
-                for h in range(chunks):
-                    before = outs[h][...] if i else refs[h][...]
-                    outs[h][...] = before + dot(hidden_refs[i * chunks + h][...], weight_ref[...])
+        for h in range(chunks):
+            total = refs[h][...]
+            for i in range(count):
+                rows = index.rows(s_ref, index.held + 1 + i, weight_ref, hidden)
+                total = total + dot(hidden_refs[i * chunks + h][...], rows)
+            outs[h][...] = total
 
     flat = [h for pieces in gathered for h in pieces]
-    return pl.pallas_call(
-        body,
-        out_shape=[jax.ShapeDtypeStruct(f.shape, f32) for f in firsts],
-        grid_spec=pltpu.PrefetchScalarGridSpec(
-            num_scalar_prefetch=1,
-            grid=(count,),
-            in_specs=[pl.BlockSpec(f.shape, fixed) for f in firsts]
-            + [pl.BlockSpec(h.shape, fixed) for h in flat]
-            + [pl.BlockSpec((hidden, columns), index.block(index.held + 1))],
-            out_specs=[pl.BlockSpec(f.shape, fixed) for f in firsts],
-        ),
-        cost_estimate=pl.CostEstimate(
-            flops=2 * sum(h.shape[0] for h in flat) * hidden * columns,
-            transcendentals=0,
-            bytes_accessed=0,
-        ),
-    )(index.vector, *firsts, *flat, weight)
+    outs = [jax.ShapeDtypeStruct(f.shape, f32) for f in firsts]
+    flops = 2 * sum(h.shape[0] for h in flat) * hidden * columns
+    return call(body, outs, (index.vector, *firsts, *flat, weight), flops, smem=1)
 
 
 def combine(own, back, info, tokens, capacity, out_type):

time: 130 us -> 118 us (0.908)
  Pallas kernels: 58.7 us -> 20.6 us
  waiting for transfers between devices: 18.9 us -> 47.9 us
  starting transfers between devices: 39.9 us -> 37 us
  other arithmetic: 2.9 us -> 0.87 us
  local copies, waits for them, and re-layouts: 7.83 us -> 9.21 us
    pallas_call x14, Pallas kernels: 58.7 us -> 20.6 us  [call(): pl.pallas_call(body, out_shape=jax.tree.map(lambda o: pltpu.VMEM(o.shape,...]
    ppermute x34, waiting for transfers between devices: 18.9 us -> 47.9 us  [send(): return lax.ppermute(value, AXES, self.pairs(move))]
    ppermute x34, starting transfers between devices: 39.9 us -> 37 us  [send(): return lax.ppermute(value, AXES, self.pairs(move))]
    unnamed x62 -> x41, local copies, waits for them, and re-layouts: 6.53 us -> 8.49 us
  transfers between devices with their start and end apart: 34 -> 34, of which waited for: 10 -> 14; matrix products, arithmetic and copies ran while one was open for 1% -> 1% of each run, Pallas kernels for 40% -> 16%
where the time goes in v1:
time: 118 us; the launch traced here: 117 us
  waiting for transfers between devices  47.9 us (41%)
  starting transfers between devices  37 us (31%)
  Pallas kernels  20.6 us (17%)
  local copies, waits for them, and re-layouts  9.21 us (8%)
    ppermute x34, waiting for transfers between devices, send(): return lax.ppermute(value, AXES, self.pairs(move))  47.9 us
    ppermute x34, starting transfers between devices, send(): return lax.ppermute(value, AXES, self.pairs(move))  37 us
    pallas_call x14, Pallas kernels, call(): pl.pallas_call(body, out_shape=jax.tree.map(lambda o: pltpu.VMEM(o.shape,...  20.6 us
    unnamed x41, local copies, waits for them, and re-layouts  8.49 us
  transfers between devices with their start and end apart: 34, of which 14 were waited for; matrix products, arithmetic and copies ran while one was open for 1% of the time, Pallas kernels for 16%

profile of v1, /device:TPU:0, one launch (start us, length us, event | category | flops | bytes accessed | tf_op | source)
XLA Modules:
  0.0 116.5 jit_solution(6930330159838820212)
XLA Ops:
  0.7 0.7 dynamic-slice_bitcast_fusion.s_ref
  1.4 1.0 copy-done.8
  2.4 0.7 copy-done.14
  3.1 0.7 copy-done.16
  3.7 0.7 copy-done.17
  4.4 0.9 shard_map.203
  5.3 3.1 %collective-permute-start = (bf16[104,1024]{1,0:T(8,128)(2,1)S(1)}, bf16[104,1024]{1,0:T(8,128)(2,1)S(1)}, u32[]{:S(2)}, u32[]{:S(2)}) collective-permute-start(bf16[104,1024]{1,0:T(8,128)(2,1)S(1)} %get-tuple-element.47.refs_1_), channel_id=1, source_target_pairs={{0,8},{1,9},{2,10},{3,11},{4,12},{5,13},{6,14},{7,15},{8,16},{9,17... | collective-permute-start | bytes 638984 | tf_op jit(solution)/shard_map/ppermute | solution.py:40
  8.3 2.6 %collective-permute-start.1 = (bf16[104,1024]{1,0:T(8,128)(2,1)S(1)}, bf16[104,1024]{1,0:T(8,128)(2,1)S(1)}, u32[]{:S(2)}, u32[]{:S(2)}) collective-permute-start(bf16[104,1024]{1,0:T(8,128)(2,1)S(1)} %get-tuple-element.47.refs_1_), channel_id=1, source_target_pairs={{0,16},{1,17},{2,18},{3,19},{4,20},{5,21},{6,22},{7,23},{8,24},{9,... | collective-permute-start | bytes 638984 | tf_op jit(solution)/shard_map/ppermute | solution.py:40
  10.9 1.3 %collective-permute-start.2 = (bf16[104,1024]{1,0:T(8,128)(2,1)S(1)}, bf16[104,1024]{1,0:T(8,128)(2,1)S(1)}, u32[]{:S(2)}, u32[]{:S(2)}) collective-permute-start(bf16[104,1024]{1,0:T(8,128)(2,1)S(1)} %get-tuple-element.47.refs_1_), channel_id=1, source_target_pairs={{0,24},{1,25},{2,26},{3,27},{4,28},{5,29},{6,30},{7,31},{8,0},{9,1... | collective-permute-start | bytes 638984 | tf_op jit(solution)/shard_map/ppermute | solution.py:40
  12.3 2.2 %copy-done = bf16[1,4096,512]{2,1,0:T(8,128)(2,1)S(1)} copy-done((bf16[1,4096,512]{2,1,0:T(8,128)(2,1)S(1)}, bf16[1,4096,512]{2,1,0:T(8,128)(2,1)}, u32[]{:S(2)}) %copy-start) | copy-done | bytes 4194328
  14.5 0.6 shard_map.205
  15.2 0.2 copy-done.12
  15.4 3.3 %shard_map.204 = (f32[256,512]{1,0:T(8,128)S(1)}, bf16[256,256]{1,0:T(8,128)(2,1)S(1)}, bf16[136,256]{1,0:T(8,128)(2,1)S(1)}) custom-call(bf16[256,256]{1,0:T(8,128)(2,1)S(1)} %copy-done.11, bf16[256,256]{1,0:T(8,128)(2,1)S(1)} %copy-done.12, bf16[256,512]{1,0:T(8,128)(2,1)S(1)} %copy-done.9, bf16[256,256]{1,0:T(8,128)(2,1)S(1)} %copy-done.13, ...), custom_call_target="tpu_custom_call" | custom-call | flops 33554432 | tf_op jit(solution)/shard_map/pallas_call | solution.py:119
  18.7 6.2 %collective-permute-done.1.refs_4_ = bf16[104,1024]{1,0:T(8,128)(2,1)S(1)} collective-permute-done((bf16[104,1024]{1,0:T(8,128)(2,1)S(1)}, bf16[104,1024]{1,0:T(8,128)(2,1)S(1)}, u32[]{:S(2)}, u32[]{:S(2)}) %collective-permute-start.1) | collective-permute-done | bytes 213024 | tf_op jit(solution)/shard_map/ppermute | solution.py:40
  24.9 6.9 %collective-permute-start.6 = (bf16[136,256]{1,0:T(8,128)(2,1)S(1)}, bf16[136,256]{1,0:T(8,128)(2,1)S(1)}, u32[]{:S(2)}, u32[]{:S(2)}) collective-permute-start(bf16[136,256]{1,0:T(8,128)(2,1)S(1)} %get-tuple-element.52), channel_id=1, source_target_pairs={{0,8},{1,9},{2,10},{3,11},{4,12},{5,13},{6,14},{7,15},{8,16},{9,17... | collective-permute-start | bytes 208904 | tf_op jit(solution)/shard_map/ppermute | solution.py:40
  31.8 3.5 %collective-permute-start.7 = (bf16[136,256]{1,0:T(8,128)(2,1)S(1)}, bf16[136,256]{1,0:T(8,128)(2,1)S(1)}, u32[]{:S(2)}, u32[]{:S(2)}) collective-permute-start(bf16[136,256]{1,0:T(8,128)(2,1)S(1)} %get-tuple-element.52), channel_id=1, source_target_pairs={{0,16},{1,17},{2,18},{3,19},{4,20},{5,21},{6,22},{7,23},{8,24},{9,... | collective-permute-start | bytes 208904 | tf_op jit(solution)/shard_map/ppermute | solution.py:40
  35.3 1.3 %collective-permute-start.8 = (bf16[136,256]{1,0:T(8,128)(2,1)S(1)}, bf16[136,256]{1,0:T(8,128)(2,1)S(1)}, u32[]{:S(2)}, u32[]{:S(2)}) collective-permute-start(bf16[136,256]{1,0:T(8,128)(2,1)S(1)} %get-tuple-element.52), channel_id=1, source_target_pairs={{0,24},{1,25},{2,26},{3,27},{4,28},{5,29},{6,30},{7,31}} | collective-permute-start | bytes 208904 | tf_op jit(solution)/shard_map/ppermute | solution.py:40
  36.6 1.6 %collective-permute-start.3 = (bf16[104,1024]{1,0:T(8,128)(2,1)S(1)}, bf16[104,1024]{1,0:T(8,128)(2,1)S(1)}, u32[]{:S(2)}, u32[]{:S(2)}) collective-permute-start(bf16[104,1024]{1,0:T(8,128)(2,1)S(1)} %collective-permute-done.refs_2_), channel_id=1, source_target_pairs={{0,1},{1,0},{2,3},{3,2},{4,6},{5,7},{6,4},{7,5},{8,9},{9,8},{10,11... | collective-permute-start | bytes 638984 | tf_op jit(solution)/shard_map/ppermute | solution.py:40
  38.2 0.5 collective-permute-start.4
  38.7 1.5 %collective-permute-start.5 = (bf16[104,1024]{1,0:T(8,128)(2,1)S(1)}, bf16[104,1024]{1,0:T(8,128)(2,1)S(1)}, u32[]{:S(2)}, u32[]{:S(2)}) collective-permute-start(bf16[104,1024]{1,0:T(8,128)(2,1)S(1)} %collective-permute-done.2.refs_6_), channel_id=1, source_target_pairs={{0,1},{1,0},{2,3},{3,2},{4,6},{5,7},{6,4},{7,5},{8,9},{9,8},{10,11... | collective-permute-start | bytes 638984 | tf_op jit(solution)/shard_map/ppermute | solution.py:40
  40.2 0.5 collective-permute-start.10
  40.7 0.6 shard_map.206
  41.4 1.2 %collective-permute-done.3.refs_3_ = bf16[104,1024]{1,0:T(8,128)(2,1)S(1)} collective-permute-done((bf16[104,1024]{1,0:T(8,128)(2,1)S(1)}, bf16[104,1024]{1,0:T(8,128)(2,1)S(1)}, u32[]{:S(2)}, u32[]{:S(2)}) %collective-permute-start.3) | collective-permute-done | bytes 213024 | tf_op jit(solution)/shard_map/ppermute | solution.py:40
  42.5 2.3 %collective-permute-done.4.refs_5_ = bf16[104,1024]{1,0:T(8,128)(2,1)S(1)} collective-permute-done((bf16[104,1024]{1,0:T(8,128)(2,1)S(1)}, bf16[104,1024]{1,0:T(8,128)(2,1)S(1)}, u32[]{:S(2)}, u32[]{:S(2)}) %collective-permute-start.4) | collective-permute-done | bytes 213024 | tf_op jit(solution)/shard_map/ppermute | solution.py:40
  44.8 2.3 %collective-permute-done.5.refs_7_ = bf16[104,1024]{1,0:T(8,128)(2,1)S(1)} collective-permute-done((bf16[104,1024]{1,0:T(8,128)(2,1)S(1)}, bf16[104,1024]{1,0:T(8,128)(2,1)S(1)}, u32[]{:S(2)}, u32[]{:S(2)}) %collective-permute-start.5) | collective-permute-done | bytes 213024 | tf_op jit(solution)/shard_map/ppermute | solution.py:40
  47.1 0.5 collective-permute-start.12
  47.6 1.5 %collective-permute-start.22 = (bf16[1024,512]{1,0:T(8,128)(2,1)S(1)}, bf16[1024,512]{1,0:T(8,128)(2,1)S(1)}, u32[]{:S(2)}, u32[]{:S(2)}) collective-permute-start(bf16[1024,512]{1,0:T(8,128)(2,1)S(1)} %shard_map.205), channel_id=1, source_target_pairs={{0,2},{1,3},{2,0},{3,1},{4,5},{5,4},{6,7},{7,6},{8,10},{9,11},{10,... | collective-permute-start | bytes 3145736 | tf_op jit(solution)/shard_map/ppermute | solution.py:40
  49.2 0.5 collective-permute-start.24
  49.7 0.5 collective-permute-start.15
  50.3 2.2 %copy-done.3 = bf16[1,2048,1024]{2,1,0:T(8,128)(2,1)S(1)} copy-done((bf16[1,2048,1024]{2,1,0:T(8,128)(2,1)S(1)}, bf16[1,2048,1024]{2,1,0:T(8,128)(2,1)}, u32[]{:S(2)}) %copy-start.3) | copy-done | bytes 4194328
  52.4 3.7 %shard_map.207 = (bf16[288,1024]{1,0:T(8,128)(2,1)S(1)}, f32[4,256]{1,0:T(4,128)S(1)}) custom-call(s32[12]{0:T(128)S(1)} %dynamic-slice_bitcast_fusion.s_ref, bf16[96,2048]{1,0:T(8,128)(2,1)S(1)} %get-tuple-element.46.refs_0_.normed_ref, bf16[104,1024]{1,0:T(8,128)(2,1)S(1)} %get-tuple-element.47.refs_1_, ...), custom_call_target="tpu_custom_call" | custom-call | flops 2415919104 | tf_op jit(solution)/shard_map/pallas_call | solution.py:119
  56.2 1.6 %collective-permute-start.23 = (bf16[288,1024]{1,0:T(8,128)(2,1)S(1)}, bf16[288,1024]{1,0:T(8,128)(2,1)S(1)}, u32[]{:S(2)}, u32[]{:S(2)}) collective-permute-start(bf16[288,1024]{1,0:T(8,128)(2,1)S(1)} %get-tuple-element.59.refs_0_), channel_id=1, source_target_pairs={{0,1},{1,0},{2,3},{3,2},{4,6},{5,7},{6,4},{7,5},{8,9},{9,8},{10,11... | collective-permute-start | bytes 1769480 | tf_op jit(solution)/shard_map/ppermute | solution.py:40
  57.8 3.9 %shard_map.208 = (bf16[288,1024]{1,0:T(8,128)(2,1)S(1)}, f32[4,256]{1,0:T(4,128)S(1)}) custom-call(s32[12]{0:T(128)S(1)} %dynamic-slice_bitcast_fusion.s_ref, bf16[96,2048]{1,0:T(8,128)(2,1)S(1)} %collective-permute-done.9.refs_0_, bf16[104,1024]{1,0:T(8,128)(2,1)S(1)} %collective-permute-done.10.refs_1_, ...), custom_call_target="tpu_custom_call" | custom-call | flops 2415919104 | tf_op jit(solution)/shard_map/pallas_call | solution.py:119
  61.7 0.6 collective-permute-start.17
  62.3 1.3 %collective-permute-done.18.refs_0_ = bf16[136,256]{1,0:T(8,128)(2,1)S(1)} collective-permute-done((bf16[136,256]{1,0:T(8,128)(2,1)S(1)}, bf16[136,256]{1,0:T(8,128)(2,1)S(1)}, u32[]{:S(2)}, u32[]{:S(2)}) %collective-permute-start.18) | collective-permute-done | bytes 69664 | tf_op jit(solution)/shard_map/ppermute | solution.py:40
  63.5 0.2 collective-permute-start.19
  63.7 1.1 collective-permute-done.19.refs_2_
  64.8 0.2 collective-permute-start.20
  64.9 1.1 collective-permute-done.20.refs_4_
  66.0 0.2 collective-permute-start.21
  66.2 1.1 collective-permute-done.21.refs_6_
  67.3 1.3 %shard_map.209.refs_0_ = bf16[304,512]{1,0:T(8,128)(2,1)S(1)} custom-call(s32[12]{0:T(128)S(1)} %dynamic-slice_bitcast_fusion.s_ref, f32[256,512]{1,0:T(8,128)S(1)} %get-tuple-element.69.local_ref, bf16[256,256]{1,0:T(8,128)(2,1)S(1)} %get-tuple-element.70.qd_ref, bf16[256,512]{1,0:T(8,128)(2,1)S(1)} %copy-done.10, f32[1,512]{1,0:T(1,128)S(1)} %bitcast.39, ...), custom_call_target="tpu_custom_call" | custom-call | flops 134217728 | tf_op jit(solution)/shard_map/pallas_call | solution.py:119
  68.7 2.0 %shard_map.210 = (f32[288,512]{1,0:T(8,128)S(1)}, f32[288,512]{1,0:T(8,128)S(1)}, f32[288,512]{1,0:T(8,128)S(1)}, f32[288,512]{1,0:T(8,128)S(1)}) custom-call(s32[12]{0:T(128)S(1)} %dynamic-slice_bitcast_fusion.s_ref, bf16[288,1024]{1,0:T(8,128)(2,1)S(1)} %get-tuple-element.59.refs_0_, bf16[288,1024]{1,0:T(8,128)(2,1)S(1)} %get-tuple-element.68.refs_1_, ...), custom_call_target="tpu_custom_call" | custom-call | flops 1207959552 | tf_op jit(solution)/shard_map/pallas_call | solution.py:119
  70.6 1.9 %collective-permute-done.23.refs_0_.refs_2_ = bf16[288,1024]{1,0:T(8,128)(2,1)S(1)} collective-permute-done((bf16[288,1024]{1,0:T(8,128)(2,1)S(1)}, bf16[288,1024]{1,0:T(8,128)(2,1)S(1)}, u32[]{:S(2)}, u32[]{:S(2)}) %collective-permute-start.23) | collective-permute-done | bytes 589856 | tf_op jit(solution)/shard_map/ppermute | solution.py:40
  72.5 13.8 %collective-permute-done.24.refs_1_ = bf16[1024,512]{1,0:T(8,128)(2,1)S(1)} collective-permute-done((bf16[1024,512]{1,0:T(8,128)(2,1)S(1)}, bf16[1024,512]{1,0:T(8,128)(2,1)S(1)}, u32[]{:S(2)}, u32[]{:S(2)}) %collective-permute-start.24) | collective-permute-done | bytes 1048608 | tf_op jit(solution)/shard_map/ppermute | solution.py:40
  86.3 0.5 shard_map.211
  86.8 0.5 shard_map.213
  87.3 1.6 %collective-permute-start.25 = (bf16[288,512]{1,0:T(8,128)(2,1)S(1)}, bf16[288,512]{1,0:T(8,128)(2,1)S(1)}, u32[]{:S(2)}, u32[]{:S(2)}) collective-permute-start(bf16[288,512]{1,0:T(8,128)(2,1)S(1)} %shard_map.213), channel_id=1, source_target_pairs={{0,2},{1,3},{2,0},{3,1},{4,5},{5,4},{6,7},{7,6},{8,10},{9,11},{10,... | collective-permute-start | bytes 884744 | tf_op jit(solution)/shard_map/ppermute | solution.py:40
  88.9 1.3 %shard_map.212 = (f32[288,512]{1,0:T(8,128)S(1)}, f32[288,512]{1,0:T(8,128)S(1)}) custom-call(s32[12]{0:T(128)S(1)} %dynamic-slice_bitcast_fusion.s_ref, f32[288,512]{1,0:T(8,128)S(1)} %get-tuple-element.78.refs_0_, f32[288,512]{1,0:T(8,128)S(1)} %get-tuple-element.79.refs_1_, bf16[288,1024]{1,0:T(8,128)(2,1)S(1)} %collective-permute-done.23.refs_0_.refs_2_, ...), custom_call_target="tpu_custom_call" | custom-call | flops 603979776 | tf_op jit(solution)/shard_map/pallas_call | solution.py:119
  90.2 3.8 %collective-permute-done.25.refs_0_ = bf16[288,512]{1,0:T(8,128)(2,1)S(1)} collective-permute-done((bf16[288,512]{1,0:T(8,128)(2,1)S(1)}, bf16[288,512]{1,0:T(8,128)(2,1)S(1)}, u32[]{:S(2)}, u32[]{:S(2)}) %collective-permute-start.25) | collective-permute-done | bytes 294944 | tf_op jit(solution)/shard_map/ppermute | solution.py:40
  94.1 0.3 shard_map.214
  94.5 1.6 %collective-permute-start.29 = (bf16[288,512]{1,0:T(8,128)(2,1)S(1)}, bf16[288,512]{1,0:T(8,128)(2,1)S(1)}, u32[]{:S(2)}, u32[]{:S(2)}) collective-permute-start(bf16[288,512]{1,0:T(8,128)(2,1)S(1)} %shard_map.211), channel_id=1, source_target_pairs={{0,2},{1,3},{2,0},{3,1},{4,5},{5,4},{6,7},{7,6},{8,10},{9,11},{10,... | collective-permute-start | bytes 884744 | tf_op jit(solution)/shard_map/ppermute | solution.py:40
  96.1 1.5 %collective-permute-start.26 = (bf16[304,512]{1,0:T(8,128)(2,1)S(1)}, bf16[304,512]{1,0:T(8,128)(2,1)S(1)}, u32[]{:S(2)}, u32[]{:S(2)}) collective-permute-start(bf16[304,512]{1,0:T(8,128)(2,1)S(1)} %shard_map.209.refs_0_), channel_id=1, source_target_pairs={{0,1},{1,0},{2,3},{3,2},{4,5},{5,4},{6,7},{7,6},{8,9},{9,8},{10,11... | collective-permute-start | bytes 933896 | tf_op jit(solution)/shard_map/ppermute | solution.py:40
  97.6 0.5 collective-permute-start.27
  98.1 1.5 %collective-permute-start.28 = (bf16[304,512]{1,0:T(8,128)(2,1)S(1)}, bf16[304,512]{1,0:T(8,128)(2,1)S(1)}, u32[]{:S(2)}, u32[]{:S(2)}) collective-permute-start(bf16[304,512]{1,0:T(8,128)(2,1)S(1)} %shard_map.209.refs_0_), channel_id=1, source_target_pairs={{0,3},{1,2},{2,1},{3,0},{4,7},{5,6},{6,5},{7,4},{8,11},{9,10},{10,... | collective-permute-start | bytes 933896 | tf_op jit(solution)/shard_map/ppermute | solution.py:40
  99.6 3.9 %collective-permute-done.29.refs_0_ = bf16[288,512]{1,0:T(8,128)(2,1)S(1)} collective-permute-done((bf16[288,512]{1,0:T(8,128)(2,1)S(1)}, bf16[288,512]{1,0:T(8,128)(2,1)S(1)}, u32[]{:S(2)}, u32[]{:S(2)}) %collective-permute-start.29) | collective-permute-done | bytes 294944 | tf_op jit(solution)/shard_map/ppermute | solution.py:40
  103.5 0.3 shard_map.216
  103.9 0.2 fusion.5
  104.2 2.1 %collective-permute-done.26.refs_1_ = bf16[304,512]{1,0:T(8,128)(2,1)S(1)} collective-permute-done((bf16[304,512]{1,0:T(8,128)(2,1)S(1)}, bf16[304,512]{1,0:T(8,128)(2,1)S(1)}, u32[]{:S(2)}, u32[]{:S(2)}) %collective-permute-start.26) | collective-permute-done | bytes 311328 | tf_op jit(solution)/shard_map/ppermute | solution.py:40
  106.3 1.6 %collective-permute-start.31 = (bf16[96,512]{1,0:T(8,128)(2,1)S(1)}, bf16[96,512]{1,0:T(8,128)(2,1)S(1)}, u32[]{:S(2)}, u32[]{:S(2)}) collective-permute-start(bf16[96,512]{1,0:T(8,128)(2,1)S(1)} %get-tuple-element.92), channel_id=1, source_target_pairs={{0,24},{1,25},{2,26},{3,27},{4,28},{5,29},{6,30},{7,31},{8,0},{9,1... | collective-permute-start | bytes 294920 | tf_op jit(solution)/shard_map/ppermute | solution.py:40
  107.9 5.7 %collective-permute-done.27.refs_2_ = bf16[304,512]{1,0:T(8,128)(2,1)S(1)} collective-permute-done((bf16[304,512]{1,0:T(8,128)(2,1)S(1)}, bf16[304,512]{1,0:T(8,128)(2,1)S(1)}, u32[]{:S(2)}, u32[]{:S(2)}) %collective-permute-start.27) | collective-permute-done | bytes 311328 | tf_op jit(solution)/shard_map/ppermute | solution.py:40
  113.7 1.4 %shard_map.215 = (bf16[256,512]{1,0:T(8,128)(2,1)S(1)}, f32[96,512]{1,0:T(8,128)S(1)}) custom-call(s32[12]{0:T(128)S(1)} %dynamic-slice_bitcast_fusion.s_ref, bf16[304,512]{1,0:T(8,128)(2,1)S(1)} %shard_map.209.refs_0_, bf16[304,512]{1,0:T(8,128)(2,1)S(1)} %collective-permute-done.26.refs_1_, bf16[304,512]{1,0:T(8,128)(2,1)S(1)} %collective-permute-done.27.refs_2_, ...), custom_call_target="tpu_custom_call" | custom-call | flops 637534208 | tf_op jit(solution)/shard_map/pallas_call | solution.py:119
  115.1 0.7 copy.22
  115.8 0.7 fusion.4
  (63 shorter events, 0.5 us)
Async XLA Ops:
  0.6 14.5 %copy-start.19 = (f32[256]{0:T(256)S(1)}, f32[256]{0:T(256)}, u32[]{:S(2)}) copy-start(f32[256]{0:T(256)} %param.25) | copy-start | bytes 3076
  0.6 14.5 %copy-start.15 = (f32[4,256]{1,0:T(4,128)S(1)}, f32[4,256]{1,0:T(4,128)}, u32[]{:S(2)}) copy-start(f32[4,256]{1,0:T(4,128)} %added_ref.1) | copy-start | bytes 12292
  1.4 1.0 copy-start.8
  2.4 0.7 copy-start.14
  3.0 0.7 copy-start.16
  3.7 0.7 copy-start.17
  4.4 10.7 %copy-start.9 = (bf16[256,512]{1,0:T(8,128)(2,1)S(1)}, bf16[256,512]{1,0:T(8,128)(2,1)}, u32[]{:S(2)}) copy-start(bf16[256,512]{1,0:T(8,128)(2,1)} %v_ref.1) | copy-start | bytes 786436
  4.4 10.7 %copy-start.11 = (bf16[256,256]{1,0:T(8,128)(2,1)S(1)}, bf16[256,256]{1,0:T(8,128)(2,1)}, u32[]{:S(2)}) copy-start(bf16[256,256]{1,0:T(8,128)(2,1)} %q_ref.1) | copy-start | bytes 393220
  5.3 13.4 %collective-permute-start = (bf16[104,1024]{1,0:T(8,128)(2,1)S(1)}, bf16[104,1024]{1,0:T(8,128)(2,1)S(1)}, u32[]{:S(2)}, u32[]{:S(2)}) collective-permute-start(bf16[104,1024]{1,0:T(8,128)(2,1)S(1)} %get-tuple-element.47.refs_1_), channel_id=1, source_target_pairs={{0,8},{1,9},{2,10},{3,11},{4,12},{5,13},{6,14},{7,15},{8,16},{9,17... | collective-permute-start | bytes 638984 | tf_op jit(solution)/shard_map/ppermute | solution.py:40
  8.3 16.5 %collective-permute-start.1 = (bf16[104,1024]{1,0:T(8,128)(2,1)S(1)}, bf16[104,1024]{1,0:T(8,128)(2,1)S(1)}, u32[]{:S(2)}, u32[]{:S(2)}) collective-permute-start(bf16[104,1024]{1,0:T(8,128)(2,1)S(1)} %get-tuple-element.47.refs_1_), channel_id=1, source_target_pairs={{0,16},{1,17},{2,18},{3,19},{4,20},{5,21},{6,22},{7,23},{8,24},{9,... | collective-permute-start | bytes 638984 | tf_op jit(solution)/shard_map/ppermute | solution.py:40
  10.9 14.0 %collective-permute-start.2 = (bf16[104,1024]{1,0:T(8,128)(2,1)S(1)}, bf16[104,1024]{1,0:T(8,128)(2,1)S(1)}, u32[]{:S(2)}, u32[]{:S(2)}) collective-permute-start(bf16[104,1024]{1,0:T(8,128)(2,1)S(1)} %get-tuple-element.47.refs_1_), channel_id=1, source_target_pairs={{0,24},{1,25},{2,26},{3,27},{4,28},{5,29},{6,30},{7,31},{8,0},{9,1... | collective-permute-start | bytes 638984 | tf_op jit(solution)/shard_map/ppermute | solution.py:40
  12.3 2.2 %copy-start = (bf16[1,4096,512]{2,1,0:T(8,128)(2,1)S(1)}, bf16[1,4096,512]{2,1,0:T(8,128)(2,1)}, u32[]{:S(2)}) copy-start(bf16[1,4096,512]{2,1,0:T(8,128)(2,1)} %param.35) | copy-start | bytes 12582916
  14.5 0.9 copy-start.12
  14.5 1.0 copy-start.13
  14.5 26.3 %copy-start.1 = (bf16[1,4096,512]{2,1,0:T(8,128)(2,1)S(1)}, bf16[1,4096,512]{2,1,0:T(8,128)(2,1)}, u32[]{:S(2)}) copy-start(bf16[1,4096,512]{2,1,0:T(8,128)(2,1)} %param.35) | copy-start | bytes 12582916
  15.1 35.2 %copy-start.2 = (bf16[1,2048,1024]{2,1,0:T(8,128)(2,1)S(1)}, bf16[1,2048,1024]{2,1,0:T(8,128)(2,1)}, u32[]{:S(2)}) copy-start(bf16[1,2048,1024]{2,1,0:T(8,128)(2,1)} %param.33) | copy-start | bytes 12582916
  24.9 13.8 %collective-permute-start.6 = (bf16[136,256]{1,0:T(8,128)(2,1)S(1)}, bf16[136,256]{1,0:T(8,128)(2,1)S(1)}, u32[]{:S(2)}, u32[]{:S(2)}) collective-permute-start(bf16[136,256]{1,0:T(8,128)(2,1)S(1)} %get-tuple-element.52), channel_id=1, source_target_pairs={{0,8},{1,9},{2,10},{3,11},{4,12},{5,13},{6,14},{7,15},{8,16},{9,17... | collective-permute-start | bytes 208904 | tf_op jit(solution)/shard_map/ppermute | solution.py:40
  31.8 8.4 %collective-permute-start.7 = (bf16[136,256]{1,0:T(8,128)(2,1)S(1)}, bf16[136,256]{1,0:T(8,128)(2,1)S(1)}, u32[]{:S(2)}, u32[]{:S(2)}) collective-permute-start(bf16[136,256]{1,0:T(8,128)(2,1)S(1)} %get-tuple-element.52), channel_id=1, source_target_pairs={{0,16},{1,17},{2,18},{3,19},{4,20},{5,21},{6,22},{7,23},{8,24},{9,... | collective-permute-start | bytes 208904 | tf_op jit(solution)/shard_map/ppermute | solution.py:40
  35.3 4.9 %collective-permute-start.8 = (bf16[136,256]{1,0:T(8,128)(2,1)S(1)}, bf16[136,256]{1,0:T(8,128)(2,1)S(1)}, u32[]{:S(2)}, u32[]{:S(2)}) collective-permute-start(bf16[136,256]{1,0:T(8,128)(2,1)S(1)} %get-tuple-element.52), channel_id=1, source_target_pairs={{0,24},{1,25},{2,26},{3,27},{4,28},{5,29},{6,30},{7,31}} | collective-permute-start | bytes 208904 | tf_op jit(solution)/shard_map/ppermute | solution.py:40
  36.6 5.9 %collective-permute-start.3 = (bf16[104,1024]{1,0:T(8,128)(2,1)S(1)}, bf16[104,1024]{1,0:T(8,128)(2,1)S(1)}, u32[]{:S(2)}, u32[]{:S(2)}) collective-permute-start(bf16[104,1024]{1,0:T(8,128)(2,1)S(1)} %collective-permute-done.refs_2_), channel_id=1, source_target_pairs={{0,1},{1,0},{2,3},{3,2},{4,6},{5,7},{6,4},{7,5},{8,9},{9,8},{10,11... | collective-permute-start | bytes 638984 | tf_op jit(solution)/shard_map/ppermute | solution.py:40
  38.2 6.6 %collective-permute-start.4 = (bf16[104,1024]{1,0:T(8,128)(2,1)S(1)}, bf16[104,1024]{1,0:T(8,128)(2,1)S(1)}, u32[]{:S(2)}, u32[]{:S(2)}) collective-permute-start(bf16[104,1024]{1,0:T(8,128)(2,1)S(1)} %collective-permute-done.1.refs_4_), channel_id=1, source_target_pairs={{0,1},{1,0},{2,3},{3,2},{4,6},{5,7},{6,4},{7,5},{8,9},{9,8},{10,11... | collective-permute-start | bytes 638984 | tf_op jit(solution)/shard_map/ppermute | solution.py:40
  38.7 8.4 %collective-permute-start.5 = (bf16[104,1024]{1,0:T(8,128)(2,1)S(1)}, bf16[104,1024]{1,0:T(8,128)(2,1)S(1)}, u32[]{:S(2)}, u32[]{:S(2)}) collective-permute-start(bf16[104,1024]{1,0:T(8,128)(2,1)S(1)} %collective-permute-done.2.refs_6_), channel_id=1, source_target_pairs={{0,1},{1,0},{2,3},{3,2},{4,6},{5,7},{6,4},{7,5},{8,9},{9,8},{10,11... | collective-permute-start | bytes 638984 | tf_op jit(solution)/shard_map/ppermute | solution.py:40
  40.2 8.9 %collective-permute-start.9 = (bf16[96,2048]{1,0:T(8,128)(2,1)S(1)}, bf16[96,2048]{1,0:T(8,128)(2,1)S(1)}, u32[]{:S(2)}, u32[]{:S(2)}) collective-permute-start(bf16[96,2048]{1,0:T(8,128)(2,1)S(1)} %get-tuple-element.46.refs_0_.normed_ref), channel_id=1, source_target_pairs={{0,4},{1,5},{2,6},{3,7},{4,0},{5,1},{6,2},{7,3},{8,12},{9,13},{10,... | collective-permute-start | bytes 1179656 | tf_op jit(solution)/shard_map/ppermute | solution.py:40
  40.2 7.4 %collective-permute-start.10 = (bf16[104,1024]{1,0:T(8,128)(2,1)S(1)}, bf16[104,1024]{1,0:T(8,128)(2,1)S(1)}, u32[]{:S(2)}, u32[]{:S(2)}) collective-permute-start(bf16[104,1024]{1,0:T(8,128)(2,1)S(1)} %get-tuple-element.47.refs_1_), channel_id=1, source_target_pairs={{0,4},{1,5},{2,6},{3,7},{4,0},{5,1},{6,2},{7,3},{8,12},{9,13},{10,... | collective-permute-start | bytes 638984 | tf_op jit(solution)/shard_map/ppermute | solution.py:40
  47.1 2.6 %collective-permute-start.11 = (bf16[104,1024]{1,0:T(8,128)(2,1)S(1)}, bf16[104,1024]{1,0:T(8,128)(2,1)S(1)}, u32[]{:S(2)}, u32[]{:S(2)}) collective-permute-start(bf16[104,1024]{1,0:T(8,128)(2,1)S(1)} %collective-permute-done.refs_2_), channel_id=1, source_target_pairs={{0,4},{1,5},{2,6},{3,7},{4,0},{5,1},{6,2},{7,3},{8,12},{9,13},{10,... | collective-permute-start | bytes 638984 | tf_op jit(solution)/shard_map/ppermute | solution.py:40
  47.1 2.6 %collective-permute-start.12 = (bf16[104,1024]{1,0:T(8,128)(2,1)S(1)}, bf16[104,1024]{1,0:T(8,128)(2,1)S(1)}, u32[]{:S(2)}, u32[]{:S(2)}) collective-permute-start(bf16[104,1024]{1,0:T(8,128)(2,1)S(1)} %collective-permute-done.3.refs_3_), channel_id=1, source_target_pairs={{0,4},{1,5},{2,6},{3,7},{4,0},{5,1},{6,2},{7,3},{8,12},{9,13},{10,... | collective-permute-start | bytes 638984 | tf_op jit(solution)/shard_map/ppermute | solution.py:40
  47.6 2.6 %collective-permute-start.13 = (bf16[104,1024]{1,0:T(8,128)(2,1)S(1)}, bf16[104,1024]{1,0:T(8,128)(2,1)S(1)}, u32[]{:S(2)}, u32[]{:S(2)}) collective-permute-start(bf16[104,1024]{1,0:T(8,128)(2,1)S(1)} %collective-permute-done.1.refs_4_), channel_id=1, source_target_pairs={{0,4},{1,5},{2,6},{3,7},{4,0},{5,1},{6,2},{7,3},{8,12},{9,13},{10,... | collective-permute-start | bytes 638984 | tf_op jit(solution)/shard_map/ppermute | solution.py:40
  47.6 21.0 %collective-permute-start.22 = (bf16[1024,512]{1,0:T(8,128)(2,1)S(1)}, bf16[1024,512]{1,0:T(8,128)(2,1)S(1)}, u32[]{:S(2)}, u32[]{:S(2)}) collective-permute-start(bf16[1024,512]{1,0:T(8,128)(2,1)S(1)} %shard_map.205), channel_id=1, source_target_pairs={{0,2},{1,3},{2,0},{3,1},{4,5},{5,4},{6,7},{7,6},{8,10},{9,11},{10,... | collective-permute-start | bytes 3145736 | tf_op jit(solution)/shard_map/ppermute | solution.py:40
  49.2 37.2 %collective-permute-start.24 = (bf16[1024,512]{1,0:T(8,128)(2,1)S(1)}, bf16[1024,512]{1,0:T(8,128)(2,1)S(1)}, u32[]{:S(2)}, u32[]{:S(2)}) collective-permute-start(bf16[1024,512]{1,0:T(8,128)(2,1)S(1)} %shard_map.206), channel_id=1, source_target_pairs={{0,2},{1,3},{2,0},{3,1},{4,5},{5,4},{6,7},{7,6},{8,10},{9,11},{10,... | collective-permute-start | bytes 3145736 | tf_op jit(solution)/shard_map/ppermute | solution.py:40
  49.7 6.5 %collective-permute-start.14 = (bf16[104,1024]{1,0:T(8,128)(2,1)S(1)}, bf16[104,1024]{1,0:T(8,128)(2,1)S(1)}, u32[]{:S(2)}, u32[]{:S(2)}) collective-permute-start(bf16[104,1024]{1,0:T(8,128)(2,1)S(1)} %collective-permute-done.4.refs_5_), channel_id=1, source_target_pairs={{0,4},{1,5},{2,6},{3,7},{4,0},{5,1},{6,2},{7,3},{8,12},{9,13},{10,... | collective-permute-start | bytes 638984 | tf_op jit(solution)/shard_map/ppermute | solution.py:40
  49.7 8.1 %collective-permute-start.15 = (bf16[104,1024]{1,0:T(8,128)(2,1)S(1)}, bf16[104,1024]{1,0:T(8,128)(2,1)S(1)}, u32[]{:S(2)}, u32[]{:S(2)}) collective-permute-start(bf16[104,1024]{1,0:T(8,128)(2,1)S(1)} %collective-permute-done.2.refs_6_), channel_id=1, source_target_pairs={{0,4},{1,5},{2,6},{3,7},{4,0},{5,1},{6,2},{7,3},{8,12},{9,13},{10,... | collective-permute-start | bytes 638984 | tf_op jit(solution)/shard_map/ppermute | solution.py:40
  50.2 7.6 %collective-permute-start.16 = (bf16[104,1024]{1,0:T(8,128)(2,1)S(1)}, bf16[104,1024]{1,0:T(8,128)(2,1)S(1)}, u32[]{:S(2)}, u32[]{:S(2)}) collective-permute-start(bf16[104,1024]{1,0:T(8,128)(2,1)S(1)} %collective-permute-done.5.refs_7_), channel_id=1, source_target_pairs={{0,4},{1,5},{2,6},{3,7},{4,0},{5,1},{6,2},{7,3},{8,12},{9,13},{10,... | collective-permute-start | bytes 638984 | tf_op jit(solution)/shard_map/ppermute | solution.py:40
  50.3 2.2 %copy-start.3 = (bf16[1,2048,1024]{2,1,0:T(8,128)(2,1)S(1)}, bf16[1,2048,1024]{2,1,0:T(8,128)(2,1)}, u32[]{:S(2)}) copy-start(bf16[1,2048,1024]{2,1,0:T(8,128)(2,1)} %param.34) | copy-start | bytes 12582916
  56.2 11.1 %copy-start.5 = (bf16[2048,256]{1,0:T(8,128)(2,1)S(1)}, bf16[2048,256]{1,0:T(8,128)(2,1)}, u32[]{:S(2)}) copy-start(bf16[2048,256]{1,0:T(8,128)(2,1)} %sg_ref.1) | copy-start | bytes 3145732
  56.2 11.1 %copy-start.6 = (bf16[2048,256]{1,0:T(8,128)(2,1)S(1)}, bf16[2048,256]{1,0:T(8,128)(2,1)}, u32[]{:S(2)}) copy-start(bf16[2048,256]{1,0:T(8,128)(2,1)} %su_ref.1) | copy-start | bytes 3145732
  56.2 11.1 %copy-start.10 = (bf16[256,512]{1,0:T(8,128)(2,1)S(1)}, bf16[256,512]{1,0:T(8,128)(2,1)}, u32[]{:S(2)}) copy-start(bf16[256,512]{1,0:T(8,128)(2,1)} %gate_ref.1) | copy-start | bytes 786436
  56.2 11.1 %copy-start.18 = (f32[512]{0:T(512)S(1)}, f32[512]{0:T(512)}, u32[]{:S(2)}) copy-start(f32[512]{0:T(512)} %param.27) | copy-start | bytes 6148
  56.2 16.3 %collective-permute-start.23 = (bf16[288,1024]{1,0:T(8,128)(2,1)S(1)}, bf16[288,1024]{1,0:T(8,128)(2,1)S(1)}, u32[]{:S(2)}, u32[]{:S(2)}) collective-permute-start(bf16[288,1024]{1,0:T(8,128)(2,1)S(1)} %get-tuple-element.59.refs_0_), channel_id=1, source_target_pairs={{0,1},{1,0},{2,3},{3,2},{4,6},{5,7},{6,4},{7,5},{8,9},{9,8},{10,11... | collective-permute-start | bytes 1769480 | tf_op jit(solution)/shard_map/ppermute | solution.py:40
  61.7 25.1 %collective-permute-start.17 = (bf16[288,1024]{1,0:T(8,128)(2,1)S(1)}, bf16[288,1024]{1,0:T(8,128)(2,1)S(1)}, u32[]{:S(2)}, u32[]{:S(2)}) collective-permute-start(bf16[288,1024]{1,0:T(8,128)(2,1)S(1)} %get-tuple-element.68.refs_1_), channel_id=1, source_target_pairs={{0,1},{1,0},{2,3},{3,2},{4,6},{5,7},{6,4},{7,5},{8,9},{9,8},{10,11... | collective-permute-start | bytes 1769480 | tf_op jit(solution)/shard_map/ppermute | solution.py:40
  62.3 1.3 %collective-permute-start.18 = (bf16[136,256]{1,0:T(8,128)(2,1)S(1)}, bf16[136,256]{1,0:T(8,128)(2,1)S(1)}, u32[]{:S(2)}, u32[]{:S(2)}) collective-permute-start(bf16[136,256]{1,0:T(8,128)(2,1)S(1)} %get-tuple-element.52), channel_id=1, source_target_pairs={{0,4},{1,5},{2,6},{3,7},{4,0},{5,1},{6,2},{7,3},{8,12},{9,13},{10,... | collective-permute-start | bytes 208904 | tf_op jit(solution)/shard_map/ppermute | solution.py:40
  63.5 1.3 %collective-permute-start.19 = (bf16[136,256]{1,0:T(8,128)(2,1)S(1)}, bf16[136,256]{1,0:T(8,128)(2,1)S(1)}, u32[]{:S(2)}, u32[]{:S(2)}) collective-permute-start(bf16[136,256]{1,0:T(8,128)(2,1)S(1)} %collective-permute-done.6.refs_1_), channel_id=1, source_target_pairs={{0,4},{1,5},{2,6},{3,7},{4,0},{5,1},{6,2},{7,3},{8,12},{9,13},{10,... | collective-permute-start | bytes 208904 | tf_op jit(solution)/shard_map/ppermute | solution.py:40
  64.8 1.3 %collective-permute-start.20 = (bf16[136,256]{1,0:T(8,128)(2,1)S(1)}, bf16[136,256]{1,0:T(8,128)(2,1)S(1)}, u32[]{:S(2)}, u32[]{:S(2)}) collective-permute-start(bf16[136,256]{1,0:T(8,128)(2,1)S(1)} %collective-permute-done.7.refs_3_), channel_id=1, source_target_pairs={{0,4},{1,5},{2,6},{3,7},{4,0},{5,1},{6,2},{7,3},{8,12},{9,13},{10,... | collective-permute-start | bytes 208904 | tf_op jit(solution)/shard_map/ppermute | solution.py:40
  66.0 1.3 %collective-permute-start.21 = (bf16[136,256]{1,0:T(8,128)(2,1)S(1)}, bf16[136,256]{1,0:T(8,128)(2,1)S(1)}, u32[]{:S(2)}, u32[]{:S(2)}) collective-permute-start(bf16[136,256]{1,0:T(8,128)(2,1)S(1)} %collective-permute-done.8.refs_5_), channel_id=1, source_target_pairs={{0,4},{1,5},{2,6},{3,7},{4,0},{5,1},{6,2},{7,3},{8,12},{9,13},{10,... | collective-permute-start | bytes 208904 | tf_op jit(solution)/shard_map/ppermute | solution.py:40
  87.3 6.8 %collective-permute-start.25 = (bf16[288,512]{1,0:T(8,128)(2,1)S(1)}, bf16[288,512]{1,0:T(8,128)(2,1)S(1)}, u32[]{:S(2)}, u32[]{:S(2)}) collective-permute-start(bf16[288,512]{1,0:T(8,128)(2,1)S(1)} %shard_map.213), channel_id=1, source_target_pairs={{0,2},{1,3},{2,0},{3,1},{4,5},{5,4},{6,7},{7,6},{8,10},{9,11},{10,... | collective-permute-start | bytes 884744 | tf_op jit(solution)/shard_map/ppermute | solution.py:40
  90.2 23.5 %copy-start.4 = (bf16[2048,512]{1,0:T(8,128)(2,1)S(1)}, bf16[2048,512]{1,0:T(8,128)(2,1)}, u32[]{:S(2)}) copy-start(bf16[2048,512]{1,0:T(8,128)(2,1)} %refs_4_.1) | copy-start | bytes 6291460
  90.2 23.5 %copy-start.7 = (bf16[1024,512]{1,0:T(8,128)(2,1)S(1)}, bf16[1024,512]{1,0:T(8,128)(2,1)}, u32[]{:S(2)}) copy-start(bf16[1024,512]{1,0:T(8,128)(2,1)} %refs_5_.1) | copy-start | bytes 3145732
  94.4 9.4 %collective-permute-start.30 = (bf16[4,96,512]{2,1,0:T(8,128)(2,1)S(1)}, bf16[4,96,512]{2,1,0:T(8,128)(2,1)S(1)}, u32[]{:S(2)}, u32[]{:S(2)}) collective-permute-start(bf16[4,96,512]{2,1,0:T(8,128)(2,1)S(1)} %shard_map.214), channel_id=1, source_target_pairs={{0,4},{1,5},{2,6},{3,7},{4,0},{5,1},{6,2},{7,3},{8,12},{9,13},{10,... | collective-permute-start | bytes 1179656 | tf_op jit(solution)/shard_map/ppermute | solution.py:40
  94.5 9.0 %collective-permute-start.29 = (bf16[288,512]{1,0:T(8,128)(2,1)S(1)}, bf16[288,512]{1,0:T(8,128)(2,1)S(1)}, u32[]{:S(2)}, u32[]{:S(2)}) collective-permute-start(bf16[288,512]{1,0:T(8,128)(2,1)S(1)} %shard_map.211), channel_id=1, source_target_pairs={{0,2},{1,3},{2,0},{3,1},{4,5},{5,4},{6,7},{7,6},{8,10},{9,11},{10,... | collective-permute-start | bytes 884744 | tf_op jit(solution)/shard_map/ppermute | solution.py:40
  96.1 10.2 %collective-permute-start.26 = (bf16[304,512]{1,0:T(8,128)(2,1)S(1)}, bf16[304,512]{1,0:T(8,128)(2,1)S(1)}, u32[]{:S(2)}, u32[]{:S(2)}) collective-permute-start(bf16[304,512]{1,0:T(8,128)(2,1)S(1)} %shard_map.209.refs_0_), channel_id=1, source_target_pairs={{0,1},{1,0},{2,3},{3,2},{4,5},{5,4},{6,7},{7,6},{8,9},{9,8},{10,11... | collective-permute-start | bytes 933896 | tf_op jit(solution)/shard_map/ppermute | solution.py:40
  97.6 16.1 %collective-permute-start.27 = (bf16[304,512]{1,0:T(8,128)(2,1)S(1)}, bf16[304,512]{1,0:T(8,128)(2,1)S(1)}, u32[]{:S(2)}, u32[]{:S(2)}) collective-permute-start(bf16[304,512]{1,0:T(8,128)(2,1)S(1)} %shard_map.209.refs_0_), channel_id=1, source_target_pairs={{0,2},{1,3},{2,0},{3,1},{4,6},{5,7},{6,4},{7,5},{8,10},{9,11},{10,... | collective-permute-start | bytes 933896 | tf_op jit(solution)/shard_map/ppermute | solution.py:40
  98.1 15.6 %collective-permute-start.28 = (bf16[304,512]{1,0:T(8,128)(2,1)S(1)}, bf16[304,512]{1,0:T(8,128)(2,1)S(1)}, u32[]{:S(2)}, u32[]{:S(2)}) collective-permute-start(bf16[304,512]{1,0:T(8,128)(2,1)S(1)} %shard_map.209.refs_0_), channel_id=1, source_target_pairs={{0,3},{1,2},{2,1},{3,0},{4,7},{5,6},{6,5},{7,4},{8,11},{9,10},{10,... | collective-permute-start | bytes 933896 | tf_op jit(solution)/shard_map/ppermute | solution.py:40
  104.1 11.7 %collective-permute-start.33 = (bf16[96,512]{1,0:T(8,128)(2,1)S(1)}, bf16[96,512]{1,0:T(8,128)(2,1)S(1)}, u32[]{:S(2)}, u32[]{:S(2)}) collective-permute-start(bf16[96,512]{1,0:T(8,128)(2,1)S(1)} %get-tuple-element.93), channel_id=1, source_target_pairs={{0,8},{1,9},{2,10},{3,11},{4,12},{5,13},{6,14},{7,15},{8,16},{9,17... | collective-permute-start | bytes 294920 | tf_op jit(solution)/shard_map/ppermute | solution.py:40
  104.1 11.7 %collective-permute-start.32 = (bf16[96,512]{1,0:T(8,128)(2,1)S(1)}, bf16[96,512]{1,0:T(8,128)(2,1)S(1)}, u32[]{:S(2)}, u32[]{:S(2)}) collective-permute-start(bf16[96,512]{1,0:T(8,128)(2,1)S(1)} %get-tuple-element.94), channel_id=1, source_target_pairs={{0,16},{1,17},{2,18},{3,19},{4,20},{5,21},{6,22},{7,23},{8,24},{9,... | collective-permute-start | bytes 294920 | tf_op jit(solution)/shard_map/ppermute | solution.py:40
  106.3 9.5 %collective-permute-start.31 = (bf16[96,512]{1,0:T(8,128)(2,1)S(1)}, bf16[96,512]{1,0:T(8,128)(2,1)S(1)}, u32[]{:S(2)}, u32[]{:S(2)}) collective-permute-start(bf16[96,512]{1,0:T(8,128)(2,1)S(1)} %get-tuple-element.92), channel_id=1, source_target_pairs={{0,24},{1,25},{2,26},{3,27},{4,28},{5,29},{6,30},{7,31},{8,0},{9,1... | collective-permute-start | bytes 294920 | tf_op jit(solution)/shard_map/ppermute | solution.py:40

commit v2 on v1

--- a/solution.py
+++ b/solution.py
@@ -2,7 +2,6 @@
 
 import jax
 import jax.numpy as jnp
-import numpy as np
 from jax import lax
 from jax.experimental import pallas as pl
 from jax.experimental.pallas import tpu as pltpu
@@ -80,46 +79,35 @@
     return value / (1.0 + jnp.exp(-value))
 
 
-def column(n, core, x, y, du, dv):
-    if core == 0:
-        return (y + dv) % n * n + (x + du) % n
-    return (y + du) % n * n + (x + dv) % n
-
-
-class Index:
+class Here:
     def __init__(self, places):
-        n = places.side
-        table = [
-            [z, c, (x + y) % n, z * 2 + c]
-            + [column(n, c, x, y, -i, k) for k in range(n) for i in range(n)]
-            + [(y - dy) % n * n + (x - dx) % n for dy in range(n) for dx in range(n)]
-            for z in range(places.chips)
-            for c in range(2)
-            for y in range(n)
-            for x in range(n)
-        ]
-        here = lax.axis_index("ep") * places.tp + lax.axis_index("tp")
-        self.vector = lax.dynamic_index_in_dim(
-            jnp.asarray(np.array(table, np.int32)), here, 0, keepdims=False
-        )
-        self.z, self.c, self.part, self.e = range(4)
-        self.held, self.given = 4, 4 + n
-        self.tp = 4 + n * n
-
-    def rows(self, s_ref, place, ref, size):
-        start = pl.multiple_of(s_ref[place] * size, size)
-        return ref[pl.ds(start, size), :]
-
-
-def call(body, outs, operands, flops, smem=0, scratch=()):
-    specs = [pl.BlockSpec(memory_space=pltpu.SMEM)] * smem
-    specs += [pl.BlockSpec(memory_space=pltpu.VMEM)] * (len(operands) - smem)
-    given = list(operands[:smem])
-    given += [pltpu.with_memory_space_constraint(v, pltpu.VMEM) for v in operands[smem:]]
+        n = self.side = places.side
+        self.e = lax.axis_index("ep")
+        j = lax.axis_index("tp")
+        self.z, self.c = lax.div(self.e, 2), lax.rem(self.e, 2)
+        self.y, self.x = lax.div(j, n), lax.rem(j, n)
+        self.part = lax.rem(self.x + self.y, n)
+
+    def along(self, dy, dx):
+        n = self.side
+        return lax.rem(self.y + dy % n, n) * n + lax.rem(self.x + dx % n, n)
+
+    def column(self, du, dv):
+        return jnp.where(self.c == 0, self.along(dv, du), self.along(du, dv))
+
+
+def rows_of(ref, block, size):
+    return ref[pl.ds(pl.multiple_of(block * size, size), size), :]
+
+
+def call(body, outs, operands, flops, scratch=(), far=0):
+    given = list(operands[:far])
+    given += [pltpu.with_memory_space_constraint(v, pltpu.VMEM) for v in operands[far:]]
     return pl.pallas_call(
         body,
         out_shape=jax.tree.map(lambda o: pltpu.VMEM(o.shape, o.dtype), outs),
-        in_specs=specs,
+        in_specs=[pl.BlockSpec(memory_space=pltpu.HBM)] * far
+        + [pl.BlockSpec(memory_space=pltpu.VMEM)] * (len(operands) - far),
         out_specs=jax.tree.map(lambda _: pl.BlockSpec(memory_space=pltpu.VMEM), outs),
         scratch_shapes=list(scratch),
         compiler_params=pltpu.CompilerParams(vmem_limit_bytes=12 << 20),
@@ -189,7 +177,7 @@
 
 
 def finish_attention(
-    index, local, qd, states, gate_pre, gain, heads, normed, shared_gate, shared_up
+    places, local, qd, states, gate_pre, gain, heads, normed, shared_gate, shared_up
 ):
     rows = local.shape[0]
     dv, dk = local.shape[1] // heads, qd.shape[1] // heads
@@ -199,15 +187,16 @@
     sharing = local.shape[1] // hidden
     part = tokens // sharing
 
-    def body(s_ref, local_ref, qd_ref, gate_ref, gain_ref, normed_ref, sg_ref, su_ref, *refs):
+    def body(local_ref, qd_ref, gate_ref, gain_ref, normed_ref, sg_ref, su_ref, *refs):
         out_ref = refs[-1]
-        first = s_ref[index.c] == 0
+        here = Here(places)
+        first = here.c == 0
         between = jnp.ones((1, heads * dk), f32)
         incoming = jnp.zeros((dv, heads * dk), f32)
         sib = refs[0][...].astype(f32)
         for hop in range(1, (len(refs) - 2) // 2 + 1):
             mine, other = refs[2 * hop - 1][...].astype(f32), refs[2 * hop][...].astype(f32)
-            inside = s_ref[index.z] >= hop
+            inside = here.z >= hop
             early, late = jnp.where(first, mine, other), jnp.where(first, other, mine)
             decay = late[dv : dv + 1]
             got = early[0:dv] * decay + late[0:dv]
@@ -232,11 +221,11 @@
             ]
 
     out = jax.ShapeDtypeStruct((rows + part, local.shape[1]), bf16)
-    operands = (index.vector, local, qd, gate_pre, gain[None, :], normed, shared_gate, shared_up)
-    return call(body, out, operands + tuple(states), 1 << 27, smem=1)
-
-
-def project(index, gathered, attention_weight, shared_weight, tokens):
+    operands = (local, qd, gate_pre, gain[None, :], normed, shared_gate, shared_up)
+    return call(body, out, operands + tuple(states), 1 << 27)
+
+
+def project(places, gathered, attention_weight, shared_weight, tokens):
     count = len(gathered)
     folded, width = gathered[0].shape
     hidden, columns = shared_weight.shape[0] // count, shared_weight.shape[1]
@@ -244,16 +233,18 @@
     part = tokens // sharing
     rows = folded - part
 
-    def body(s_ref, *refs):
+    def body(*refs):
         weight_ref, shared_ref, mixed_ref, out_ref = refs[count:]
         mixed = shared = 0.0
+        here = Here(places)
         for i in range(count):
             ref = refs[i]
-            mixed = mixed + dot(ref[0:rows, :], index.rows(s_ref, index.tp + i, weight_ref, width))
+            block = here.along(-(i // here.side), -(i % here.side))
+            mixed = mixed + dot(ref[0:rows, :], rows_of(weight_ref, block, width))
             units = jnp.concatenate(
                 [ref[rows:, q * hidden : (q + 1) * hidden] for q in range(sharing)], axis=0
             )
-            shared = shared + dot(units, index.rows(s_ref, index.tp + i, shared_ref, hidden))
+            shared = shared + dot(units, rows_of(shared_ref, block, hidden))
         mixed_ref[...] = mixed.astype(bf16)
         out_ref[...] = shared
 
@@ -261,8 +252,8 @@
         jax.ShapeDtypeStruct((rows, columns), bf16),
         jax.ShapeDtypeStruct((tokens, columns), f32),
     )
-    operands = (index.vector, *gathered, attention_weight, shared_weight)
-    return call(body, outs, operands, 2 * folded * width * columns * count, smem=1)
+    operands = (*gathered, attention_weight, shared_weight)
+    return call(body, outs, operands, 2 * folded * width * columns * count)
 
 
 def prepare_rows(places, parts, rows, gain, index, scores, experts):
@@ -272,14 +263,26 @@
     pad = -(-tokens // 128) * 128
     extra = -(-experts // 8) * 8
 
-    def body(s_ref, rows_ref, gain_ref, index_ref, score_ref, normed_ref, packed_ref):
+    def body(rows_hbm, gain_hbm, index_hbm, score_hbm, normed_ref, packed_ref, *scratch):
+        rows_ref, gain_ref, index_ref, score_ref, done = scratch
+        copies = [
+            pltpu.make_async_copy(source, target, done.at[i])
+            for i, (source, target) in enumerate(
+                zip((rows_hbm, gain_hbm, index_hbm, score_hbm), scratch[:4])
+            )
+        ]
+        for copy in copies:
+            copy.start()
+        for copy in copies:
+            copy.wait()
+        here = Here(places)
         value = rows_ref[...].astype(f32)
         mean_square = jnp.mean(value * value, axis=1, keepdims=True)
         normed = (value * lax.rsqrt(mean_square + epsilon) * gain_ref[...]).astype(bf16)
         normed_ref[...] = normed
         for q in range(parts):
 
-            @pl.when(s_ref[places.part] == q)
+            @pl.when(here.part == q)
             def _():
                 packed_ref[0:tokens, :] = normed[:, q * piece : (q + 1) * piece]
 
@@ -305,8 +308,10 @@
         jax.ShapeDtypeStruct((tokens, width), bf16),
         jax.ShapeDtypeStruct((tokens + extra, piece), bf16),
     )
-    operands = (places.vector, rows, gain[None, :], index.T, scores.T)
-    return call(body, outs, operands, 1 << 22, smem=1)
+    operands = (rows, gain[None, :], index.T, scores.T)
+    scratch = [pltpu.VMEM(v.shape, v.dtype) for v in operands]
+    scratch.append(pltpu.SemaphoreType.DMA((4,)))
+    return call(body, outs, operands, 1 << 22, scratch=scratch, far=4)
 
 
 def group_of(sources, capacity):
@@ -316,7 +321,7 @@
     return group
 
 
-def expert_up(index, own, far, capacity, gate_weight, up_weight):
+def expert_up(places, own, far, capacity, gate_weight, up_weight):
     parts = len(far[0])
     tokens, width = own[0].shape
     packed_rows, piece = own[1].shape
@@ -329,17 +334,18 @@
     step = min(256, hidden)
     flat = list(own) + [p for pieces in far for p in pieces]
 
-    def body(s_ref, *refs):
+    def body(*refs):
         row_refs = refs[: len(flat)]
         gate_ref, up_ref, out_ref, info_ref, rows_ref, section_ref = refs[len(flat) :]
-        expert = lax.broadcasted_iota(jnp.int32, (extra, 2 * pad), 0) == s_ref[index.e]
+        here = Here(places)
+        expert = lax.broadcasted_iota(jnp.int32, (extra, 2 * pad), 0) == here.e
         if pad > tokens:
             for s in range(sources):
                 rows_ref[s * pad + tokens : (s + 1) * pad, :] = jnp.zeros((pad - tokens, width), bf16)
         rows_ref[0:tokens, :] = row_refs[0][...]
         for q in range(parts):
 
-            @pl.when(s_ref[index.part] == q)
+            @pl.when(here.part == q)
             def _():
                 for s in range(1, sources):
                     for i in range(parts):
@@ -374,25 +380,28 @@
         jax.ShapeDtypeStruct((sources, 2 * pad), f32),
     )
     scratch = (pltpu.VMEM((sources * pad, width), bf16), pltpu.VMEM((slots, width), bf16))
-    operands = (index.vector, *flat, gate_weight, up_weight)
-    return call(body, outs, operands, 4 * slots * width * hidden, smem=1, scratch=scratch)
-
-
-def take_block(index, weight, place, hidden):
-    def body(s_ref, in_ref, out_ref):
-        out_ref[...] = index.rows(s_ref, place, in_ref, hidden)
+    operands = (*flat, gate_weight, up_weight)
+    return call(body, outs, operands, 4 * slots * width * hidden, scratch=scratch)
+
+
+def take_block(places, weight, du, dv, hidden):
+    def body(in_ref, out_ref, done):
+        start = pl.multiple_of(Here(places).column(du, dv) * hidden, hidden)
+        copy = pltpu.make_async_copy(in_ref.at[pl.ds(start, hidden), :], out_ref, done)
+        copy.start()
+        copy.wait()
 
     out = jax.ShapeDtypeStruct((hidden, weight.shape[1]), weight.dtype)
-    return call(body, out, (index.vector, weight), 1 << 20, smem=1)
-
-
-def down_first(index, hiddens, weight, traded):
+    return call(body, out, (weight,), 1 << 20, scratch=(pltpu.SemaphoreType.DMA,), far=1)
+
+
+def down_first(places, hiddens, weight, traded):
     hidden, columns = hiddens[0].shape[1], weight.shape[1]
     chunks, partners = len(hiddens), len(traded)
 
-    def body(s_ref, *refs):
+    def body(*refs):
         outs = refs[chunks + 1 + partners :]
-        weights = [index.rows(s_ref, index.held, refs[chunks], hidden)]
+        weights = [rows_of(refs[chunks], Here(places).column(0, 0), hidden)]
         weights += [ref[...] for ref in refs[chunks + 1 : chunks + 1 + partners]]
         for w, weight in enumerate(weights):
             for h in range(chunks):
@@ -402,7 +411,7 @@
         jax.ShapeDtypeStruct((h.shape[0], columns), f32) for _ in range(1 + partners) for h in hiddens
     ]
     flops = 2 * sum(h.shape[0] for h in hiddens) * hidden * columns * (1 + partners)
-    outs = call(body, shapes, (index.vector, *hiddens, weight, *traded), flops, smem=1)
+    outs = call(body, shapes, (*hiddens, weight, *traded), flops)
     return [outs[w * chunks : (w + 1) * chunks] for w in range(1 + partners)]
 
 
@@ -420,25 +429,26 @@
     return call(body, out, (first, *hiddens, *weights), flops)
 
 
-def down_own(index, firsts, gathered, weight):
+def down_own(places, firsts, gathered, weight):
     count, chunks = len(gathered), len(firsts)
     hidden, columns = gathered[0][0].shape[1], weight.shape[1]
 
-    def body(s_ref, *refs):
+    def body(*refs):
         hidden_refs = refs[chunks : chunks + count * chunks]
         weight_ref = refs[chunks + count * chunks]
         outs = refs[chunks + count * chunks + 1 :]
+        here = Here(places)
         for h in range(chunks):
             total = refs[h][...]
             for i in range(count):
-                rows = index.rows(s_ref, index.held + 1 + i, weight_ref, hidden)
+                rows = rows_of(weight_ref, here.column(-1 - i, 0), hidden)
                 total = total + dot(hidden_refs[i * chunks + h][...], rows)
             outs[h][...] = total
 
     flat = [h for pieces in gathered for h in pieces]
     outs = [jax.ShapeDtypeStruct(f.shape, f32) for f in firsts]
     flops = 2 * sum(h.shape[0] for h in flat) * hidden * columns
-    return call(body, outs, (index.vector, *firsts, *flat, weight), flops, smem=1)
+    return call(body, outs, (*firsts, *flat, weight), flops)
 
 
 def combine(own, back, info, tokens, capacity, out_type):
@@ -488,7 +498,6 @@
     shared_down_weight,
 ):
     at = Places()
-    index = Index(at)
     n, chips, experts = at.side, at.chips, at.ep
     heads = added_log_decay.shape[0]
     tokens, top_count = routed_expert_index.shape
@@ -500,11 +509,11 @@
     )
     hidden = gate_weight.shape[1]
 
-    def down_block(k, i):
-        return take_block(index, down_weight, index.given + (k - 1) * n + i, hidden)
+    def trade(k, i):
+        return at.along_v(take_block(at, down_weight, -i, k, hidden), k)
 
     normed, packed = prepare_rows(
-        index,
+        at,
         n,
         second_batch_rows,
         expert_norm_gain,
@@ -512,8 +521,12 @@
         router_chosen_scores,
         experts,
     )
-    far = [at.along_z(packed, k) for k in range(1, chips)]
-    early = [down_block(k, 0) for k in range(1, n)]
+    middle = chips // 2
+    far = {middle: at.along_z(packed, middle)}
+    traded = [[trade(k, 0)] for k in range(1, n)]
+    far |= {k: at.along_z(packed, k) for k in range(1, chips) if k != middle}
+    for k in range(1, n):
+        traded[k - 1] += [trade(k, i) for i in range(1, n)]
     o_local, q_device, own_state = local_attention(
         first_batch_queries,
         first_batch_keys,
@@ -522,29 +535,23 @@
         channel_decay_bias,
         added_log_decay,
     )
-    far, own_state, early = hold((far, own_state, early))
-    traded = [[at.along_v(early[k - 1], k)] for k in range(1, n)]
-    arrived = [at.up_z(own_state, hop) for hop in range(1, chips)]
-    far = [[a] + [at.along_u(a, i) for i in range(1, n)] for a in far]
-    late = [[down_block(k, i) for i in range(1, n)] for k in range(1, n)]
-    far, arrived, late = hold((far, arrived, late))
+    arrived = [at.along_z(own_state, hop) for hop in range(1, chips)]
     states = [at.to_sibling(own_state)]
     for state in arrived:
         states += [state, at.to_sibling(state)]
-    for k in range(1, n):
-        traded[k - 1] += [at.along_v(block, k) for block in late[k - 1]]
-    ups = [expert_up(index, (normed, packed), far, capacity, gate_weight, up_weight)]
-    other = (
-        (at.to_sibling(normed), at.to_sibling(packed)),
-        [[at.to_sibling(p) for p in pieces] for pieces in far],
-    )
+    parts = [far[k] for k in range(1, chips)]
+    far = [[a] + [at.along_u(a, i) for i in range(1, n)] for a in parts]
+    other = ((at.to_sibling(normed), at.to_sibling(packed)), [[at.to_sibling(a)] for a in parts])
+    for pieces, others in zip(far, other[1]):
+        others += [at.to_sibling(p) for p in pieces[1:]]
+    ups = [expert_up(at, (normed, packed), far, capacity, gate_weight, up_weight)]
     gathered_first = [at.along_u(ups[0][0], i) for i in range(1, n)]
     _, other = hold((ups[0][0], other))
-    ups.append(expert_up(index, *other, capacity, gate_weight, up_weight))
+    ups.append(expert_up(at, *other, capacity, gate_weight, up_weight))
     hiddens = [up[0] for up in ups]
     gathered_second = [at.along_u(hiddens[1], i) for i in range(1, n)]
     both = finish_attention(
-        index,
+        at,
         o_local,
         q_device,
         states,
@@ -555,7 +562,7 @@
         shared_gate_weight,
         shared_up_weight,
     )
-    firsts = down_first(index, hiddens, down_weight, [t[0] for t in traded])
+    firsts = down_first(at, hiddens, down_weight, [t[0] for t in traded])
 
     def partials(chunk, gathered):
         return [
@@ -568,7 +575,7 @@
     partial = partials(1, gathered_second)
     back.append([at.along_v(partial[k - 1], -k) for k in range(1, n)])
     gathered = [list(pair) for pair in zip(gathered_first, gathered_second)]
-    owns = down_own(index, firsts[0], gathered, down_weight)
+    owns = down_own(at, firsts[0], gathered, down_weight)
     here, there = [
         combine(owns[chunk], back[chunk], ups[chunk][1], tokens, capacity, (f32, bf16)[chunk])
         for chunk in range(2)
@@ -586,7 +593,7 @@
         for dx in range(n)
     ]
     token_mixed, shared_total = project(
-        index, mixed, attention_output_weight, shared_down_weight, tokens
+        at, mixed, attention_output_weight, shared_down_weight, tokens
     )
     channel_mixed = (routed_total + shared_total).astype(bf16)
     return (token_mixed, channel_mixed)

time: 118 us -> 106 us (0.90)
  Pallas kernels: 20.6 us -> 15.9 us
  local copies, waits for them, and re-layouts: 9.21 us -> 6.04 us
  starting transfers between devices: 37 us -> 35.1 us
  waiting for transfers between devices: 47.9 us -> 46.6 us
    pallas_call x14, Pallas kernels: 20.6 us -> 15.9 us  [call(): pl.pallas_call(body, out_shape=jax.tree.map(lambda o: pltpu.VMEM(o.shape,...]
    unnamed x41, local copies, waits for them, and re-layouts: 8.49 us -> 6.02 us
    ppermute x34, starting transfers between devices: 37 us -> 35.1 us  [send(): return lax.ppermute(value, AXES, self.pairs(move))]
    ppermute x34, waiting for transfers between devices: 47.9 us -> 46.6 us  [send(): return lax.ppermute(value, AXES, self.pairs(move))]
  transfers between devices with their start and end apart: 34 -> 34, of which waited for: 14 -> 14; matrix products, arithmetic and copies ran while one was open for 1% -> 1% of each run, Pallas kernels for 16% -> 14%
where the time goes in v2:
time: 106 us; the launch traced here: 105 us
  waiting for transfers between devices  46.6 us (44%)
  starting transfers between devices  35.1 us (33%)
  Pallas kernels  15.9 us (15%)
  local copies, waits for them, and re-layouts  6.04 us (6%)
    ppermute x34, waiting for transfers between devices, send(): return lax.ppermute(value, AXES, self.pairs(move))  46.6 us
    ppermute x34, starting transfers between devices, send(): return lax.ppermute(value, AXES, self.pairs(move))  35.1 us
    pallas_call x14, Pallas kernels, call(): pl.pallas_call(body, out_shape=jax.tree.map(lambda o: pltpu.VMEM(o.shape,...  15.9 us
    unnamed x41, local copies, waits for them, and re-layouts  6.02 us
  transfers between devices with their start and end apart: 34, of which 14 were waited for; matrix products, arithmetic and copies ran while one was open for 1% of the time, Pallas kernels for 14%

profile of v2, /device:TPU:0, one launch (start us, length us, event | category | flops | bytes accessed | tf_op | source)
XLA Modules:
  0.0 105.4 jit_solution(17280572326316713804)
XLA Ops:
  0.6 1.0 copy-done.8
  1.6 0.7 copy-done.14
  2.3 0.7 copy-done.16
  3.0 0.7 copy-done.17
  3.7 0.6 shard_map.194
  4.3 3.1 %collective-permute-start = (bf16[104,1024]{1,0:T(8,128)(2,1)S(1)}, bf16[104,1024]{1,0:T(8,128)(2,1)S(1)}, u32[]{:S(2)}, u32[]{:S(2)}) collective-permute-start(bf16[104,1024]{1,0:T(8,128)(2,1)S(1)} %get-tuple-element.32.refs_1_), channel_id=1, source_target_pairs={{0,8},{1,9},{2,10},{3,11},{4,12},{5,13},{6,14},{7,15},{8,16},{9,17... | collective-permute-start | bytes 638984 | tf_op jit(solution)/shard_map/ppermute | solution.py:39
  7.4 2.6 %collective-permute-start.2 = (bf16[104,1024]{1,0:T(8,128)(2,1)S(1)}, bf16[104,1024]{1,0:T(8,128)(2,1)S(1)}, u32[]{:S(2)}, u32[]{:S(2)}) collective-permute-start(bf16[104,1024]{1,0:T(8,128)(2,1)S(1)} %get-tuple-element.32.refs_1_), channel_id=1, source_target_pairs={{0,16},{1,17},{2,18},{3,19},{4,20},{5,21},{6,22},{7,23},{8,24},{9,... | collective-permute-start | bytes 638984 | tf_op jit(solution)/shard_map/ppermute | solution.py:39
  10.0 1.3 %collective-permute-start.4 = (bf16[104,1024]{1,0:T(8,128)(2,1)S(1)}, bf16[104,1024]{1,0:T(8,128)(2,1)S(1)}, u32[]{:S(2)}, u32[]{:S(2)}) collective-permute-start(bf16[104,1024]{1,0:T(8,128)(2,1)S(1)} %get-tuple-element.32.refs_1_), channel_id=1, source_target_pairs={{0,24},{1,25},{2,26},{3,27},{4,28},{5,29},{6,30},{7,31},{8,0},{9,1... | collective-permute-start | bytes 638984 | tf_op jit(solution)/shard_map/ppermute | solution.py:39
  11.3 4.3 %collective-permute-done.refs_2_ = bf16[104,1024]{1,0:T(8,128)(2,1)S(1)} collective-permute-done((bf16[104,1024]{1,0:T(8,128)(2,1)S(1)}, bf16[104,1024]{1,0:T(8,128)(2,1)S(1)}, u32[]{:S(2)}, u32[]{:S(2)}) %collective-permute-start) | collective-permute-done | bytes 213024 | tf_op jit(solution)/shard_map/ppermute | solution.py:39
  15.6 1.7 %collective-permute-start.1 = (bf16[104,1024]{1,0:T(8,128)(2,1)S(1)}, bf16[104,1024]{1,0:T(8,128)(2,1)S(1)}, u32[]{:S(2)}, u32[]{:S(2)}) collective-permute-start(bf16[104,1024]{1,0:T(8,128)(2,1)S(1)} %collective-permute-done.refs_2_), channel_id=1, source_target_pairs={{0,1},{1,0},{2,3},{3,2},{4,6},{5,7},{6,4},{7,5},{8,9},{9,8},{10,11... | collective-permute-start | bytes 638984 | tf_op jit(solution)/shard_map/ppermute | solution.py:39
  17.3 6.5 %collective-permute-done.2.refs_4_ = bf16[104,1024]{1,0:T(8,128)(2,1)S(1)} collective-permute-done((bf16[104,1024]{1,0:T(8,128)(2,1)S(1)}, bf16[104,1024]{1,0:T(8,128)(2,1)S(1)}, u32[]{:S(2)}, u32[]{:S(2)}) %collective-permute-start.2) | collective-permute-done | bytes 213024 | tf_op jit(solution)/shard_map/ppermute | solution.py:39
  23.8 1.5 %collective-permute-start.3 = (bf16[104,1024]{1,0:T(8,128)(2,1)S(1)}, bf16[104,1024]{1,0:T(8,128)(2,1)S(1)}, u32[]{:S(2)}, u32[]{:S(2)}) collective-permute-start(bf16[104,1024]{1,0:T(8,128)(2,1)S(1)} %collective-permute-done.2.refs_4_), channel_id=1, source_target_pairs={{0,1},{1,0},{2,3},{3,2},{4,6},{5,7},{6,4},{7,5},{8,9},{9,8},{10,11... | collective-permute-start | bytes 638984 | tf_op jit(solution)/shard_map/ppermute | solution.py:39
  25.3 0.5 collective-permute-start.5
  25.9 0.5 collective-permute-start.10
  26.4 2.2 %copy-done = bf16[1,4096,512]{2,1,0:T(8,128)(2,1)S(1)} copy-done((bf16[1,4096,512]{2,1,0:T(8,128)(2,1)S(1)}, bf16[1,4096,512]{2,1,0:T(8,128)(2,1)}, u32[]{:S(2)}) %copy-start) | copy-done | bytes 4194328
  28.7 0.1 shard_map.199
  28.8 0.9 collective-permute-done.3.refs_5_
  29.7 1.5 %collective-permute-start.22 = (bf16[1024,512]{1,0:T(8,128)(2,1)S(1)}, bf16[1024,512]{1,0:T(8,128)(2,1)S(1)}, u32[]{:S(2)}, u32[]{:S(2)}) collective-permute-start(bf16[1024,512]{1,0:T(8,128)(2,1)S(1)} %shard_map.199), channel_id=1, source_target_pairs={{0,2},{1,3},{2,0},{3,1},{4,5},{5,4},{6,7},{7,6},{8,10},{9,11},{10,... | collective-permute-start | bytes 3145736 | tf_op jit(solution)/shard_map/ppermute | solution.py:39
  31.2 0.1 shard_map.201
  31.3 0.7 collective-permute-done.5.refs_7_
  32.0 1.5 %collective-permute-start.24 = (bf16[1024,512]{1,0:T(8,128)(2,1)S(1)}, bf16[1024,512]{1,0:T(8,128)(2,1)S(1)}, u32[]{:S(2)}, u32[]{:S(2)}) collective-permute-start(bf16[1024,512]{1,0:T(8,128)(2,1)S(1)} %shard_map.201), channel_id=1, source_target_pairs={{0,2},{1,3},{2,0},{3,1},{4,5},{5,4},{6,7},{7,6},{8,10},{9,11},{10,... | collective-permute-start | bytes 3145736 | tf_op jit(solution)/shard_map/ppermute | solution.py:39
  33.5 3.3 %shard_map.197 = (f32[256,512]{1,0:T(8,128)S(1)}, bf16[256,256]{1,0:T(8,128)(2,1)S(1)}, bf16[136,256]{1,0:T(8,128)(2,1)S(1)}) custom-call(bf16[256,256]{1,0:T(8,128)(2,1)S(1)} %copy-done.11, bf16[256,256]{1,0:T(8,128)(2,1)S(1)} %copy-done.12, bf16[256,512]{1,0:T(8,128)(2,1)S(1)} %copy-done.9, bf16[256,256]{1,0:T(8,128)(2,1)S(1)} %copy-done.13, ...), custom_call_target="tpu_custom_call" | custom-call | flops 33554432 | tf_op jit(solution)/shard_map/pallas_call | solution.py:106
  36.8 0.5 collective-permute-start.11
  37.3 0.1 collective-permute-start.13
  37.4 3.2 %shard_map.195 = (bf16[288,1024]{1,0:T(8,128)(2,1)S(1)}, f32[4,256]{1,0:T(4,128)S(1)}) custom-call(bf16[96,2048]{1,0:T(8,128)(2,1)S(1)} %get-tuple-element.31.refs_0_.normed_ref, bf16[104,1024]{1,0:T(8,128)(2,1)S(1)} %get-tuple-element.32.refs_1_, bf16[104,1024]{1,0:T(8,128)(2,1)S(1)} %collective-permute-done.refs_2_, ...), custom_call_target="tpu_custom_call" | custom-call | flops 2415919104 | tf_op jit(solution)/shard_map/pallas_call | solution.py:106
  40.6 0.5 collective-permute-start.15
  41.1 1.6 %collective-permute-start.23 = (bf16[288,1024]{1,0:T(8,128)(2,1)S(1)}, bf16[288,1024]{1,0:T(8,128)(2,1)S(1)}, u32[]{:S(2)}, u32[]{:S(2)}) collective-permute-start(bf16[288,1024]{1,0:T(8,128)(2,1)S(1)} %get-tuple-element.33.refs_0_), channel_id=1, source_target_pairs={{0,1},{1,0},{2,3},{3,2},{4,6},{5,7},{6,4},{7,5},{8,9},{9,8},{10,11... | collective-permute-start | bytes 1769480 | tf_op jit(solution)/shard_map/ppermute | solution.py:39
  42.7 3.2 %shard_map.196 = (bf16[288,1024]{1,0:T(8,128)(2,1)S(1)}, f32[4,256]{1,0:T(4,128)S(1)}) custom-call(bf16[96,2048]{1,0:T(8,128)(2,1)S(1)} %collective-permute-done.6.refs_0_, bf16[104,1024]{1,0:T(8,128)(2,1)S(1)} %collective-permute-done.7.refs_1_, bf16[104,1024]{1,0:T(8,128)(2,1)S(1)} %collective-permute-done.8.refs_2_, ...), custom_call_target="tpu_custom_call" | custom-call | flops 2415919104 | tf_op jit(solution)/shard_map/pallas_call | solution.py:106
  45.9 0.6 collective-permute-start.14
  46.5 3.3 %collective-permute-start.16 = (bf16[136,256]{1,0:T(8,128)(2,1)S(1)}, bf16[136,256]{1,0:T(8,128)(2,1)S(1)}, u32[]{:S(2)}, u32[]{:S(2)}) collective-permute-start(bf16[136,256]{1,0:T(8,128)(2,1)S(1)} %get-tuple-element.45), channel_id=1, source_target_pairs={{0,8},{1,9},{2,10},{3,11},{4,12},{5,13},{6,14},{7,15},{8,16},{9,17... | collective-permute-start | bytes 208904 | tf_op jit(solution)/shard_map/ppermute | solution.py:39
  49.8 5.1 %collective-permute-done.16.refs_1_ = bf16[136,256]{1,0:T(8,128)(2,1)S(1)} collective-permute-done((bf16[136,256]{1,0:T(8,128)(2,1)S(1)}, bf16[136,256]{1,0:T(8,128)(2,1)S(1)}, u32[]{:S(2)}, u32[]{:S(2)}) %collective-permute-start.16) | collective-permute-done | bytes 69664 | tf_op jit(solution)/shard_map/ppermute | solution.py:39
  54.9 0.2 collective-permute-start.18
  55.1 5.5 %collective-permute-done.18.refs_3_ = bf16[136,256]{1,0:T(8,128)(2,1)S(1)} collective-permute-done((bf16[136,256]{1,0:T(8,128)(2,1)S(1)}, bf16[136,256]{1,0:T(8,128)(2,1)S(1)}, u32[]{:S(2)}, u32[]{:S(2)}) %collective-permute-start.18) | collective-permute-done | bytes 69664 | tf_op jit(solution)/shard_map/ppermute | solution.py:39
  60.6 1.5 %collective-permute-start.20 = (bf16[136,256]{1,0:T(8,128)(2,1)S(1)}, bf16[136,256]{1,0:T(8,128)(2,1)S(1)}, u32[]{:S(2)}, u32[]{:S(2)}) collective-permute-start(bf16[136,256]{1,0:T(8,128)(2,1)S(1)} %get-tuple-element.45), channel_id=1, source_target_pairs={{0,24},{1,25},{2,26},{3,27},{4,28},{5,29},{6,30},{7,31},{8,0},{9,1... | collective-permute-start | bytes 208904 | tf_op jit(solution)/shard_map/ppermute | solution.py:39
  62.1 2.8 %collective-permute-done.20.refs_5_ = bf16[136,256]{1,0:T(8,128)(2,1)S(1)} collective-permute-done((bf16[136,256]{1,0:T(8,128)(2,1)S(1)}, bf16[136,256]{1,0:T(8,128)(2,1)S(1)}, u32[]{:S(2)}, u32[]{:S(2)}) %collective-permute-start.20) | collective-permute-done | bytes 69664 | tf_op jit(solution)/shard_map/ppermute | solution.py:39
  64.9 1.3 %collective-permute-done.17.refs_2_ = bf16[136,256]{1,0:T(8,128)(2,1)S(1)} collective-permute-done((bf16[136,256]{1,0:T(8,128)(2,1)S(1)}, bf16[136,256]{1,0:T(8,128)(2,1)S(1)}, u32[]{:S(2)}, u32[]{:S(2)}) %collective-permute-start.17) | collective-permute-done | bytes 69664 | tf_op jit(solution)/shard_map/ppermute | solution.py:39
  66.2 0.2 collective-permute-start.19
  66.3 1.1 %collective-permute-done.19.refs_4_ = bf16[136,256]{1,0:T(8,128)(2,1)S(1)} collective-permute-done((bf16[136,256]{1,0:T(8,128)(2,1)S(1)}, bf16[136,256]{1,0:T(8,128)(2,1)S(1)}, u32[]{:S(2)}, u32[]{:S(2)}) %collective-permute-start.19) | collective-permute-done | bytes 69664 | tf_op jit(solution)/shard_map/ppermute | solution.py:39
  67.4 0.2 collective-permute-start.21
  67.6 1.1 %collective-permute-done.21.refs_6_ = bf16[136,256]{1,0:T(8,128)(2,1)S(1)} collective-permute-done((bf16[136,256]{1,0:T(8,128)(2,1)S(1)}, bf16[136,256]{1,0:T(8,128)(2,1)S(1)}, u32[]{:S(2)}, u32[]{:S(2)}) %collective-permute-start.21) | collective-permute-done | bytes 69664 | tf_op jit(solution)/shard_map/ppermute | solution.py:39
  68.7 0.8 shard_map.198.refs_0_
  69.5 1.4 %shard_map.200 = (f32[288,512]{1,0:T(8,128)S(1)}, f32[288,512]{1,0:T(8,128)S(1)}, f32[288,512]{1,0:T(8,128)S(1)}, f32[288,512]{1,0:T(8,128)S(1)}) custom-call(bf16[288,1024]{1,0:T(8,128)(2,1)S(1)} %get-tuple-element.33.refs_0_, bf16[288,1024]{1,0:T(8,128)(2,1)S(1)} %get-tuple-element.42.refs_1_, bf16[4096,512]{1,0:T(8,128)(2,1)S(1)} %bitcast.28, ...), custom_call_target="tpu_custom_call" | custom-call | flops 1207959552 | tf_op jit(solution)/shard_map/pallas_call | solution.py:106
  71.0 0.5 shard_map.202
  71.5 0.5 shard_map.204
  72.0 0.6 collective-permute-start.25
  72.5 0.8 shard_map.203
  73.4 5.4 %collective-permute-done.25.refs_0_ = bf16[288,512]{1,0:T(8,128)(2,1)S(1)} collective-permute-done((bf16[288,512]{1,0:T(8,128)(2,1)S(1)}, bf16[288,512]{1,0:T(8,128)(2,1)S(1)}, u32[]{:S(2)}, u32[]{:S(2)}) %collective-permute-start.25) | collective-permute-done | bytes 294944 | tf_op jit(solution)/shard_map/ppermute | solution.py:39
  78.8 0.4 shard_map.205
  79.1 0.1 collective-permute-start.30
  79.2 0.6 collective-permute-start.29
  79.8 6.2 %collective-permute-done.29.refs_0_ = bf16[288,512]{1,0:T(8,128)(2,1)S(1)} collective-permute-done((bf16[288,512]{1,0:T(8,128)(2,1)S(1)}, bf16[288,512]{1,0:T(8,128)(2,1)S(1)}, u32[]{:S(2)}, u32[]{:S(2)}) %collective-permute-start.29) | collective-permute-done | bytes 294944 | tf_op jit(solution)/shard_map/ppermute | solution.py:39
  86.0 0.4 shard_map.207
  86.3 1.5 %collective-permute-start.26 = (bf16[304,512]{1,0:T(8,128)(2,1)S(1)}, bf16[304,512]{1,0:T(8,128)(2,1)S(1)}, u32[]{:S(2)}, u32[]{:S(2)}) collective-permute-start(bf16[304,512]{1,0:T(8,128)(2,1)S(1)} %shard_map.198.refs_0_), channel_id=1, source_target_pairs={{0,1},{1,0},{2,3},{3,2},{4,5},{5,4},{6,7},{7,6},{8,9},{9,8},{10,11... | collective-permute-start | bytes 933896 | tf_op jit(solution)/shard_map/ppermute | solution.py:39
  87.9 0.5 collective-permute-start.27
  88.4 1.5 %collective-permute-start.28 = (bf16[304,512]{1,0:T(8,128)(2,1)S(1)}, bf16[304,512]{1,0:T(8,128)(2,1)S(1)}, u32[]{:S(2)}, u32[]{:S(2)}) collective-permute-start(bf16[304,512]{1,0:T(8,128)(2,1)S(1)} %shard_map.198.refs_0_), channel_id=1, source_target_pairs={{0,3},{1,2},{2,1},{3,0},{4,7},{5,6},{6,5},{7,4},{8,11},{9,10},{10,... | collective-permute-start | bytes 933896 | tf_op jit(solution)/shard_map/ppermute | solution.py:39
  89.9 0.2 fusion.5
  90.1 0.8 collective-permute-start.33
  90.9 3.1 %collective-permute-start.32 = (bf16[96,512]{1,0:T(8,128)(2,1)S(1)}, bf16[96,512]{1,0:T(8,128)(2,1)S(1)}, u32[]{:S(2)}, u32[]{:S(2)}) collective-permute-start(bf16[96,512]{1,0:T(8,128)(2,1)S(1)} %get-tuple-element.64), channel_id=1, source_target_pairs={{0,16},{1,17},{2,18},{3,19},{4,20},{5,21},{6,22},{7,23},{8,24},{9,... | collective-permute-start | bytes 294920 | tf_op jit(solution)/shard_map/ppermute | solution.py:39
  94.0 2.6 %collective-permute-done.26.refs_1_ = bf16[304,512]{1,0:T(8,128)(2,1)S(1)} collective-permute-done((bf16[304,512]{1,0:T(8,128)(2,1)S(1)}, bf16[304,512]{1,0:T(8,128)(2,1)S(1)}, u32[]{:S(2)}, u32[]{:S(2)}) %collective-permute-start.26) | collective-permute-done | bytes 311328 | tf_op jit(solution)/shard_map/ppermute | solution.py:39
  96.6 3.3 %collective-permute-start.31 = (bf16[96,512]{1,0:T(8,128)(2,1)S(1)}, bf16[96,512]{1,0:T(8,128)(2,1)S(1)}, u32[]{:S(2)}, u32[]{:S(2)}) collective-permute-start(bf16[96,512]{1,0:T(8,128)(2,1)S(1)} %get-tuple-element.62), channel_id=1, source_target_pairs={{0,24},{1,25},{2,26},{3,27},{4,28},{5,29},{6,30},{7,31},{8,0},{9,1... | collective-permute-start | bytes 294920 | tf_op jit(solution)/shard_map/ppermute | solution.py:39
  100.0 3.1 %collective-permute-done.27.refs_2_ = bf16[304,512]{1,0:T(8,128)(2,1)S(1)} collective-permute-done((bf16[304,512]{1,0:T(8,128)(2,1)S(1)}, bf16[304,512]{1,0:T(8,128)(2,1)S(1)}, u32[]{:S(2)}, u32[]{:S(2)}) %collective-permute-start.27) | collective-permute-done | bytes 311328 | tf_op jit(solution)/shard_map/ppermute | solution.py:39
  103.1 0.9 shard_map.206
  104.0 0.7 copy.21
  104.7 0.7 fusion.4
  (62 shorter events, 0.3 us)
Async XLA Ops:
  0.6 1.0 copy-start.8
  1.6 0.7 copy-start.14
  2.3 0.7 copy-start.16
  3.0 0.7 copy-start.17
  4.3 11.3 %collective-permute-start = (bf16[104,1024]{1,0:T(8,128)(2,1)S(1)}, bf16[104,1024]{1,0:T(8,128)(2,1)S(1)}, u32[]{:S(2)}, u32[]{:S(2)}) collective-permute-start(bf16[104,1024]{1,0:T(8,128)(2,1)S(1)} %get-tuple-element.32.refs_1_), channel_id=1, source_target_pairs={{0,8},{1,9},{2,10},{3,11},{4,12},{5,13},{6,14},{7,15},{8,16},{9,17... | collective-permute-start | bytes 638984 | tf_op jit(solution)/shard_map/ppermute | solution.py:39
  7.4 18.5 %collective-permute-start.6 = (bf16[96,2048]{1,0:T(8,128)(2,1)S(1)}, bf16[96,2048]{1,0:T(8,128)(2,1)S(1)}, u32[]{:S(2)}, u32[]{:S(2)}) collective-permute-start(bf16[96,2048]{1,0:T(8,128)(2,1)S(1)} %get-tuple-element.31.refs_0_.normed_ref), channel_id=1, source_target_pairs={{0,4},{1,5},{2,6},{3,7},{4,0},{5,1},{6,2},{7,3},{8,12},{9,13},{10,... | collective-permute-start | bytes 1179656 | tf_op jit(solution)/shard_map/ppermute | solution.py:39
  7.4 16.4 %collective-permute-start.2 = (bf16[104,1024]{1,0:T(8,128)(2,1)S(1)}, bf16[104,1024]{1,0:T(8,128)(2,1)S(1)}, u32[]{:S(2)}, u32[]{:S(2)}) collective-permute-start(bf16[104,1024]{1,0:T(8,128)(2,1)S(1)} %get-tuple-element.32.refs_1_), channel_id=1, source_target_pairs={{0,16},{1,17},{2,18},{3,19},{4,20},{5,21},{6,22},{7,23},{8,24},{9,... | collective-permute-start | bytes 638984 | tf_op jit(solution)/shard_map/ppermute | solution.py:39
  10.0 15.3 %collective-permute-start.4 = (bf16[104,1024]{1,0:T(8,128)(2,1)S(1)}, bf16[104,1024]{1,0:T(8,128)(2,1)S(1)}, u32[]{:S(2)}, u32[]{:S(2)}) collective-permute-start(bf16[104,1024]{1,0:T(8,128)(2,1)S(1)} %get-tuple-element.32.refs_1_), channel_id=1, source_target_pairs={{0,24},{1,25},{2,26},{3,27},{4,28},{5,29},{6,30},{7,31},{8,0},{9,1... | collective-permute-start | bytes 638984 | tf_op jit(solution)/shard_map/ppermute | solution.py:39
  11.3 14.5 %collective-permute-start.7 = (bf16[104,1024]{1,0:T(8,128)(2,1)S(1)}, bf16[104,1024]{1,0:T(8,128)(2,1)S(1)}, u32[]{:S(2)}, u32[]{:S(2)}) collective-permute-start(bf16[104,1024]{1,0:T(8,128)(2,1)S(1)} %get-tuple-element.32.refs_1_), channel_id=1, source_target_pairs={{0,4},{1,5},{2,6},{3,7},{4,0},{5,1},{6,2},{7,3},{8,12},{9,13},{10,... | collective-permute-start | bytes 638984 | tf_op jit(solution)/shard_map/ppermute | solution.py:39
  15.6 10.8 %collective-permute-start.1 = (bf16[104,1024]{1,0:T(8,128)(2,1)S(1)}, bf16[104,1024]{1,0:T(8,128)(2,1)S(1)}, u32[]{:S(2)}, u32[]{:S(2)}) collective-permute-start(bf16[104,1024]{1,0:T(8,128)(2,1)S(1)} %collective-permute-done.refs_2_), channel_id=1, source_target_pairs={{0,1},{1,0},{2,3},{3,2},{4,6},{5,7},{6,4},{7,5},{8,9},{9,8},{10,11... | collective-permute-start | bytes 638984 | tf_op jit(solution)/shard_map/ppermute | solution.py:39
  23.8 5.8 %collective-permute-start.3 = (bf16[104,1024]{1,0:T(8,128)(2,1)S(1)}, bf16[104,1024]{1,0:T(8,128)(2,1)S(1)}, u32[]{:S(2)}, u32[]{:S(2)}) collective-permute-start(bf16[104,1024]{1,0:T(8,128)(2,1)S(1)} %collective-permute-done.2.refs_4_), channel_id=1, source_target_pairs={{0,1},{1,0},{2,3},{3,2},{4,6},{5,7},{6,4},{7,5},{8,9},{9,8},{10,11... | collective-permute-start | bytes 638984 | tf_op jit(solution)/shard_map/ppermute | solution.py:39
  25.3 6.7 %collective-permute-start.5 = (bf16[104,1024]{1,0:T(8,128)(2,1)S(1)}, bf16[104,1024]{1,0:T(8,128)(2,1)S(1)}, u32[]{:S(2)}, u32[]{:S(2)}) collective-permute-start(bf16[104,1024]{1,0:T(8,128)(2,1)S(1)} %collective-permute-done.4.refs_6_), channel_id=1, source_target_pairs={{0,1},{1,0},{2,3},{3,2},{4,6},{5,7},{6,4},{7,5},{8,9},{9,8},{10,11... | collective-permute-start | bytes 638984 | tf_op jit(solution)/shard_map/ppermute | solution.py:39
  25.9 10.9 %collective-permute-start.8 = (bf16[104,1024]{1,0:T(8,128)(2,1)S(1)}, bf16[104,1024]{1,0:T(8,128)(2,1)S(1)}, u32[]{:S(2)}, u32[]{:S(2)}) collective-permute-start(bf16[104,1024]{1,0:T(8,128)(2,1)S(1)} %collective-permute-done.refs_2_), channel_id=1, source_target_pairs={{0,4},{1,5},{2,6},{3,7},{4,0},{5,1},{6,2},{7,3},{8,12},{9,13},{10,... | collective-permute-start | bytes 638984 | tf_op jit(solution)/shard_map/ppermute | solution.py:39
  25.9 11.0 %collective-permute-start.10 = (bf16[104,1024]{1,0:T(8,128)(2,1)S(1)}, bf16[104,1024]{1,0:T(8,128)(2,1)S(1)}, u32[]{:S(2)}, u32[]{:S(2)}) collective-permute-start(bf16[104,1024]{1,0:T(8,128)(2,1)S(1)} %collective-permute-done.2.refs_4_), channel_id=1, source_target_pairs={{0,4},{1,5},{2,6},{3,7},{4,0},{5,1},{6,2},{7,3},{8,12},{9,13},{10,... | collective-permute-start | bytes 638984 | tf_op jit(solution)/shard_map/ppermute | solution.py:39
  26.4 11.0 %collective-permute-start.12 = (bf16[104,1024]{1,0:T(8,128)(2,1)S(1)}, bf16[104,1024]{1,0:T(8,128)(2,1)S(1)}, u32[]{:S(2)}, u32[]{:S(2)}) collective-permute-start(bf16[104,1024]{1,0:T(8,128)(2,1)S(1)} %collective-permute-done.4.refs_6_), channel_id=1, source_target_pairs={{0,4},{1,5},{2,6},{3,7},{4,0},{5,1},{6,2},{7,3},{8,12},{9,13},{10,... | collective-permute-start | bytes 638984 | tf_op jit(solution)/shard_map/ppermute | solution.py:39
  26.4 2.2 %copy-start = (bf16[1,4096,512]{2,1,0:T(8,128)(2,1)S(1)}, bf16[1,4096,512]{2,1,0:T(8,128)(2,1)}, u32[]{:S(2)}) copy-start(bf16[1,4096,512]{2,1,0:T(8,128)(2,1)} %param.34) | copy-start | bytes 12582916
  28.6 4.9 %copy-start.9 = (bf16[256,512]{1,0:T(8,128)(2,1)S(1)}, bf16[256,512]{1,0:T(8,128)(2,1)}, u32[]{:S(2)}) copy-start(bf16[256,512]{1,0:T(8,128)(2,1)} %v_ref.1) | copy-start | bytes 786436
  28.6 4.9 %copy-start.11 = (bf16[256,256]{1,0:T(8,128)(2,1)S(1)}, bf16[256,256]{1,0:T(8,128)(2,1)}, u32[]{:S(2)}) copy-start(bf16[256,256]{1,0:T(8,128)(2,1)} %q_ref.1) | copy-start | bytes 393220
  28.6 4.9 %copy-start.12 = (bf16[256,256]{1,0:T(8,128)(2,1)S(1)}, bf16[256,256]{1,0:T(8,128)(2,1)}, u32[]{:S(2)}) copy-start(bf16[256,256]{1,0:T(8,128)(2,1)} %k_ref.1) | copy-start | bytes 393220
  28.6 4.9 %copy-start.13 = (bf16[256,256]{1,0:T(8,128)(2,1)S(1)}, bf16[256,256]{1,0:T(8,128)(2,1)}, u32[]{:S(2)}) copy-start(bf16[256,256]{1,0:T(8,128)(2,1)} %d_ref.1) | copy-start | bytes 393220
  28.6 4.9 %copy-start.15 = (f32[4,256]{1,0:T(4,128)S(1)}, f32[4,256]{1,0:T(4,128)}, u32[]{:S(2)}) copy-start(f32[4,256]{1,0:T(4,128)} %added_ref.1) | copy-start | bytes 12292
  28.7 4.9 %copy-start.19 = (f32[256]{0:T(256)S(1)}, f32[256]{0:T(256)}, u32[]{:S(2)}) copy-start(f32[256]{0:T(256)} %param.24) | copy-start | bytes 3076
  28.7 8.8 %copy-start.3 = (bf16[1,2048,1024]{2,1,0:T(8,128)(2,1)S(1)}, bf16[1,2048,1024]{2,1,0:T(8,128)(2,1)}, u32[]{:S(2)}) copy-start(bf16[1,2048,1024]{2,1,0:T(8,128)(2,1)} %param.33) | copy-start | bytes 12582916
  28.8 8.6 %copy-start.2 = (bf16[1,2048,1024]{2,1,0:T(8,128)(2,1)S(1)}, bf16[1,2048,1024]{2,1,0:T(8,128)(2,1)}, u32[]{:S(2)}) copy-start(bf16[1,2048,1024]{2,1,0:T(8,128)(2,1)} %param.32) | copy-start | bytes 12582916
  29.7 39.9 %collective-permute-start.22 = (bf16[1024,512]{1,0:T(8,128)(2,1)S(1)}, bf16[1024,512]{1,0:T(8,128)(2,1)S(1)}, u32[]{:S(2)}, u32[]{:S(2)}) collective-permute-start(bf16[1024,512]{1,0:T(8,128)(2,1)S(1)} %shard_map.199), channel_id=1, source_target_pairs={{0,2},{1,3},{2,0},{3,1},{4,5},{5,4},{6,7},{7,6},{8,10},{9,11},{10,... | collective-permute-start | bytes 3145736 | tf_op jit(solution)/shard_map/ppermute | solution.py:39
  32.0 39.0 %collective-permute-start.24 = (bf16[1024,512]{1,0:T(8,128)(2,1)S(1)}, bf16[1024,512]{1,0:T(8,128)(2,1)S(1)}, u32[]{:S(2)}, u32[]{:S(2)}) collective-permute-start(bf16[1024,512]{1,0:T(8,128)(2,1)S(1)} %shard_map.201), channel_id=1, source_target_pairs={{0,2},{1,3},{2,0},{3,1},{4,5},{5,4},{6,7},{7,6},{8,10},{9,11},{10,... | collective-permute-start | bytes 3145736 | tf_op jit(solution)/shard_map/ppermute | solution.py:39
  36.8 3.8 %collective-permute-start.9 = (bf16[104,1024]{1,0:T(8,128)(2,1)S(1)}, bf16[104,1024]{1,0:T(8,128)(2,1)S(1)}, u32[]{:S(2)}, u32[]{:S(2)}) collective-permute-start(bf16[104,1024]{1,0:T(8,128)(2,1)S(1)} %collective-permute-done.1.refs_3_), channel_id=1, source_target_pairs={{0,4},{1,5},{2,6},{3,7},{4,0},{5,1},{6,2},{7,3},{8,12},{9,13},{10,... | collective-permute-start | bytes 638984 | tf_op jit(solution)/shard_map/ppermute | solution.py:39
  36.8 4.3 %collective-permute-start.11 = (bf16[104,1024]{1,0:T(8,128)(2,1)S(1)}, bf16[104,1024]{1,0:T(8,128)(2,1)S(1)}, u32[]{:S(2)}, u32[]{:S(2)}) collective-permute-start(bf16[104,1024]{1,0:T(8,128)(2,1)S(1)} %collective-permute-done.3.refs_5_), channel_id=1, source_target_pairs={{0,4},{1,5},{2,6},{3,7},{4,0},{5,1},{6,2},{7,3},{8,12},{9,13},{10,... | collective-permute-start | bytes 638984 | tf_op jit(solution)/shard_map/ppermute | solution.py:39
  37.3 5.3 %collective-permute-start.13 = (bf16[104,1024]{1,0:T(8,128)(2,1)S(1)}, bf16[104,1024]{1,0:T(8,128)(2,1)S(1)}, u32[]{:S(2)}, u32[]{:S(2)}) collective-permute-start(bf16[104,1024]{1,0:T(8,128)(2,1)S(1)} %collective-permute-done.5.refs_7_), channel_id=1, source_target_pairs={{0,4},{1,5},{2,6},{3,7},{4,0},{5,1},{6,2},{7,3},{8,12},{9,13},{10,... | collective-permute-start | bytes 638984 | tf_op jit(solution)/shard_map/ppermute | solution.py:39
  40.6 5.9 %collective-permute-start.15 = (bf16[136,256]{1,0:T(8,128)(2,1)S(1)}, bf16[136,256]{1,0:T(8,128)(2,1)S(1)}, u32[]{:S(2)}, u32[]{:S(2)}) collective-permute-start(bf16[136,256]{1,0:T(8,128)(2,1)S(1)} %get-tuple-element.45), channel_id=1, source_target_pairs={{0,4},{1,5},{2,6},{3,7},{4,0},{5,1},{6,2},{7,3},{8,12},{9,13},{10,... | collective-permute-start | bytes 208904 | tf_op jit(solution)/shard_map/ppermute | solution.py:39
  41.1 27.6 %copy-start.5 = (bf16[2048,256]{1,0:T(8,128)(2,1)S(1)}, bf16[2048,256]{1,0:T(8,128)(2,1)}, u32[]{:S(2)}) copy-start(bf16[2048,256]{1,0:T(8,128)(2,1)} %sg_ref.1) | copy-start | bytes 3145732
  41.1 27.6 %copy-start.6 = (bf16[2048,256]{1,0:T(8,128)(2,1)S(1)}, bf16[2048,256]{1,0:T(8,128)(2,1)}, u32[]{:S(2)}) copy-start(bf16[2048,256]{1,0:T(8,128)(2,1)} %su_ref.1) | copy-start | bytes 3145732
  41.1 27.6 %copy-start.10 = (bf16[256,512]{1,0:T(8,128)(2,1)S(1)}, bf16[256,512]{1,0:T(8,128)(2,1)}, u32[]{:S(2)}) copy-start(bf16[256,512]{1,0:T(8,128)(2,1)} %gate_ref.1) | copy-start | bytes 786436
  41.1 27.6 %copy-start.18 = (f32[512]{0:T(512)S(1)}, f32[512]{0:T(512)}, u32[]{:S(2)}) copy-start(f32[512]{0:T(512)} %param.26) | copy-start | bytes 6148
  41.1 29.9 %collective-permute-start.23 = (bf16[288,1024]{1,0:T(8,128)(2,1)S(1)}, bf16[288,1024]{1,0:T(8,128)(2,1)S(1)}, u32[]{:S(2)}, u32[]{:S(2)}) collective-permute-start(bf16[288,1024]{1,0:T(8,128)(2,1)S(1)} %get-tuple-element.33.refs_0_), channel_id=1, source_target_pairs={{0,1},{1,0},{2,3},{3,2},{4,6},{5,7},{6,4},{7,5},{8,9},{9,8},{10,11... | collective-permute-start | bytes 1769480 | tf_op jit(solution)/shard_map/ppermute | solution.py:39
  45.8 23.7 %copy-start.1 = (bf16[1,4096,512]{2,1,0:T(8,128)(2,1)S(1)}, bf16[1,4096,512]{2,1,0:T(8,128)(2,1)}, u32[]{:S(2)}) copy-start(bf16[1,4096,512]{2,1,0:T(8,128)(2,1)} %param.34) | copy-start | bytes 12582916
  45.9 25.6 %collective-permute-start.14 = (bf16[288,1024]{1,0:T(8,128)(2,1)S(1)}, bf16[288,1024]{1,0:T(8,128)(2,1)S(1)}, u32[]{:S(2)}, u32[]{:S(2)}) collective-permute-start(bf16[288,1024]{1,0:T(8,128)(2,1)S(1)} %get-tuple-element.42.refs_1_), channel_id=1, source_target_pairs={{0,1},{1,0},{2,3},{3,2},{4,6},{5,7},{6,4},{7,5},{8,9},{9,8},{10,11... | collective-permute-start | bytes 1769480 | tf_op jit(solution)/shard_map/ppermute | solution.py:39
  46.5 8.4 %collective-permute-start.16 = (bf16[136,256]{1,0:T(8,128)(2,1)S(1)}, bf16[136,256]{1,0:T(8,128)(2,1)S(1)}, u32[]{:S(2)}, u32[]{:S(2)}) collective-permute-start(bf16[136,256]{1,0:T(8,128)(2,1)S(1)} %get-tuple-element.45), channel_id=1, source_target_pairs={{0,8},{1,9},{2,10},{3,11},{4,12},{5,13},{6,14},{7,15},{8,16},{9,17... | collective-permute-start | bytes 208904 | tf_op jit(solution)/shard_map/ppermute | solution.py:39
  54.9 5.7 %collective-permute-start.18 = (bf16[136,256]{1,0:T(8,128)(2,1)S(1)}, bf16[136,256]{1,0:T(8,128)(2,1)S(1)}, u32[]{:S(2)}, u32[]{:S(2)}) collective-permute-start(bf16[136,256]{1,0:T(8,128)(2,1)S(1)} %get-tuple-element.45), channel_id=1, source_target_pairs={{0,16},{1,17},{2,18},{3,19},{4,20},{5,21},{6,22},{7,23},{8,24},{9,... | collective-permute-start | bytes 208904 | tf_op jit(solution)/shard_map/ppermute | solution.py:39
  60.6 4.3 %collective-permute-start.20 = (bf16[136,256]{1,0:T(8,128)(2,1)S(1)}, bf16[136,256]{1,0:T(8,128)(2,1)S(1)}, u32[]{:S(2)}, u32[]{:S(2)}) collective-permute-start(bf16[136,256]{1,0:T(8,128)(2,1)S(1)} %get-tuple-element.45), channel_id=1, source_target_pairs={{0,24},{1,25},{2,26},{3,27},{4,28},{5,29},{6,30},{7,31},{8,0},{9,1... | collective-permute-start | bytes 208904 | tf_op jit(solution)/shard_map/ppermute | solution.py:39
  64.9 1.3 %collective-permute-start.17 = (bf16[136,256]{1,0:T(8,128)(2,1)S(1)}, bf16[136,256]{1,0:T(8,128)(2,1)S(1)}, u32[]{:S(2)}, u32[]{:S(2)}) collective-permute-start(bf16[136,256]{1,0:T(8,128)(2,1)S(1)} %collective-permute-done.16.refs_1_), channel_id=1, source_target_pairs={{0,4},{1,5},{2,6},{3,7},{4,0},{5,1},{6,2},{7,3},{8,12},{9,13},{10,... | collective-permute-start | bytes 208904 | tf_op jit(solution)/shard_map/ppermute | solution.py:39
  66.2 1.3 %collective-permute-start.19 = (bf16[136,256]{1,0:T(8,128)(2,1)S(1)}, bf16[136,256]{1,0:T(8,128)(2,1)S(1)}, u32[]{:S(2)}, u32[]{:S(2)}) collective-permute-start(bf16[136,256]{1,0:T(8,128)(2,1)S(1)} %collective-permute-done.18.refs_3_), channel_id=1, source_target_pairs={{0,4},{1,5},{2,6},{3,7},{4,0},{5,1},{6,2},{7,3},{8,12},{9,13},{10,... | collective-permute-start | bytes 208904 | tf_op jit(solution)/shard_map/ppermute | solution.py:39
  67.4 1.3 %collective-permute-start.21 = (bf16[136,256]{1,0:T(8,128)(2,1)S(1)}, bf16[136,256]{1,0:T(8,128)(2,1)S(1)}, u32[]{:S(2)}, u32[]{:S(2)}) collective-permute-start(bf16[136,256]{1,0:T(8,128)(2,1)S(1)} %collective-permute-done.20.refs_5_), channel_id=1, source_target_pairs={{0,4},{1,5},{2,6},{3,7},{4,0},{5,1},{6,2},{7,3},{8,12},{9,13},{10,... | collective-permute-start | bytes 208904 | tf_op jit(solution)/shard_map/ppermute | solution.py:39
  72.0 6.8 %collective-permute-start.25 = (bf16[288,512]{1,0:T(8,128)(2,1)S(1)}, bf16[288,512]{1,0:T(8,128)(2,1)S(1)}, u32[]{:S(2)}, u32[]{:S(2)}) collective-permute-start(bf16[288,512]{1,0:T(8,128)(2,1)S(1)} %shard_map.204), channel_id=1, source_target_pairs={{0,2},{1,3},{2,0},{3,1},{4,5},{5,4},{6,7},{7,6},{8,10},{9,11},{10,... | collective-permute-start | bytes 884744 | tf_op jit(solution)/shard_map/ppermute | solution.py:39
  73.3 29.8 %copy-start.4 = (bf16[2048,512]{1,0:T(8,128)(2,1)S(1)}, bf16[2048,512]{1,0:T(8,128)(2,1)}, u32[]{:S(2)}) copy-start(bf16[2048,512]{1,0:T(8,128)(2,1)} %refs_4_.1) | copy-start | bytes 6291460
  73.3 29.8 %copy-start.7 = (bf16[1024,512]{1,0:T(8,128)(2,1)S(1)}, bf16[1024,512]{1,0:T(8,128)(2,1)}, u32[]{:S(2)}) copy-start(bf16[1024,512]{1,0:T(8,128)(2,1)} %refs_5_.1) | copy-start | bytes 3145732
  79.1 10.8 %collective-permute-start.30 = (bf16[4,96,512]{2,1,0:T(8,128)(2,1)S(1)}, bf16[4,96,512]{2,1,0:T(8,128)(2,1)S(1)}, u32[]{:S(2)}, u32[]{:S(2)}) collective-permute-start(bf16[4,96,512]{2,1,0:T(8,128)(2,1)S(1)} %shard_map.205), channel_id=1, source_target_pairs={{0,4},{1,5},{2,6},{3,7},{4,0},{5,1},{6,2},{7,3},{8,12},{9,13},{10,... | collective-permute-start | bytes 1179656 | tf_op jit(solution)/shard_map/ppermute | solution.py:39
  79.2 6.8 %collective-permute-start.29 = (bf16[288,512]{1,0:T(8,128)(2,1)S(1)}, bf16[288,512]{1,0:T(8,128)(2,1)S(1)}, u32[]{:S(2)}, u32[]{:S(2)}) collective-permute-start(bf16[288,512]{1,0:T(8,128)(2,1)S(1)} %shard_map.202), channel_id=1, source_target_pairs={{0,2},{1,3},{2,0},{3,1},{4,5},{5,4},{6,7},{7,6},{8,10},{9,11},{10,... | collective-permute-start | bytes 884744 | tf_op jit(solution)/shard_map/ppermute | solution.py:39
  86.3 10.3 %collective-permute-start.26 = (bf16[304,512]{1,0:T(8,128)(2,1)S(1)}, bf16[304,512]{1,0:T(8,128)(2,1)S(1)}, u32[]{:S(2)}, u32[]{:S(2)}) collective-permute-start(bf16[304,512]{1,0:T(8,128)(2,1)S(1)} %shard_map.198.refs_0_), channel_id=1, source_target_pairs={{0,1},{1,0},{2,3},{3,2},{4,5},{5,4},{6,7},{7,6},{8,9},{9,8},{10,11... | collective-permute-start | bytes 933896 | tf_op jit(solution)/shard_map/ppermute | solution.py:39
  87.9 15.2 %collective-permute-start.27 = (bf16[304,512]{1,0:T(8,128)(2,1)S(1)}, bf16[304,512]{1,0:T(8,128)(2,1)S(1)}, u32[]{:S(2)}, u32[]{:S(2)}) collective-permute-start(bf16[304,512]{1,0:T(8,128)(2,1)S(1)} %shard_map.198.refs_0_), channel_id=1, source_target_pairs={{0,2},{1,3},{2,0},{3,1},{4,6},{5,7},{6,4},{7,5},{8,10},{9,11},{10,... | collective-permute-start | bytes 933896 | tf_op jit(solution)/shard_map/ppermute | solution.py:39
  88.4 14.7 %collective-permute-start.28 = (bf16[304,512]{1,0:T(8,128)(2,1)S(1)}, bf16[304,512]{1,0:T(8,128)(2,1)S(1)}, u32[]{:S(2)}, u32[]{:S(2)}) collective-permute-start(bf16[304,512]{1,0:T(8,128)(2,1)S(1)} %shard_map.198.refs_0_), channel_id=1, source_target_pairs={{0,3},{1,2},{2,1},{3,0},{4,7},{5,6},{6,5},{7,4},{8,11},{9,10},{10,... | collective-permute-start | bytes 933896 | tf_op jit(solution)/shard_map/ppermute | solution.py:39
  90.1 14.6 %collective-permute-start.33 = (bf16[96,512]{1,0:T(8,128)(2,1)S(1)}, bf16[96,512]{1,0:T(8,128)(2,1)S(1)}, u32[]{:S(2)}, u32[]{:S(2)}) collective-permute-start(bf16[96,512]{1,0:T(8,128)(2,1)S(1)} %get-tuple-element.63), channel_id=1, source_target_pairs={{0,8},{1,9},{2,10},{3,11},{4,12},{5,13},{6,14},{7,15},{8,16},{9,17... | collective-permute-start | bytes 294920 | tf_op jit(solution)/shard_map/ppermute | solution.py:39
  90.9 13.8 %collective-permute-start.32 = (bf16[96,512]{1,0:T(8,128)(2,1)S(1)}, bf16[96,512]{1,0:T(8,128)(2,1)S(1)}, u32[]{:S(2)}, u32[]{:S(2)}) collective-permute-start(bf16[96,512]{1,0:T(8,128)(2,1)S(1)} %get-tuple-element.64), channel_id=1, source_target_pairs={{0,16},{1,17},{2,18},{3,19},{4,20},{5,21},{6,22},{7,23},{8,24},{9,... | collective-permute-start | bytes 294920 | tf_op jit(solution)/shard_map/ppermute | solution.py:39
  96.6 8.1 %collective-permute-start.31 = (bf16[96,512]{1,0:T(8,128)(2,1)S(1)}, bf16[96,512]{1,0:T(8,128)(2,1)S(1)}, u32[]{:S(2)}, u32[]{:S(2)}) collective-permute-start(bf16[96,512]{1,0:T(8,128)(2,1)S(1)} %get-tuple-element.62), channel_id=1, source_target_pairs={{0,24},{1,25},{2,26},{3,27},{4,28},{5,29},{6,30},{7,31},{8,0},{9,1... | collective-permute-start | bytes 294920 | tf_op jit(solution)/shard_map/ppermute | solution.py:39

commit v3 on v2

--- a/solution.py
+++ b/solution.py
@@ -9,6 +9,7 @@
 
 
 BLOCK = 64
+PIECES = 2
 epsilon = 1e-06
 temper = 16.0
 routed_scale = 2.5
@@ -101,7 +102,7 @@
 
 
 def call(body, outs, operands, flops, scratch=(), far=0):
-    given = list(operands[:far])
+    given = [pltpu.with_memory_space_constraint(v, pltpu.HBM) for v in operands[:far]]
     given += [pltpu.with_memory_space_constraint(v, pltpu.VMEM) for v in operands[far:]]
     return pl.pallas_call(
         body,
@@ -384,28 +385,41 @@
     return call(body, outs, operands, 4 * slots * width * hidden, scratch=scratch)
 
 
-def take_block(places, weight, du, dv, hidden):
+def take_piece(places, weight, du, dv, piece, hidden):
+    size = hidden // PIECES
+
     def body(in_ref, out_ref, done):
-        start = pl.multiple_of(Here(places).column(du, dv) * hidden, hidden)
-        copy = pltpu.make_async_copy(in_ref.at[pl.ds(start, hidden), :], out_ref, done)
+        start = Here(places).column(du, dv) * hidden + piece * size
+        copy = pltpu.make_async_copy(
+            in_ref.at[pl.ds(pl.multiple_of(start, size), size), :], out_ref, done
+        )
         copy.start()
         copy.wait()
 
-    out = jax.ShapeDtypeStruct((hidden, weight.shape[1]), weight.dtype)
+    out = jax.ShapeDtypeStruct((size, weight.shape[1]), weight.dtype)
     return call(body, out, (weight,), 1 << 20, scratch=(pltpu.SemaphoreType.DMA,), far=1)
+
+
+def dot_pieces(ref, pieces):
+    size = pieces[0].shape[0]
+    return sum(dot(ref[:, p * size : (p + 1) * size], piece[...]) for p, piece in enumerate(pieces))
 
 
 def down_first(places, hiddens, weight, traded):
     hidden, columns = hiddens[0].shape[1], weight.shape[1]
     chunks, partners = len(hiddens), len(traded)
+    traded = [piece for pieces in traded for piece in pieces]
 
     def body(*refs):
-        outs = refs[chunks + 1 + partners :]
-        weights = [rows_of(refs[chunks], Here(places).column(0, 0), hidden)]
-        weights += [ref[...] for ref in refs[chunks + 1 : chunks + 1 + partners]]
-        for w, weight in enumerate(weights):
-            for h in range(chunks):
-                outs[w * chunks + h][...] = dot(refs[h][...], weight)
+        outs = refs[chunks + 1 + len(traded) :]
+        weight = rows_of(refs[chunks], Here(places).column(0, 0), hidden)
+        for h in range(chunks):
+            outs[h][...] = dot(refs[h][...], weight)
+            for w in range(partners):
+                first = chunks + 1 + w * PIECES
+                outs[(w + 1) * chunks + h][...] = dot_pieces(
+                    refs[h], refs[first : first + PIECES]
+                )
 
     shapes = [
         jax.ShapeDtypeStruct((h.shape[0], columns), f32) for _ in range(1 + partners) for h in hiddens
@@ -421,12 +435,14 @@
     def body(first_ref, *refs):
         total = first_ref[...]
         for i in range(count):
-            total = total + dot(refs[i][...], refs[count + i][...])
+            first = count + i * PIECES
+            total = total + dot_pieces(refs[i], refs[first : first + PIECES])
         refs[-1][...] = total.astype(bf16)
 
     out = jax.ShapeDtypeStruct(first.shape, bf16)
     flops = 2 * first.size * hiddens[0].shape[1] * count
-    return call(body, out, (first, *hiddens, *weights), flops)
+    pieces = [piece for slices in weights for piece in slices]
+    return call(body, out, (first, *hiddens, *pieces), flops)
 
 
 def down_own(places, firsts, gathered, weight):
@@ -509,8 +525,15 @@
     )
     hidden = gate_weight.shape[1]
 
-    def trade(k, i):
-        return at.along_v(take_block(at, down_weight, -i, k, hidden), k)
+    traded = [[[] for _ in range(n)] for _ in range(1, n)]
+    lacking = [(i, piece) for i in range(n) for piece in range(PIECES)]
+
+    def trade(quarter):
+        share = len(lacking) // 4
+        for i, piece in lacking[quarter * share : (quarter + 1) * share]:
+            for k in range(1, n):
+                taken = take_piece(at, down_weight, -i, k, piece, hidden)
+                traded[k - 1][i].append(at.along_v(taken, k))
 
     normed, packed = prepare_rows(
         at,
@@ -523,10 +546,10 @@
     )
     middle = chips // 2
     far = {middle: at.along_z(packed, middle)}
-    traded = [[trade(k, 0)] for k in range(1, n)]
+    trade(0)
     far |= {k: at.along_z(packed, k) for k in range(1, chips) if k != middle}
-    for k in range(1, n):
-        traded[k - 1] += [trade(k, i) for i in range(1, n)]
+    trade(1)
+    trade(2)
     o_local, q_device, own_state = local_attention(
         first_batch_queries,
         first_batch_keys,
@@ -544,6 +567,7 @@
     other = ((at.to_sibling(normed), at.to_sibling(packed)), [[at.to_sibling(a)] for a in parts])
     for pieces, others in zip(far, other[1]):
         others += [at.to_sibling(p) for p in pieces[1:]]
+    trade(3)
     ups = [expert_up(at, (normed, packed), far, capacity, gate_weight, up_weight)]
     gathered_first = [at.along_u(ups[0][0], i) for i in range(1, n)]
     _, other = hold((ups[0][0], other))
@@ -576,11 +600,8 @@
     back.append([at.along_v(partial[k - 1], -k) for k in range(1, n)])
     gathered = [list(pair) for pair in zip(gathered_first, gathered_second)]
     owns = down_own(at, firsts[0], gathered, down_weight)
-    here, there = [
-        combine(owns[chunk], back[chunk], ups[chunk][1], tokens, capacity, (f32, bf16)[chunk])
-        for chunk in range(2)
-    ]
-    there, to_send = hold((there, both))
+    here = combine(owns[0], back[0], ups[0][1], tokens, capacity, f32)
+    there = combine(owns[1], back[1], ups[1][1], tokens, capacity, bf16)
     from_sibling = at.to_sibling(there)
     chip_sum = here + from_sibling.astype(f32)
     routed_total = chip_sum[0]
@@ -588,7 +609,7 @@
         routed_total = routed_total + at.along_z(chip_sum[k].astype(bf16), -k).astype(f32)
 
     mixed = [
-        both if dy == 0 and dx == 0 else at.along_tp(to_send, dy, dx)
+        both if dy == 0 and dx == 0 else at.along_tp(both, dy, dx)
         for dy in range(n)
         for dx in range(n)
     ]

time: 106 us -> 117 us (1.10)
  Pallas kernels: 15.9 us -> 21.3 us
  starting transfers between devices: 35.1 us -> 38.3 us
  waiting for transfers between devices: 46.6 us -> 48.7 us
    pallas_call x14 -> x16, Pallas kernels: 15.9 us -> 21.3 us  [call(): pl.pallas_call(body, out_shape=jax.tree.map(lambda o: pltpu.VMEM(o.shape,...]
    ppermute x34 -> x36, starting transfers between devices: 35.1 us -> 38.3 us  [send(): return lax.ppermute(value, AXES, self.pairs(move))]
    ppermute x34 -> x36, waiting for transfers between devices: 46.6 us -> 48.7 us  [send(): return lax.ppermute(value, AXES, self.pairs(move))]
    unnamed x41 -> x31, local copies, waits for them, and re-layouts: 6.02 us -> 5.78 us
  transfers between devices with their start and end apart: 34 -> 36, of which waited for: 14 -> 10; matrix products, arithmetic and copies ran while one was open for 1% -> 1% of each run, Pallas kernels for 14% -> 15%
where the time goes in v3:
time: 117 us; the launch traced here: 116 us
  waiting for transfers between devices  48.7 us (42%)
  starting transfers between devices  38.3 us (33%)
  Pallas kernels  21.3 us (18%)
  local copies, waits for them, and re-layouts  5.8 us (5%)
    ppermute x36, waiting for transfers between devices, send(): return lax.ppermute(value, AXES, self.pairs(move))  48.7 us
    ppermute x36, starting transfers between devices, send(): return lax.ppermute(value, AXES, self.pairs(move))  38.3 us
    pallas_call x16, Pallas kernels, call(): pl.pallas_call(body, out_shape=jax.tree.map(lambda o: pltpu.VMEM(o.shape,...  21.3 us
    unnamed x31, local copies, waits for them, and re-layouts  5.78 us
  transfers between devices with their start and end apart: 36, of which 10 were waited for; matrix products, arithmetic and copies ran while one was open for 1% of the time, Pallas kernels for 15%

profile of v3, /device:TPU:0, one launch (start us, length us, event | category | flops | bytes accessed | tf_op | source)
XLA Modules:
  0.0 115.9 jit_solution(16347369919759882742)
XLA Ops:
  0.6 0.9 copy-done.7
  1.6 0.9 copy-done.9
  2.5 0.9 copy-done.10
  3.4 0.9 copy-done.11
  4.3 0.7 copy-done.12
  5.0 0.7 copy-done.14
  5.7 3.3 %shard_map.197 = (f32[256,512]{1,0:T(8,128)S(1)}, bf16[256,256]{1,0:T(8,128)(2,1)S(1)}, bf16[136,256]{1,0:T(8,128)(2,1)S(1)}) custom-call(bf16[256,256]{1,0:T(8,128)(2,1)S(1)} %copy-done.9, bf16[256,256]{1,0:T(8,128)(2,1)S(1)} %copy-done.10, bf16[256,512]{1,0:T(8,128)(2,1)S(1)} %copy-done.7, bf16[256,256]{1,0:T(8,128)(2,1)S(1)} %copy-done.11, ...), custom_call_target="tpu_custom_call" | custom-call | flops 33554432 | tf_op jit(solution)/shard_map/pallas_call | solution.py:107
  8.9 3.1 %collective-permute-start.16 = (bf16[136,256]{1,0:T(8,128)(2,1)S(1)}, bf16[136,256]{1,0:T(8,128)(2,1)S(1)}, u32[]{:S(2)}, u32[]{:S(2)}) collective-permute-start(bf16[136,256]{1,0:T(8,128)(2,1)S(1)} %get-tuple-element.43), channel_id=1, source_target_pairs={{0,8},{1,9},{2,10},{3,11},{4,12},{5,13},{6,14},{7,15},{8,16},{9,17... | collective-permute-start | bytes 208904 | tf_op jit(solution)/shard_map/ppermute | solution.py:40
  12.0 1.4 %shard_map.194 = (bf16[96,2048]{1,0:T(8,128)(2,1)S(1)}, bf16[104,1024]{1,0:T(8,128)(2,1)S(1)}) custom-call(bf16[96,2048]{1,0:T(8,128)(2,1)} %rows_hbm.1, f32[1,2048]{1,0:T(1,128)} %bitcast.38, s32[4,96]{1,0:T(4,128)} %bitcast.39, f32[4,96]{1,0:T(4,128)} %bitcast.40), custom_call_target="tpu_custom_call" | custom-call | flops 4194304 | tf_op jit(solution)/shard_map/pallas_call | solution.py:107
  13.3 1.6 %collective-permute-start = (bf16[104,1024]{1,0:T(8,128)(2,1)S(1)}, bf16[104,1024]{1,0:T(8,128)(2,1)S(1)}, u32[]{:S(2)}, u32[]{:S(2)}) collective-permute-start(bf16[104,1024]{1,0:T(8,128)(2,1)S(1)} %get-tuple-element.30.refs_1_), channel_id=1, source_target_pairs={{0,8},{1,9},{2,10},{3,11},{4,12},{5,13},{6,14},{7,15},{8,16},{9,17... | collective-permute-start | bytes 638984 | tf_op jit(solution)/shard_map/ppermute | solution.py:40
  15.0 1.2 %collective-permute-start.2 = (bf16[104,1024]{1,0:T(8,128)(2,1)S(1)}, bf16[104,1024]{1,0:T(8,128)(2,1)S(1)}, u32[]{:S(2)}, u32[]{:S(2)}) collective-permute-start(bf16[104,1024]{1,0:T(8,128)(2,1)S(1)} %get-tuple-element.30.refs_1_), channel_id=1, source_target_pairs={{0,16},{1,17},{2,18},{3,19},{4,20},{5,21},{6,22},{7,23},{8,24},{9,... | collective-permute-start | bytes 638984 | tf_op jit(solution)/shard_map/ppermute | solution.py:40
  16.2 2.8 %collective-permute-start.4 = (bf16[104,1024]{1,0:T(8,128)(2,1)S(1)}, bf16[104,1024]{1,0:T(8,128)(2,1)S(1)}, u32[]{:S(2)}, u32[]{:S(2)}) collective-permute-start(bf16[104,1024]{1,0:T(8,128)(2,1)S(1)} %get-tuple-element.30.refs_1_), channel_id=1, source_target_pairs={{0,24},{1,25},{2,26},{3,27},{4,28},{5,29},{6,30},{7,31},{8,0},{9,1... | collective-permute-start | bytes 638984 | tf_op jit(solution)/shard_map/ppermute | solution.py:40
  18.9 4.5 %collective-permute-done.refs_2_ = bf16[104,1024]{1,0:T(8,128)(2,1)S(1)} collective-permute-done((bf16[104,1024]{1,0:T(8,128)(2,1)S(1)}, bf16[104,1024]{1,0:T(8,128)(2,1)S(1)}, u32[]{:S(2)}, u32[]{:S(2)}) %collective-permute-start) | collective-permute-done | bytes 213024 | tf_op jit(solution)/shard_map/ppermute | solution.py:40
  23.4 1.5 %collective-permute-start.1 = (bf16[104,1024]{1,0:T(8,128)(2,1)S(1)}, bf16[104,1024]{1,0:T(8,128)(2,1)S(1)}, u32[]{:S(2)}, u32[]{:S(2)}) collective-permute-start(bf16[104,1024]{1,0:T(8,128)(2,1)S(1)} %collective-permute-done.refs_2_), channel_id=1, source_target_pairs={{0,1},{1,0},{2,3},{3,2},{4,6},{5,7},{6,4},{7,5},{8,9},{9,8},{10,11... | collective-permute-start | bytes 638984 | tf_op jit(solution)/shard_map/ppermute | solution.py:40
  24.9 6.2 %collective-permute-done.2.refs_4_ = bf16[104,1024]{1,0:T(8,128)(2,1)S(1)} collective-permute-done((bf16[104,1024]{1,0:T(8,128)(2,1)S(1)}, bf16[104,1024]{1,0:T(8,128)(2,1)S(1)}, u32[]{:S(2)}, u32[]{:S(2)}) %collective-permute-start.2) | collective-permute-done | bytes 213024 | tf_op jit(solution)/shard_map/ppermute | solution.py:40
  31.1 1.5 %collective-permute-start.3 = (bf16[104,1024]{1,0:T(8,128)(2,1)S(1)}, bf16[104,1024]{1,0:T(8,128)(2,1)S(1)}, u32[]{:S(2)}, u32[]{:S(2)}) collective-permute-start(bf16[104,1024]{1,0:T(8,128)(2,1)S(1)} %collective-permute-done.2.refs_4_), channel_id=1, source_target_pairs={{0,1},{1,0},{2,3},{3,2},{4,6},{5,7},{6,4},{7,5},{8,9},{9,8},{10,11... | collective-permute-start | bytes 638984 | tf_op jit(solution)/shard_map/ppermute | solution.py:40
  32.6 0.6 collective-permute-start.5
  33.1 0.5 collective-permute-start.10
  33.7 3.2 %collective-permute-done.3.refs_5_ = bf16[104,1024]{1,0:T(8,128)(2,1)S(1)} collective-permute-done((bf16[104,1024]{1,0:T(8,128)(2,1)S(1)}, bf16[104,1024]{1,0:T(8,128)(2,1)S(1)}, u32[]{:S(2)}, u32[]{:S(2)}) %collective-permute-start.3) | collective-permute-done | bytes 213024 | tf_op jit(solution)/shard_map/ppermute | solution.py:40
  37.0 2.3 %collective-permute-done.5.refs_7_ = bf16[104,1024]{1,0:T(8,128)(2,1)S(1)} collective-permute-done((bf16[104,1024]{1,0:T(8,128)(2,1)S(1)}, bf16[104,1024]{1,0:T(8,128)(2,1)S(1)}, u32[]{:S(2)}, u32[]{:S(2)}) %collective-permute-start.5) | collective-permute-done | bytes 213024 | tf_op jit(solution)/shard_map/ppermute | solution.py:40
  39.2 0.5 collective-permute-start.13
  39.8 1.2 %shard_map.199 = bf16[512,512]{1,0:T(8,128)(2,1)S(1)} custom-call(bf16[4096,512]{1,0:T(8,128)(2,1)} %bitcast.26), custom_call_target="tpu_custom_call" | custom-call | flops 1048576 | tf_op jit(solution)/shard_map/pallas_call | solution.py:107
  41.0 1.6 %collective-permute-start.22 = (bf16[512,512]{1,0:T(8,128)(2,1)S(1)}, bf16[512,512]{1,0:T(8,128)(2,1)S(1)}, u32[]{:S(2)}, u32[]{:S(2)}) collective-permute-start(bf16[512,512]{1,0:T(8,128)(2,1)S(1)} %shard_map.199), channel_id=1, source_target_pairs={{0,2},{1,3},{2,0},{3,1},{4,5},{5,4},{6,7},{7,6},{8,10},{9,11},{10,... | collective-permute-start | bytes 1572872 | tf_op jit(solution)/shard_map/ppermute | solution.py:40
  42.5 1.0 shard_map.200
  43.7 4.5 %collective-permute-start.18 = (bf16[136,256]{1,0:T(8,128)(2,1)S(1)}, bf16[136,256]{1,0:T(8,128)(2,1)S(1)}, u32[]{:S(2)}, u32[]{:S(2)}) collective-permute-start(bf16[136,256]{1,0:T(8,128)(2,1)S(1)} %get-tuple-element.43), channel_id=1, source_target_pairs={{0,16},{1,17},{2,18},{3,19},{4,20},{5,21},{6,22},{7,23},{8,24},{9,... | collective-permute-start | bytes 208904 | tf_op jit(solution)/shard_map/ppermute | solution.py:40
  48.2 1.8 %collective-permute-start.20 = (bf16[136,256]{1,0:T(8,128)(2,1)S(1)}, bf16[136,256]{1,0:T(8,128)(2,1)S(1)}, u32[]{:S(2)}, u32[]{:S(2)}) collective-permute-start(bf16[136,256]{1,0:T(8,128)(2,1)S(1)} %get-tuple-element.43), channel_id=1, source_target_pairs={{0,24},{1,25},{2,26},{3,27},{4,28},{5,29},{6,30},{7,31},{8,0},{9,1... | collective-permute-start | bytes 208904 | tf_op jit(solution)/shard_map/ppermute | solution.py:40
  50.0 0.1 collective-permute-start.17
  50.2 3.2 %shard_map.195 = (bf16[288,1024]{1,0:T(8,128)(2,1)S(1)}, f32[4,256]{1,0:T(4,128)S(1)}) custom-call(bf16[96,2048]{1,0:T(8,128)(2,1)S(1)} %get-tuple-element.29.refs_0_.normed_ref, bf16[104,1024]{1,0:T(8,128)(2,1)S(1)} %get-tuple-element.30.refs_1_, bf16[104,1024]{1,0:T(8,128)(2,1)S(1)} %collective-permute-done.refs_2_, ...), custom_call_target="tpu_custom_call" | custom-call | flops 2415919104 | tf_op jit(solution)/shard_map/pallas_call | solution.py:107
  53.4 1.3 %collective-permute-start.23 = (bf16[512,512]{1,0:T(8,128)(2,1)S(1)}, bf16[512,512]{1,0:T(8,128)(2,1)S(1)}, u32[]{:S(2)}, u32[]{:S(2)}) collective-permute-start(bf16[512,512]{1,0:T(8,128)(2,1)S(1)} %shard_map.200), channel_id=1, source_target_pairs={{0,2},{1,3},{2,0},{3,1},{4,5},{5,4},{6,7},{7,6},{8,10},{9,11},{10,... | collective-permute-start | bytes 1572872 | tf_op jit(solution)/shard_map/ppermute | solution.py:40
  54.7 0.3 collective-permute-start.19
  55.0 0.2 collective-permute-start.21
  55.2 1.5 %collective-permute-start.24 = (bf16[288,1024]{1,0:T(8,128)(2,1)S(1)}, bf16[288,1024]{1,0:T(8,128)(2,1)S(1)}, u32[]{:S(2)}, u32[]{:S(2)}) collective-permute-start(bf16[288,1024]{1,0:T(8,128)(2,1)S(1)} %get-tuple-element.31.refs_0_), channel_id=1, source_target_pairs={{0,1},{1,0},{2,3},{3,2},{4,6},{5,7},{6,4},{7,5},{8,9},{9,8},{10,11... | collective-permute-start | bytes 1769480 | tf_op jit(solution)/shard_map/ppermute | solution.py:40
  56.7 3.3 %shard_map.196 = (bf16[288,1024]{1,0:T(8,128)(2,1)S(1)}, f32[4,256]{1,0:T(4,128)S(1)}) custom-call(bf16[96,2048]{1,0:T(8,128)(2,1)S(1)} %collective-permute-done.6.refs_0_, bf16[104,1024]{1,0:T(8,128)(2,1)S(1)} %collective-permute-done.7.refs_1_, bf16[104,1024]{1,0:T(8,128)(2,1)S(1)} %collective-permute-done.8.refs_2_, ...), custom_call_target="tpu_custom_call" | custom-call | flops 2415919104 | tf_op jit(solution)/shard_map/pallas_call | solution.py:107
  60.1 0.6 collective-permute-start.14
  60.7 1.1 shard_map.202
  61.9 1.2 %shard_map.203 = bf16[512,512]{1,0:T(8,128)(2,1)S(1)} custom-call(bf16[4096,512]{1,0:T(8,128)(2,1)} %bitcast.29), custom_call_target="tpu_custom_call" | custom-call | flops 1048576 | tf_op jit(solution)/shard_map/pallas_call | solution.py:107
  63.1 1.1 collective-permute-start.25
  64.2 1.0 collective-permute-start.26
  65.2 0.8 shard_map.198.refs_0_
  66.0 1.1 collective-permute-done.23.refs_4_
  67.1 1.4 %shard_map.201 = (f32[288,512]{1,0:T(8,128)S(1)}, f32[288,512]{1,0:T(8,128)S(1)}, f32[288,512]{1,0:T(8,128)S(1)}, f32[288,512]{1,0:T(8,128)S(1)}) custom-call(bf16[288,1024]{1,0:T(8,128)(2,1)S(1)} %get-tuple-element.31.refs_0_, bf16[288,1024]{1,0:T(8,128)(2,1)S(1)} %get-tuple-element.40.refs_1_, bf16[4096,512]{1,0:T(8,128)(2,1)S(1)} %bitcast.30, ...), custom_call_target="tpu_custom_call" | custom-call | flops 1207959552 | tf_op jit(solution)/shard_map/pallas_call | solution.py:107
  68.5 9.8 %collective-permute-done.25.refs_1_ = bf16[512,512]{1,0:T(8,128)(2,1)S(1)} collective-permute-done((bf16[512,512]{1,0:T(8,128)(2,1)S(1)}, bf16[512,512]{1,0:T(8,128)(2,1)S(1)}, u32[]{:S(2)}, u32[]{:S(2)}) %collective-permute-start.25) | collective-permute-done | bytes 524320 | tf_op jit(solution)/shard_map/ppermute | solution.py:40
  78.3 8.2 %collective-permute-done.26.refs_2_ = bf16[512,512]{1,0:T(8,128)(2,1)S(1)} collective-permute-done((bf16[512,512]{1,0:T(8,128)(2,1)S(1)}, bf16[512,512]{1,0:T(8,128)(2,1)S(1)}, u32[]{:S(2)}, u32[]{:S(2)}) %collective-permute-start.26) | collective-permute-done | bytes 524320 | tf_op jit(solution)/shard_map/ppermute | solution.py:40
  86.5 0.5 shard_map.204
  87.0 0.5 shard_map.208
  87.5 1.3 %collective-permute-start.31 = (bf16[288,512]{1,0:T(8,128)(2,1)S(1)}, bf16[288,512]{1,0:T(8,128)(2,1)S(1)}, u32[]{:S(2)}, u32[]{:S(2)}) collective-permute-start(bf16[288,512]{1,0:T(8,128)(2,1)S(1)} %shard_map.208), channel_id=1, source_target_pairs={{0,2},{1,3},{2,0},{3,1},{4,5},{5,4},{6,7},{7,6},{8,10},{9,11},{10,... | collective-permute-start | bytes 884744 | tf_op jit(solution)/shard_map/ppermute | solution.py:40
  88.8 0.8 shard_map.206
  89.6 4.7 %collective-permute-done.31.refs_0_ = bf16[288,512]{1,0:T(8,128)(2,1)S(1)} collective-permute-done((bf16[288,512]{1,0:T(8,128)(2,1)S(1)}, bf16[288,512]{1,0:T(8,128)(2,1)S(1)}, u32[]{:S(2)}, u32[]{:S(2)}) %collective-permute-start.31) | collective-permute-done | bytes 294944 | tf_op jit(solution)/shard_map/ppermute | solution.py:40
  94.2 0.3 shard_map.209
  94.6 0.1 collective-permute-start.32
  94.7 1.3 %collective-permute-start.30 = (bf16[288,512]{1,0:T(8,128)(2,1)S(1)}, bf16[288,512]{1,0:T(8,128)(2,1)S(1)}, u32[]{:S(2)}, u32[]{:S(2)}) collective-permute-start(bf16[288,512]{1,0:T(8,128)(2,1)S(1)} %shard_map.204), channel_id=1, source_target_pairs={{0,2},{1,3},{2,0},{3,1},{4,5},{5,4},{6,7},{7,6},{8,10},{9,11},{10,... | collective-permute-start | bytes 884744 | tf_op jit(solution)/shard_map/ppermute | solution.py:40
  96.0 1.5 %collective-permute-start.27 = (bf16[304,512]{1,0:T(8,128)(2,1)S(1)}, bf16[304,512]{1,0:T(8,128)(2,1)S(1)}, u32[]{:S(2)}, u32[]{:S(2)}) collective-permute-start(bf16[304,512]{1,0:T(8,128)(2,1)S(1)} %shard_map.198.refs_0_), channel_id=1, source_target_pairs={{0,1},{1,0},{2,3},{3,2},{4,5},{5,4},{6,7},{7,6},{8,9},{9,8},{10,11... | collective-permute-start | bytes 933896 | tf_op jit(solution)/shard_map/ppermute | solution.py:40
  97.5 0.8 collective-permute-start.28
  98.3 1.2 %collective-permute-start.29 = (bf16[304,512]{1,0:T(8,128)(2,1)S(1)}, bf16[304,512]{1,0:T(8,128)(2,1)S(1)}, u32[]{:S(2)}, u32[]{:S(2)}) collective-permute-start(bf16[304,512]{1,0:T(8,128)(2,1)S(1)} %shard_map.198.refs_0_), channel_id=1, source_target_pairs={{0,3},{1,2},{2,1},{3,0},{4,7},{5,6},{6,5},{7,4},{8,11},{9,10},{10,... | collective-permute-start | bytes 933896 | tf_op jit(solution)/shard_map/ppermute | solution.py:40
  99.5 4.2 %collective-permute-done.30.refs_0_ = bf16[288,512]{1,0:T(8,128)(2,1)S(1)} collective-permute-done((bf16[288,512]{1,0:T(8,128)(2,1)S(1)}, bf16[288,512]{1,0:T(8,128)(2,1)S(1)}, u32[]{:S(2)}, u32[]{:S(2)}) %collective-permute-start.30) | collective-permute-done | bytes 294944 | tf_op jit(solution)/shard_map/ppermute | solution.py:40
  103.7 0.3 shard_map.207
  104.0 0.1 fusion.5
  104.2 0.6 collective-permute-start.35
  104.9 1.3 %collective-permute-start.34 = (bf16[96,512]{1,0:T(8,128)(2,1)S(1)}, bf16[96,512]{1,0:T(8,128)(2,1)S(1)}, u32[]{:S(2)}, u32[]{:S(2)}) collective-permute-start(bf16[96,512]{1,0:T(8,128)(2,1)S(1)} %get-tuple-element.60), channel_id=1, source_target_pairs={{0,16},{1,17},{2,18},{3,19},{4,20},{5,21},{6,22},{7,23},{8,24},{9,... | collective-permute-start | bytes 294920 | tf_op jit(solution)/shard_map/ppermute | solution.py:40
  106.2 2.8 %collective-permute-start.33 = (bf16[96,512]{1,0:T(8,128)(2,1)S(1)}, bf16[96,512]{1,0:T(8,128)(2,1)S(1)}, u32[]{:S(2)}, u32[]{:S(2)}) collective-permute-start(bf16[96,512]{1,0:T(8,128)(2,1)S(1)} %get-tuple-element.58), channel_id=1, source_target_pairs={{0,24},{1,25},{2,26},{3,27},{4,28},{5,29},{6,30},{7,31},{8,0},{9,1... | collective-permute-start | bytes 294920 | tf_op jit(solution)/shard_map/ppermute | solution.py:40
  109.1 4.5 %collective-permute-done.28.refs_2_ = bf16[304,512]{1,0:T(8,128)(2,1)S(1)} collective-permute-done((bf16[304,512]{1,0:T(8,128)(2,1)S(1)}, bf16[304,512]{1,0:T(8,128)(2,1)S(1)}, u32[]{:S(2)}, u32[]{:S(2)}) %collective-permute-start.28) | collective-permute-done | bytes 311328 | tf_op jit(solution)/shard_map/ppermute | solution.py:40
  113.6 0.9 shard_map.205
  114.5 0.7 copy.21
  115.2 0.7 fusion.4
  (58 shorter events, 0.3 us)
Async XLA Ops:
  0.6 1.0 copy-start.7
  1.6 0.9 copy-start.9
  2.5 0.9 copy-start.10
  3.4 0.9 copy-start.11
  4.3 0.7 copy-start.12
  5.0 0.7 copy-start.14
  8.9 10.0 %collective-permute-start.16 = (bf16[136,256]{1,0:T(8,128)(2,1)S(1)}, bf16[136,256]{1,0:T(8,128)(2,1)S(1)}, u32[]{:S(2)}, u32[]{:S(2)}) collective-permute-start(bf16[136,256]{1,0:T(8,128)(2,1)S(1)} %get-tuple-element.43), channel_id=1, source_target_pairs={{0,8},{1,9},{2,10},{3,11},{4,12},{5,13},{6,14},{7,15},{8,16},{9,17... | collective-permute-start | bytes 208904 | tf_op jit(solution)/shard_map/ppermute | solution.py:40
  13.3 10.1 %collective-permute-start = (bf16[104,1024]{1,0:T(8,128)(2,1)S(1)}, bf16[104,1024]{1,0:T(8,128)(2,1)S(1)}, u32[]{:S(2)}, u32[]{:S(2)}) collective-permute-start(bf16[104,1024]{1,0:T(8,128)(2,1)S(1)} %get-tuple-element.30.refs_1_), channel_id=1, source_target_pairs={{0,8},{1,9},{2,10},{3,11},{4,12},{5,13},{6,14},{7,15},{8,16},{9,17... | collective-permute-start | bytes 638984 | tf_op jit(solution)/shard_map/ppermute | solution.py:40
  15.0 18.2 %collective-permute-start.6 = (bf16[96,2048]{1,0:T(8,128)(2,1)S(1)}, bf16[96,2048]{1,0:T(8,128)(2,1)S(1)}, u32[]{:S(2)}, u32[]{:S(2)}) collective-permute-start(bf16[96,2048]{1,0:T(8,128)(2,1)S(1)} %get-tuple-element.29.refs_0_.normed_ref), channel_id=1, source_target_pairs={{0,4},{1,5},{2,6},{3,7},{4,0},{5,1},{6,2},{7,3},{8,12},{9,13},{10,... | collective-permute-start | bytes 1179656 | tf_op jit(solution)/shard_map/ppermute | solution.py:40
  15.0 16.1 %collective-permute-start.2 = (bf16[104,1024]{1,0:T(8,128)(2,1)S(1)}, bf16[104,1024]{1,0:T(8,128)(2,1)S(1)}, u32[]{:S(2)}, u32[]{:S(2)}) collective-permute-start(bf16[104,1024]{1,0:T(8,128)(2,1)S(1)} %get-tuple-element.30.refs_1_), channel_id=1, source_target_pairs={{0,16},{1,17},{2,18},{3,19},{4,20},{5,21},{6,22},{7,23},{8,24},{9,... | collective-permute-start | bytes 638984 | tf_op jit(solution)/shard_map/ppermute | solution.py:40
  16.2 16.4 %collective-permute-start.4 = (bf16[104,1024]{1,0:T(8,128)(2,1)S(1)}, bf16[104,1024]{1,0:T(8,128)(2,1)S(1)}, u32[]{:S(2)}, u32[]{:S(2)}) collective-permute-start(bf16[104,1024]{1,0:T(8,128)(2,1)S(1)} %get-tuple-element.30.refs_1_), channel_id=1, source_target_pairs={{0,24},{1,25},{2,26},{3,27},{4,28},{5,29},{6,30},{7,31},{8,0},{9,1... | collective-permute-start | bytes 638984 | tf_op jit(solution)/shard_map/ppermute | solution.py:40
  18.9 14.2 %collective-permute-start.7 = (bf16[104,1024]{1,0:T(8,128)(2,1)S(1)}, bf16[104,1024]{1,0:T(8,128)(2,1)S(1)}, u32[]{:S(2)}, u32[]{:S(2)}) collective-permute-start(bf16[104,1024]{1,0:T(8,128)(2,1)S(1)} %get-tuple-element.30.refs_1_), channel_id=1, source_target_pairs={{0,4},{1,5},{2,6},{3,7},{4,0},{5,1},{6,2},{7,3},{8,12},{9,13},{10,... | collective-permute-start | bytes 638984 | tf_op jit(solution)/shard_map/ppermute | solution.py:40
  23.4 10.2 %collective-permute-start.1 = (bf16[104,1024]{1,0:T(8,128)(2,1)S(1)}, bf16[104,1024]{1,0:T(8,128)(2,1)S(1)}, u32[]{:S(2)}, u32[]{:S(2)}) collective-permute-start(bf16[104,1024]{1,0:T(8,128)(2,1)S(1)} %collective-permute-done.refs_2_), channel_id=1, source_target_pairs={{0,1},{1,0},{2,3},{3,2},{4,6},{5,7},{6,4},{7,5},{8,9},{9,8},{10,11... | collective-permute-start | bytes 638984 | tf_op jit(solution)/shard_map/ppermute | solution.py:40
  31.1 5.8 %collective-permute-start.3 = (bf16[104,1024]{1,0:T(8,128)(2,1)S(1)}, bf16[104,1024]{1,0:T(8,128)(2,1)S(1)}, u32[]{:S(2)}, u32[]{:S(2)}) collective-permute-start(bf16[104,1024]{1,0:T(8,128)(2,1)S(1)} %collective-permute-done.2.refs_4_), channel_id=1, source_target_pairs={{0,1},{1,0},{2,3},{3,2},{4,6},{5,7},{6,4},{7,5},{8,9},{9,8},{10,11... | collective-permute-start | bytes 638984 | tf_op jit(solution)/shard_map/ppermute | solution.py:40
  32.6 6.6 %collective-permute-start.5 = (bf16[104,1024]{1,0:T(8,128)(2,1)S(1)}, bf16[104,1024]{1,0:T(8,128)(2,1)S(1)}, u32[]{:S(2)}, u32[]{:S(2)}) collective-permute-start(bf16[104,1024]{1,0:T(8,128)(2,1)S(1)} %collective-permute-done.4.refs_6_), channel_id=1, source_target_pairs={{0,1},{1,0},{2,3},{3,2},{4,6},{5,7},{6,4},{7,5},{8,9},{9,8},{10,11... | collective-permute-start | bytes 638984 | tf_op jit(solution)/shard_map/ppermute | solution.py:40
  33.1 6.1 %collective-permute-start.8 = (bf16[104,1024]{1,0:T(8,128)(2,1)S(1)}, bf16[104,1024]{1,0:T(8,128)(2,1)S(1)}, u32[]{:S(2)}, u32[]{:S(2)}) collective-permute-start(bf16[104,1024]{1,0:T(8,128)(2,1)S(1)} %collective-permute-done.refs_2_), channel_id=1, source_target_pairs={{0,4},{1,5},{2,6},{3,7},{4,0},{5,1},{6,2},{7,3},{8,12},{9,13},{10,... | collective-permute-start | bytes 638984 | tf_op jit(solution)/shard_map/ppermute | solution.py:40
  33.1 7.8 %collective-permute-start.10 = (bf16[104,1024]{1,0:T(8,128)(2,1)S(1)}, bf16[104,1024]{1,0:T(8,128)(2,1)S(1)}, u32[]{:S(2)}, u32[]{:S(2)}) collective-permute-start(bf16[104,1024]{1,0:T(8,128)(2,1)S(1)} %collective-permute-done.2.refs_4_), channel_id=1, source_target_pairs={{0,4},{1,5},{2,6},{3,7},{4,0},{5,1},{6,2},{7,3},{8,12},{9,13},{10,... | collective-permute-start | bytes 638984 | tf_op jit(solution)/shard_map/ppermute | solution.py:40
  33.7 9.9 %collective-permute-start.12 = (bf16[104,1024]{1,0:T(8,128)(2,1)S(1)}, bf16[104,1024]{1,0:T(8,128)(2,1)S(1)}, u32[]{:S(2)}, u32[]{:S(2)}) collective-permute-start(bf16[104,1024]{1,0:T(8,128)(2,1)S(1)} %collective-permute-done.4.refs_6_), channel_id=1, source_target_pairs={{0,4},{1,5},{2,6},{3,7},{4,0},{5,1},{6,2},{7,3},{8,12},{9,13},{10,... | collective-permute-start | bytes 638984 | tf_op jit(solution)/shard_map/ppermute | solution.py:40
  37.0 6.7 %collective-permute-start.9 = (bf16[104,1024]{1,0:T(8,128)(2,1)S(1)}, bf16[104,1024]{1,0:T(8,128)(2,1)S(1)}, u32[]{:S(2)}, u32[]{:S(2)}) collective-permute-start(bf16[104,1024]{1,0:T(8,128)(2,1)S(1)} %collective-permute-done.1.refs_3_), channel_id=1, source_target_pairs={{0,4},{1,5},{2,6},{3,7},{4,0},{5,1},{6,2},{7,3},{8,12},{9,13},{10,... | collective-permute-start | bytes 638984 | tf_op jit(solution)/shard_map/ppermute | solution.py:40
  39.2 9.0 %collective-permute-start.11 = (bf16[104,1024]{1,0:T(8,128)(2,1)S(1)}, bf16[104,1024]{1,0:T(8,128)(2,1)S(1)}, u32[]{:S(2)}, u32[]{:S(2)}) collective-permute-start(bf16[104,1024]{1,0:T(8,128)(2,1)S(1)} %collective-permute-done.3.refs_5_), channel_id=1, source_target_pairs={{0,4},{1,5},{2,6},{3,7},{4,0},{5,1},{6,2},{7,3},{8,12},{9,13},{10,... | collective-permute-start | bytes 638984 | tf_op jit(solution)/shard_map/ppermute | solution.py:40
  39.2 10.8 %collective-permute-start.13 = (bf16[104,1024]{1,0:T(8,128)(2,1)S(1)}, bf16[104,1024]{1,0:T(8,128)(2,1)S(1)}, u32[]{:S(2)}, u32[]{:S(2)}) collective-permute-start(bf16[104,1024]{1,0:T(8,128)(2,1)S(1)} %collective-permute-done.5.refs_7_), channel_id=1, source_target_pairs={{0,4},{1,5},{2,6},{3,7},{4,0},{5,1},{6,2},{7,3},{8,12},{9,13},{10,... | collective-permute-start | bytes 638984 | tf_op jit(solution)/shard_map/ppermute | solution.py:40
  39.8 10.4 %copy-start.1 = (bf16[1,2048,1024]{2,1,0:T(8,128)(2,1)S(1)}, bf16[1,2048,1024]{2,1,0:T(8,128)(2,1)}, u32[]{:S(2)}) copy-start(bf16[1,2048,1024]{2,1,0:T(8,128)(2,1)} %param.32) | copy-start | bytes 12582916
  39.8 10.4 %copy-start.2 = (bf16[1,2048,1024]{2,1,0:T(8,128)(2,1)S(1)}, bf16[1,2048,1024]{2,1,0:T(8,128)(2,1)}, u32[]{:S(2)}) copy-start(bf16[1,2048,1024]{2,1,0:T(8,128)(2,1)} %param.33) | copy-start | bytes 12582916
  41.0 23.3 %collective-permute-start.22 = (bf16[512,512]{1,0:T(8,128)(2,1)S(1)}, bf16[512,512]{1,0:T(8,128)(2,1)S(1)}, u32[]{:S(2)}, u32[]{:S(2)}) collective-permute-start(bf16[512,512]{1,0:T(8,128)(2,1)S(1)} %shard_map.199), channel_id=1, source_target_pairs={{0,2},{1,3},{2,0},{3,1},{4,5},{5,4},{6,7},{7,6},{8,10},{9,11},{10,... | collective-permute-start | bytes 1572872 | tf_op jit(solution)/shard_map/ppermute | solution.py:40
  43.6 9.7 %collective-permute-start.15 = (bf16[136,256]{1,0:T(8,128)(2,1)S(1)}, bf16[136,256]{1,0:T(8,128)(2,1)S(1)}, u32[]{:S(2)}, u32[]{:S(2)}) collective-permute-start(bf16[136,256]{1,0:T(8,128)(2,1)S(1)} %get-tuple-element.43), channel_id=1, source_target_pairs={{0,4},{1,5},{2,6},{3,7},{4,0},{5,1},{6,2},{7,3},{8,12},{9,13},{10,... | collective-permute-start | bytes 208904 | tf_op jit(solution)/shard_map/ppermute | solution.py:40
  43.7 11.0 %collective-permute-start.18 = (bf16[136,256]{1,0:T(8,128)(2,1)S(1)}, bf16[136,256]{1,0:T(8,128)(2,1)S(1)}, u32[]{:S(2)}, u32[]{:S(2)}) collective-permute-start(bf16[136,256]{1,0:T(8,128)(2,1)S(1)} %get-tuple-element.43), channel_id=1, source_target_pairs={{0,16},{1,17},{2,18},{3,19},{4,20},{5,21},{6,22},{7,23},{8,24},{9,... | collective-permute-start | bytes 208904 | tf_op jit(solution)/shard_map/ppermute | solution.py:40
  48.2 6.8 %collective-permute-start.20 = (bf16[136,256]{1,0:T(8,128)(2,1)S(1)}, bf16[136,256]{1,0:T(8,128)(2,1)S(1)}, u32[]{:S(2)}, u32[]{:S(2)}) collective-permute-start(bf16[136,256]{1,0:T(8,128)(2,1)S(1)} %get-tuple-element.43), channel_id=1, source_target_pairs={{0,24},{1,25},{2,26},{3,27},{4,28},{5,29},{6,30},{7,31},{8,0},{9,1... | collective-permute-start | bytes 208904 | tf_op jit(solution)/shard_map/ppermute | solution.py:40
  50.0 5.1 %collective-permute-start.17 = (bf16[136,256]{1,0:T(8,128)(2,1)S(1)}, bf16[136,256]{1,0:T(8,128)(2,1)S(1)}, u32[]{:S(2)}, u32[]{:S(2)}) collective-permute-start(bf16[136,256]{1,0:T(8,128)(2,1)S(1)} %collective-permute-done.16.refs_1_), channel_id=1, source_target_pairs={{0,4},{1,5},{2,6},{3,7},{4,0},{5,1},{6,2},{7,3},{8,12},{9,13},{10,... | collective-permute-start | bytes 208904 | tf_op jit(solution)/shard_map/ppermute | solution.py:40
  53.4 13.7 %collective-permute-start.23 = (bf16[512,512]{1,0:T(8,128)(2,1)S(1)}, bf16[512,512]{1,0:T(8,128)(2,1)S(1)}, u32[]{:S(2)}, u32[]{:S(2)}) collective-permute-start(bf16[512,512]{1,0:T(8,128)(2,1)S(1)} %shard_map.200), channel_id=1, source_target_pairs={{0,2},{1,3},{2,0},{3,1},{4,5},{5,4},{6,7},{7,6},{8,10},{9,11},{10,... | collective-permute-start | bytes 1572872 | tf_op jit(solution)/shard_map/ppermute | solution.py:40
  54.7 5.4 %collective-permute-start.19 = (bf16[136,256]{1,0:T(8,128)(2,1)S(1)}, bf16[136,256]{1,0:T(8,128)(2,1)S(1)}, u32[]{:S(2)}, u32[]{:S(2)}) collective-permute-start(bf16[136,256]{1,0:T(8,128)(2,1)S(1)} %collective-permute-done.18.refs_3_), channel_id=1, source_target_pairs={{0,4},{1,5},{2,6},{3,7},{4,0},{5,1},{6,2},{7,3},{8,12},{9,13},{10,... | collective-permute-start | bytes 208904 | tf_op jit(solution)/shard_map/ppermute | solution.py:40
  55.0 8.1 %collective-permute-start.21 = (bf16[136,256]{1,0:T(8,128)(2,1)S(1)}, bf16[136,256]{1,0:T(8,128)(2,1)S(1)}, u32[]{:S(2)}, u32[]{:S(2)}) collective-permute-start(bf16[136,256]{1,0:T(8,128)(2,1)S(1)} %collective-permute-done.20.refs_5_), channel_id=1, source_target_pairs={{0,4},{1,5},{2,6},{3,7},{4,0},{5,1},{6,2},{7,3},{8,12},{9,13},{10,... | collective-permute-start | bytes 208904 | tf_op jit(solution)/shard_map/ppermute | solution.py:40
  55.2 31.3 %collective-permute-start.24 = (bf16[288,1024]{1,0:T(8,128)(2,1)S(1)}, bf16[288,1024]{1,0:T(8,128)(2,1)S(1)}, u32[]{:S(2)}, u32[]{:S(2)}) collective-permute-start(bf16[288,1024]{1,0:T(8,128)(2,1)S(1)} %get-tuple-element.31.refs_0_), channel_id=1, source_target_pairs={{0,1},{1,0},{2,3},{3,2},{4,6},{5,7},{6,4},{7,5},{8,9},{9,8},{10,11... | collective-permute-start | bytes 1769480 | tf_op jit(solution)/shard_map/ppermute | solution.py:40
  60.1 5.1 %copy-start.4 = (bf16[2048,256]{1,0:T(8,128)(2,1)S(1)}, bf16[2048,256]{1,0:T(8,128)(2,1)}, u32[]{:S(2)}) copy-start(bf16[2048,256]{1,0:T(8,128)(2,1)} %sg_ref.1) | copy-start | bytes 3145732
  60.1 5.1 %copy-start.5 = (bf16[2048,256]{1,0:T(8,128)(2,1)S(1)}, bf16[2048,256]{1,0:T(8,128)(2,1)}, u32[]{:S(2)}) copy-start(bf16[2048,256]{1,0:T(8,128)(2,1)} %su_ref.1) | copy-start | bytes 3145732
  60.1 5.1 %copy-start.8 = (bf16[256,512]{1,0:T(8,128)(2,1)S(1)}, bf16[256,512]{1,0:T(8,128)(2,1)}, u32[]{:S(2)}) copy-start(bf16[256,512]{1,0:T(8,128)(2,1)} %gate_ref.1) | copy-start | bytes 786436
  60.1 5.1 %copy-start.13 = (f32[512]{0:T(512)S(1)}, f32[512]{0:T(512)}, u32[]{:S(2)}) copy-start(f32[512]{0:T(512)} %param.26) | copy-start | bytes 6148
  60.1 26.9 %collective-permute-start.14 = (bf16[288,1024]{1,0:T(8,128)(2,1)S(1)}, bf16[288,1024]{1,0:T(8,128)(2,1)S(1)}, u32[]{:S(2)}, u32[]{:S(2)}) collective-permute-start(bf16[288,1024]{1,0:T(8,128)(2,1)S(1)} %get-tuple-element.40.refs_1_), channel_id=1, source_target_pairs={{0,1},{1,0},{2,3},{3,2},{4,6},{5,7},{6,4},{7,5},{8,9},{9,8},{10,11... | collective-permute-start | bytes 1769480 | tf_op jit(solution)/shard_map/ppermute | solution.py:40
  61.8 5.2 %copy-start = (bf16[1,4096,512]{2,1,0:T(8,128)(2,1)S(1)}, bf16[1,4096,512]{2,1,0:T(8,128)(2,1)}, u32[]{:S(2)}) copy-start(bf16[1,4096,512]{2,1,0:T(8,128)(2,1)} %param.34) | copy-start | bytes 12582916
  63.1 15.2 %collective-permute-start.25 = (bf16[512,512]{1,0:T(8,128)(2,1)S(1)}, bf16[512,512]{1,0:T(8,128)(2,1)S(1)}, u32[]{:S(2)}, u32[]{:S(2)}) collective-permute-start(bf16[512,512]{1,0:T(8,128)(2,1)S(1)} %shard_map.202), channel_id=1, source_target_pairs={{0,2},{1,3},{2,0},{3,1},{4,5},{5,4},{6,7},{7,6},{8,10},{9,11},{10,... | collective-permute-start | bytes 1572872 | tf_op jit(solution)/shard_map/ppermute | solution.py:40
  64.2 22.3 %collective-permute-start.26 = (bf16[512,512]{1,0:T(8,128)(2,1)S(1)}, bf16[512,512]{1,0:T(8,128)(2,1)S(1)}, u32[]{:S(2)}, u32[]{:S(2)}) collective-permute-start(bf16[512,512]{1,0:T(8,128)(2,1)S(1)} %shard_map.203), channel_id=1, source_target_pairs={{0,2},{1,3},{2,0},{3,1},{4,5},{5,4},{6,7},{7,6},{8,10},{9,11},{10,... | collective-permute-start | bytes 1572872 | tf_op jit(solution)/shard_map/ppermute | solution.py:40
  87.5 6.8 %collective-permute-start.31 = (bf16[288,512]{1,0:T(8,128)(2,1)S(1)}, bf16[288,512]{1,0:T(8,128)(2,1)S(1)}, u32[]{:S(2)}, u32[]{:S(2)}) collective-permute-start(bf16[288,512]{1,0:T(8,128)(2,1)S(1)} %shard_map.208), channel_id=1, source_target_pairs={{0,2},{1,3},{2,0},{3,1},{4,5},{5,4},{6,7},{7,6},{8,10},{9,11},{10,... | collective-permute-start | bytes 884744 | tf_op jit(solution)/shard_map/ppermute | solution.py:40
  89.6 24.0 %copy-start.3 = (bf16[2048,512]{1,0:T(8,128)(2,1)S(1)}, bf16[2048,512]{1,0:T(8,128)(2,1)}, u32[]{:S(2)}) copy-start(bf16[2048,512]{1,0:T(8,128)(2,1)} %refs_4_.1) | copy-start | bytes 6291460
  89.6 24.0 %copy-start.6 = (bf16[1024,512]{1,0:T(8,128)(2,1)S(1)}, bf16[1024,512]{1,0:T(8,128)(2,1)}, u32[]{:S(2)}) copy-start(bf16[1024,512]{1,0:T(8,128)(2,1)} %refs_5_.1) | copy-start | bytes 3145732
  94.6 9.4 %collective-permute-start.32 = (bf16[4,96,512]{2,1,0:T(8,128)(2,1)S(1)}, bf16[4,96,512]{2,1,0:T(8,128)(2,1)S(1)}, u32[]{:S(2)}, u32[]{:S(2)}) collective-permute-start(bf16[4,96,512]{2,1,0:T(8,128)(2,1)S(1)} %shard_map.209), channel_id=1, source_target_pairs={{0,4},{1,5},{2,6},{3,7},{4,0},{5,1},{6,2},{7,3},{8,12},{9,13},{10,... | collective-permute-start | bytes 1179656 | tf_op jit(solution)/shard_map/ppermute | solution.py:40
  94.7 9.0 %collective-permute-start.30 = (bf16[288,512]{1,0:T(8,128)(2,1)S(1)}, bf16[288,512]{1,0:T(8,128)(2,1)S(1)}, u32[]{:S(2)}, u32[]{:S(2)}) collective-permute-start(bf16[288,512]{1,0:T(8,128)(2,1)S(1)} %shard_map.204), channel_id=1, source_target_pairs={{0,2},{1,3},{2,0},{3,1},{4,5},{5,4},{6,7},{7,6},{8,10},{9,11},{10,... | collective-permute-start | bytes 884744 | tf_op jit(solution)/shard_map/ppermute | solution.py:40
  96.0 10.2 %collective-permute-start.27 = (bf16[304,512]{1,0:T(8,128)(2,1)S(1)}, bf16[304,512]{1,0:T(8,128)(2,1)S(1)}, u32[]{:S(2)}, u32[]{:S(2)}) collective-permute-start(bf16[304,512]{1,0:T(8,128)(2,1)S(1)} %shard_map.198.refs_0_), channel_id=1, source_target_pairs={{0,1},{1,0},{2,3},{3,2},{4,5},{5,4},{6,7},{7,6},{8,9},{9,8},{10,11... | collective-permute-start | bytes 933896 | tf_op jit(solution)/shard_map/ppermute | solution.py:40
  97.5 16.1 %collective-permute-start.28 = (bf16[304,512]{1,0:T(8,128)(2,1)S(1)}, bf16[304,512]{1,0:T(8,128)(2,1)S(1)}, u32[]{:S(2)}, u32[]{:S(2)}) collective-permute-start(bf16[304,512]{1,0:T(8,128)(2,1)S(1)} %shard_map.198.refs_0_), channel_id=1, source_target_pairs={{0,2},{1,3},{2,0},{3,1},{4,6},{5,7},{6,4},{7,5},{8,10},{9,11},{10,... | collective-permute-start | bytes 933896 | tf_op jit(solution)/shard_map/ppermute | solution.py:40
  98.3 15.3 %collective-permute-start.29 = (bf16[304,512]{1,0:T(8,128)(2,1)S(1)}, bf16[304,512]{1,0:T(8,128)(2,1)S(1)}, u32[]{:S(2)}, u32[]{:S(2)}) collective-permute-start(bf16[304,512]{1,0:T(8,128)(2,1)S(1)} %shard_map.198.refs_0_), channel_id=1, source_target_pairs={{0,3},{1,2},{2,1},{3,0},{4,7},{5,6},{6,5},{7,4},{8,11},{9,10},{10,... | collective-permute-start | bytes 933896 | tf_op jit(solution)/shard_map/ppermute | solution.py:40
  104.2 11.0 %collective-permute-start.35 = (bf16[96,512]{1,0:T(8,128)(2,1)S(1)}, bf16[96,512]{1,0:T(8,128)(2,1)S(1)}, u32[]{:S(2)}, u32[]{:S(2)}) collective-permute-start(bf16[96,512]{1,0:T(8,128)(2,1)S(1)} %get-tuple-element.59), channel_id=1, source_target_pairs={{0,8},{1,9},{2,10},{3,11},{4,12},{5,13},{6,14},{7,15},{8,16},{9,17... | collective-permute-start | bytes 294920 | tf_op jit(solution)/shard_map/ppermute | solution.py:40
  104.9 10.3 %collective-permute-start.34 = (bf16[96,512]{1,0:T(8,128)(2,1)S(1)}, bf16[96,512]{1,0:T(8,128)(2,1)S(1)}, u32[]{:S(2)}, u32[]{:S(2)}) collective-permute-start(bf16[96,512]{1,0:T(8,128)(2,1)S(1)} %get-tuple-element.60), channel_id=1, source_target_pairs={{0,16},{1,17},{2,18},{3,19},{4,20},{5,21},{6,22},{7,23},{8,24},{9,... | collective-permute-start | bytes 294920 | tf_op jit(solution)/shard_map/ppermute | solution.py:40
  106.2 9.0 %collective-permute-start.33 = (bf16[96,512]{1,0:T(8,128)(2,1)S(1)}, bf16[96,512]{1,0:T(8,128)(2,1)S(1)}, u32[]{:S(2)}, u32[]{:S(2)}) collective-permute-start(bf16[96,512]{1,0:T(8,128)(2,1)S(1)} %get-tuple-element.58), channel_id=1, source_target_pairs={{0,24},{1,25},{2,26},{3,27},{4,28},{5,29},{6,30},{7,31},{8,0},{9,1... | collective-permute-start | bytes 294920 | tf_op jit(solution)/shard_map/ppermute | solution.py:40

commit v4 on v3

--- a/solution.py
+++ b/solution.py
@@ -385,19 +385,26 @@
     return call(body, outs, operands, 4 * slots * width * hidden, scratch=scratch)
 
 
-def take_piece(places, weight, du, dv, piece, hidden):
+def take_pieces(places, weight, wanted, hidden):
     size = hidden // PIECES
 
-    def body(in_ref, out_ref, done):
-        start = Here(places).column(du, dv) * hidden + piece * size
-        copy = pltpu.make_async_copy(
-            in_ref.at[pl.ds(pl.multiple_of(start, size), size), :], out_ref, done
-        )
-        copy.start()
-        copy.wait()
-
-    out = jax.ShapeDtypeStruct((size, weight.shape[1]), weight.dtype)
-    return call(body, out, (weight,), 1 << 20, scratch=(pltpu.SemaphoreType.DMA,), far=1)
+    def body(in_ref, *refs):
+        outs, done = refs[:-1], refs[-1]
+        here = Here(places)
+        copies = []
+        for i, (du, dv, piece) in enumerate(wanted):
+            start = pl.multiple_of(here.column(du, dv) * hidden + piece * size, size)
+            copies.append(
+                pltpu.make_async_copy(in_ref.at[pl.ds(start, size), :], outs[i], done.at[i])
+            )
+        for copy in copies:
+            copy.start()
+        for copy in copies:
+            copy.wait()
+
+    outs = [jax.ShapeDtypeStruct((size, weight.shape[1]), weight.dtype) for _ in wanted]
+    scratch = (pltpu.SemaphoreType.DMA((len(wanted),)),)
+    return call(body, outs, (weight,), 1 << 20, scratch=scratch, far=1)
 
 
 def dot_pieces(ref, pieces):
@@ -527,13 +534,14 @@
 
     traded = [[[] for _ in range(n)] for _ in range(1, n)]
     lacking = [(i, piece) for i in range(n) for piece in range(PIECES)]
-
-    def trade(quarter):
-        share = len(lacking) // 4
-        for i, piece in lacking[quarter * share : (quarter + 1) * share]:
-            for k in range(1, n):
-                taken = take_piece(at, down_weight, -i, k, piece, hidden)
-                traded[k - 1][i].append(at.along_v(taken, k))
+    wanted = [(i, k, piece) for i, piece in lacking for k in range(1, n)]
+    taken = take_pieces(at, down_weight, [(-i, k, p) for i, k, p in wanted], hidden)
+    quarter = len(wanted) // 4
+
+    def trade(number):
+        for at_piece in range(number * quarter, (number + 1) * quarter):
+            i, k, _ = wanted[at_piece]
+            traded[k - 1][i].append(at.along_v(taken[at_piece], k))
 
     normed, packed = prepare_rows(
         at,
@@ -547,8 +555,8 @@
     middle = chips // 2
     far = {middle: at.along_z(packed, middle)}
     trade(0)
+    trade(1)
     far |= {k: at.along_z(packed, k) for k in range(1, chips) if k != middle}
-    trade(1)
     trade(2)
     o_local, q_device, own_state = local_attention(
         first_batch_queries,
@@ -595,7 +603,7 @@
 
     partial = partials(0, gathered_first)
     back = [[at.along_v(partial[k - 1], -k) for k in range(1, n)]]
-    gathered_second, both, _ = hold((gathered_second, both, partial))
+    gathered_second, _ = hold((gathered_second, partial))
     partial = partials(1, gathered_second)
     back.append([at.along_v(partial[k - 1], -k) for k in range(1, n)])
     gathered = [list(pair) for pair in zip(gathered_first, gathered_second)]

time: 117 us -> 118 us (level)
  waiting for transfers between devices: 48.7 us -> 56.9 us
  Pallas kernels: 21.3 us -> 18.2 us
  local copies, waits for them, and re-layouts: 5.8 us -> 2.99 us
    ppermute x36, waiting for transfers between devices: 48.7 us -> 56.9 us  [send(): return lax.ppermute(value, AXES, self.pairs(move))]
    pallas_call x16 -> x13, Pallas kernels: 21.3 us -> 18.2 us  [call(): pl.pallas_call(body, out_shape=jax.tree.map(lambda o: pltpu.VMEM(o.shape,...]
    unnamed x31 -> x33, local copies, waits for them, and re-layouts: 5.78 us -> 2.97 us
  transfers between devices with their start and end apart: 36 -> 36, of which waited for: 10 -> 16; matrix products, arithmetic and copies ran while one was open for 1% -> 1% of each run, Pallas kernels for 15% -> 13%
where the time goes in v4:
time: 118 us
  waiting for transfers between devices  56.9 us (48%)
  starting transfers between devices  37.8 us (32%)
  Pallas kernels  18.2 us (15%)
  local copies, waits for them, and re-layouts  2.99 us (3%)
    ppermute x36, waiting for transfers between devices, send(): return lax.ppermute(value, AXES, self.pairs(move))  56.9 us
    ppermute x36, starting transfers between devices, send(): return lax.ppermute(value, AXES, self.pairs(move))  37.8 us
    pallas_call x13, Pallas kernels, call(): pl.pallas_call(body, out_shape=jax.tree.map(lambda o: pltpu.VMEM(o.shape,...  18.2 us
    unnamed x33, local copies, waits for them, and re-layouts  2.97 us
  transfers between devices with their start and end apart: 36, of which 16 were waited for; matrix products, arithmetic and copies ran while one was open for 1% of the time, Pallas kernels for 13%

profile of v4, /device:TPU:0, one launch (start us, length us, event | category | flops | bytes accessed | tf_op | source)
XLA Modules:
  0.0 117.6 jit_solution(115037866915124005)
XLA Ops:
  0.6 1.5 %shard_map.195 = (bf16[96,2048]{1,0:T(8,128)(2,1)S(1)}, bf16[104,1024]{1,0:T(8,128)(2,1)S(1)}) custom-call(bf16[96,2048]{1,0:T(8,128)(2,1)} %rows_hbm.1, f32[1,2048]{1,0:T(1,128)} %bitcast.35, s32[4,96]{1,0:T(4,128)} %bitcast.36, f32[4,96]{1,0:T(4,128)} %bitcast.37), custom_call_target="tpu_custom_call" | custom-call | flops 4194304 | tf_op jit(solution)/shard_map/pallas_call | solution.py:107
  2.2 0.6 collective-permute-start.16
  2.7 2.6 %collective-permute-start.10 = (bf16[104,1024]{1,0:T(8,128)(2,1)S(1)}, bf16[104,1024]{1,0:T(8,128)(2,1)S(1)}, u32[]{:S(2)}, u32[]{:S(2)}) collective-permute-start(bf16[104,1024]{1,0:T(8,128)(2,1)S(1)} %get-tuple-element.37.refs_1_), channel_id=1, source_target_pairs={{0,8},{1,9},{2,10},{3,11},{4,12},{5,13},{6,14},{7,15},{8,16},{9,17... | collective-permute-start | bytes 638984 | tf_op jit(solution)/shard_map/ppermute | solution.py:40
  5.4 2.6 %collective-permute-start.12 = (bf16[104,1024]{1,0:T(8,128)(2,1)S(1)}, bf16[104,1024]{1,0:T(8,128)(2,1)S(1)}, u32[]{:S(2)}, u32[]{:S(2)}) collective-permute-start(bf16[104,1024]{1,0:T(8,128)(2,1)S(1)} %get-tuple-element.37.refs_1_), channel_id=1, source_target_pairs={{0,16},{1,17},{2,18},{3,19},{4,20},{5,21},{6,22},{7,23},{8,24},{9,... | collective-permute-start | bytes 638984 | tf_op jit(solution)/shard_map/ppermute | solution.py:40
  7.9 1.3 %collective-permute-start.14 = (bf16[104,1024]{1,0:T(8,128)(2,1)S(1)}, bf16[104,1024]{1,0:T(8,128)(2,1)S(1)}, u32[]{:S(2)}, u32[]{:S(2)}) collective-permute-start(bf16[104,1024]{1,0:T(8,128)(2,1)S(1)} %get-tuple-element.37.refs_1_), channel_id=1, source_target_pairs={{0,24},{1,25},{2,26},{3,27},{4,28},{5,29},{6,30},{7,31},{8,0},{9,1... | collective-permute-start | bytes 638984 | tf_op jit(solution)/shard_map/ppermute | solution.py:40
  9.3 4.3 %collective-permute-done.10.refs_2_ = bf16[104,1024]{1,0:T(8,128)(2,1)S(1)} collective-permute-done((bf16[104,1024]{1,0:T(8,128)(2,1)S(1)}, bf16[104,1024]{1,0:T(8,128)(2,1)S(1)}, u32[]{:S(2)}, u32[]{:S(2)}) %collective-permute-start.10) | collective-permute-done | bytes 213024 | tf_op jit(solution)/shard_map/ppermute | solution.py:40
  13.6 1.7 %collective-permute-start.11 = (bf16[104,1024]{1,0:T(8,128)(2,1)S(1)}, bf16[104,1024]{1,0:T(8,128)(2,1)S(1)}, u32[]{:S(2)}, u32[]{:S(2)}) collective-permute-start(bf16[104,1024]{1,0:T(8,128)(2,1)S(1)} %collective-permute-done.10.refs_2_), channel_id=1, source_target_pairs={{0,1},{1,0},{2,3},{3,2},{4,6},{5,7},{6,4},{7,5},{8,9},{9,8},{10,11... | collective-permute-start | bytes 638984 | tf_op jit(solution)/shard_map/ppermute | solution.py:40
  15.3 7.1 %collective-permute-done.12.refs_4_ = bf16[104,1024]{1,0:T(8,128)(2,1)S(1)} collective-permute-done((bf16[104,1024]{1,0:T(8,128)(2,1)S(1)}, bf16[104,1024]{1,0:T(8,128)(2,1)S(1)}, u32[]{:S(2)}, u32[]{:S(2)}) %collective-permute-start.12) | collective-permute-done | bytes 213024 | tf_op jit(solution)/shard_map/ppermute | solution.py:40
  22.5 1.5 %collective-permute-start.13 = (bf16[104,1024]{1,0:T(8,128)(2,1)S(1)}, bf16[104,1024]{1,0:T(8,128)(2,1)S(1)}, u32[]{:S(2)}, u32[]{:S(2)}) collective-permute-start(bf16[104,1024]{1,0:T(8,128)(2,1)S(1)} %collective-permute-done.12.refs_4_), channel_id=1, source_target_pairs={{0,1},{1,0},{2,3},{3,2},{4,6},{5,7},{6,4},{7,5},{8,9},{9,8},{10,11... | collective-permute-start | bytes 638984 | tf_op jit(solution)/shard_map/ppermute | solution.py:40
  24.0 0.5 collective-permute-start.15
  24.5 0.5 collective-permute-start.20
  25.0 1.5 %shard_map.200 = (bf16[512,512]{1,0:T(8,128)(2,1)S(1)}, bf16[512,512]{1,0:T(8,128)(2,1)S(1)}, bf16[512,512]{1,0:T(8,128)(2,1)S(1)}, bf16[512,512]{1,0:T(8,128)(2,1)S(1)}) custom-call(bf16[4096,512]{1,0:T(8,128)(2,1)} %bitcast.26), custom_call_target="tpu_custom_call" | custom-call | flops 1048576 | tf_op jit(solution)/shard_map/pallas_call | solution.py:107
  26.6 1.6 %collective-permute-start.24 = (bf16[512,512]{1,0:T(8,128)(2,1)S(1)}, bf16[512,512]{1,0:T(8,128)(2,1)S(1)}, u32[]{:S(2)}, u32[]{:S(2)}) collective-permute-start(bf16[512,512]{1,0:T(8,128)(2,1)S(1)} %get-tuple-element.48), channel_id=1, source_target_pairs={{0,2},{1,3},{2,0},{3,1},{4,5},{5,4},{6,7},{7,6},{8,10},{9,11},{10,... | collective-permute-start | bytes 1572872 | tf_op jit(solution)/shard_map/ppermute | solution.py:40
  28.2 0.1 collective-permute-done.13.refs_5_
  28.3 3.6 %collective-permute-done.15.refs_7_ = bf16[104,1024]{1,0:T(8,128)(2,1)S(1)} collective-permute-done((bf16[104,1024]{1,0:T(8,128)(2,1)S(1)}, bf16[104,1024]{1,0:T(8,128)(2,1)S(1)}, u32[]{:S(2)}, u32[]{:S(2)}) %collective-permute-start.15) | collective-permute-done | bytes 213024 | tf_op jit(solution)/shard_map/ppermute | solution.py:40
  31.9 0.5 collective-permute-start.21
  32.4 0.1 collective-permute-start.23
  32.5 2.2 %copy-done.2 = bf16[1,2048,1024]{2,1,0:T(8,128)(2,1)S(1)} copy-done((bf16[1,2048,1024]{2,1,0:T(8,128)(2,1)S(1)}, bf16[1,2048,1024]{2,1,0:T(8,128)(2,1)}, u32[]{:S(2)}) %copy-start.2) | copy-done | bytes 4194328
  34.7 3.2 %shard_map.198 = (bf16[288,1024]{1,0:T(8,128)(2,1)S(1)}, f32[4,256]{1,0:T(4,128)S(1)}) custom-call(bf16[96,2048]{1,0:T(8,128)(2,1)S(1)} %get-tuple-element.34.normed_ref.refs_0_, bf16[104,1024]{1,0:T(8,128)(2,1)S(1)} %get-tuple-element.37.refs_1_, bf16[104,1024]{1,0:T(8,128)(2,1)S(1)} %collective-permute-done.10.refs_2_, ...), custom_call_target="tpu_custom_call" | custom-call | flops 2415919104 | tf_op jit(solution)/shard_map/pallas_call | solution.py:107
  37.8 1.6 %collective-permute-start.25 = (bf16[512,512]{1,0:T(8,128)(2,1)S(1)}, bf16[512,512]{1,0:T(8,128)(2,1)S(1)}, u32[]{:S(2)}, u32[]{:S(2)}) collective-permute-start(bf16[512,512]{1,0:T(8,128)(2,1)S(1)} %get-tuple-element.49), channel_id=1, source_target_pairs={{0,2},{1,3},{2,0},{3,1},{4,5},{5,4},{6,7},{7,6},{8,10},{9,11},{10,... | collective-permute-start | bytes 1572872 | tf_op jit(solution)/shard_map/ppermute | solution.py:40
  39.4 1.5 %collective-permute-start.26 = (bf16[288,1024]{1,0:T(8,128)(2,1)S(1)}, bf16[288,1024]{1,0:T(8,128)(2,1)S(1)}, u32[]{:S(2)}, u32[]{:S(2)}) collective-permute-start(bf16[288,1024]{1,0:T(8,128)(2,1)S(1)} %get-tuple-element.38.refs_0_), channel_id=1, source_target_pairs={{0,1},{1,0},{2,3},{3,2},{4,6},{5,7},{6,4},{7,5},{8,9},{9,8},{10,11... | collective-permute-start | bytes 1769480 | tf_op jit(solution)/shard_map/ppermute | solution.py:40
  40.9 3.1 %shard_map.199 = (bf16[288,1024]{1,0:T(8,128)(2,1)S(1)}, f32[4,256]{1,0:T(4,128)S(1)}) custom-call(bf16[96,2048]{1,0:T(8,128)(2,1)S(1)} %collective-permute-done.16.refs_0_, bf16[104,1024]{1,0:T(8,128)(2,1)S(1)} %collective-permute-done.17.refs_1_, bf16[104,1024]{1,0:T(8,128)(2,1)S(1)} %collective-permute-done.18.refs_2_, ...), custom_call_target="tpu_custom_call" | custom-call | flops 2415919104 | tf_op jit(solution)/shard_map/pallas_call | solution.py:107
  44.1 0.6 collective-permute-start.27
  44.7 0.5 collective-permute-start.28
  45.2 1.5 %collective-permute-start.29 = (bf16[512,512]{1,0:T(8,128)(2,1)S(1)}, bf16[512,512]{1,0:T(8,128)(2,1)S(1)}, u32[]{:S(2)}, u32[]{:S(2)}) collective-permute-start(bf16[512,512]{1,0:T(8,128)(2,1)S(1)} %get-tuple-element.54), channel_id=1, source_target_pairs={{0,2},{1,3},{2,0},{3,1},{4,5},{5,4},{6,7},{7,6},{8,10},{9,11},{10,... | collective-permute-start | bytes 1572872 | tf_op jit(solution)/shard_map/ppermute | solution.py:40
  46.7 5.3 %collective-permute-done.25.refs_4_ = bf16[512,512]{1,0:T(8,128)(2,1)S(1)} collective-permute-done((bf16[512,512]{1,0:T(8,128)(2,1)S(1)}, bf16[512,512]{1,0:T(8,128)(2,1)S(1)}, u32[]{:S(2)}, u32[]{:S(2)}) %collective-permute-start.25) | collective-permute-done | bytes 524320 | tf_op jit(solution)/shard_map/ppermute | solution.py:40
  52.0 1.4 %shard_map.201 = (f32[288,512]{1,0:T(8,128)S(1)}, f32[288,512]{1,0:T(8,128)S(1)}, f32[288,512]{1,0:T(8,128)S(1)}, f32[288,512]{1,0:T(8,128)S(1)}) custom-call(bf16[288,1024]{1,0:T(8,128)(2,1)S(1)} %get-tuple-element.38.refs_0_, bf16[288,1024]{1,0:T(8,128)(2,1)S(1)} %get-tuple-element.47.refs_1_, bf16[4096,512]{1,0:T(8,128)(2,1)S(1)} %bitcast.27, ...), custom_call_target="tpu_custom_call" | custom-call | flops 1207959552 | tf_op jit(solution)/shard_map/pallas_call | solution.py:107
  53.4 9.8 %collective-permute-done.28.refs_1_ = bf16[512,512]{1,0:T(8,128)(2,1)S(1)} collective-permute-done((bf16[512,512]{1,0:T(8,128)(2,1)S(1)}, bf16[512,512]{1,0:T(8,128)(2,1)S(1)}, u32[]{:S(2)}, u32[]{:S(2)}) %collective-permute-start.28) | collective-permute-done | bytes 524320 | tf_op jit(solution)/shard_map/ppermute | solution.py:40
  63.3 7.7 %collective-permute-done.29.refs_2_ = bf16[512,512]{1,0:T(8,128)(2,1)S(1)} collective-permute-done((bf16[512,512]{1,0:T(8,128)(2,1)S(1)}, bf16[512,512]{1,0:T(8,128)(2,1)S(1)}, u32[]{:S(2)}, u32[]{:S(2)}) %collective-permute-start.29) | collective-permute-done | bytes 524320 | tf_op jit(solution)/shard_map/ppermute | solution.py:40
  71.0 0.5 shard_map.202
  71.5 0.5 shard_map.205
  71.9 0.0 copy-start.8
  72.0 0.0 copy-start.12
  72.0 1.6 %collective-permute-start.31 = (bf16[288,512]{1,0:T(8,128)(2,1)S(1)}, bf16[288,512]{1,0:T(8,128)(2,1)S(1)}, u32[]{:S(2)}, u32[]{:S(2)}) collective-permute-start(bf16[288,512]{1,0:T(8,128)(2,1)S(1)} %shard_map.205), channel_id=1, source_target_pairs={{0,2},{1,3},{2,0},{3,1},{4,5},{5,4},{6,7},{7,6},{8,10},{9,11},{10,... | collective-permute-start | bytes 884744 | tf_op jit(solution)/shard_map/ppermute | solution.py:40
  73.6 0.8 shard_map.203
  74.4 4.4 %collective-permute-done.31.refs_0_ = bf16[288,512]{1,0:T(8,128)(2,1)S(1)} collective-permute-done((bf16[288,512]{1,0:T(8,128)(2,1)S(1)}, bf16[288,512]{1,0:T(8,128)(2,1)S(1)}, u32[]{:S(2)}, u32[]{:S(2)}) %collective-permute-start.31) | collective-permute-done | bytes 294944 | tf_op jit(solution)/shard_map/ppermute | solution.py:40
  78.8 0.3 shard_map.206
  79.2 0.1 collective-permute-start.32
  79.2 1.6 %collective-permute-start.30 = (bf16[288,512]{1,0:T(8,128)(2,1)S(1)}, bf16[288,512]{1,0:T(8,128)(2,1)S(1)}, u32[]{:S(2)}, u32[]{:S(2)}) collective-permute-start(bf16[288,512]{1,0:T(8,128)(2,1)S(1)} %shard_map.202), channel_id=1, source_target_pairs={{0,2},{1,3},{2,0},{3,1},{4,5},{5,4},{6,7},{7,6},{8,10},{9,11},{10,... | collective-permute-start | bytes 884744 | tf_op jit(solution)/shard_map/ppermute | solution.py:40
  80.9 3.3 %shard_map.194 = (f32[256,512]{1,0:T(8,128)S(1)}, bf16[256,256]{1,0:T(8,128)(2,1)S(1)}, bf16[136,256]{1,0:T(8,128)(2,1)S(1)}) custom-call(bf16[256,256]{1,0:T(8,128)(2,1)S(1)} %copy-done.10, bf16[256,256]{1,0:T(8,128)(2,1)S(1)} %copy-done.11, bf16[256,512]{1,0:T(8,128)(2,1)S(1)} %copy-done.8, bf16[256,256]{1,0:T(8,128)(2,1)S(1)} %copy-done.12, ...), custom_call_target="tpu_custom_call" | custom-call | flops 33554432 | tf_op jit(solution)/shard_map/pallas_call | solution.py:107
  84.1 2.0 %collective-permute-start.1 = (bf16[136,256]{1,0:T(8,128)(2,1)S(1)}, bf16[136,256]{1,0:T(8,128)(2,1)S(1)}, u32[]{:S(2)}, u32[]{:S(2)}) collective-permute-start(bf16[136,256]{1,0:T(8,128)(2,1)S(1)} %get-tuple-element.35), channel_id=1, source_target_pairs={{0,8},{1,9},{2,10},{3,11},{4,12},{5,13},{6,14},{7,15},{8,16},{9,17... | collective-permute-start | bytes 208904 | tf_op jit(solution)/shard_map/ppermute | solution.py:40
  86.1 4.6 %collective-permute-start.3 = (bf16[136,256]{1,0:T(8,128)(2,1)S(1)}, bf16[136,256]{1,0:T(8,128)(2,1)S(1)}, u32[]{:S(2)}, u32[]{:S(2)}) collective-permute-start(bf16[136,256]{1,0:T(8,128)(2,1)S(1)} %get-tuple-element.35), channel_id=1, source_target_pairs={{0,16},{1,17},{2,18},{3,19},{4,20},{5,21},{6,22},{7,23},{8,24},{9,... | collective-permute-start | bytes 208904 | tf_op jit(solution)/shard_map/ppermute | solution.py:40
  90.8 2.6 %collective-permute-done.1.refs_1_ = bf16[136,256]{1,0:T(8,128)(2,1)S(1)} collective-permute-done((bf16[136,256]{1,0:T(8,128)(2,1)S(1)}, bf16[136,256]{1,0:T(8,128)(2,1)S(1)}, u32[]{:S(2)}, u32[]{:S(2)}) %collective-permute-start.1) | collective-permute-done | bytes 69664 | tf_op jit(solution)/shard_map/ppermute | solution.py:40
  93.4 2.1 %collective-permute-done.3.refs_3_ = bf16[136,256]{1,0:T(8,128)(2,1)S(1)} collective-permute-done((bf16[136,256]{1,0:T(8,128)(2,1)S(1)}, bf16[136,256]{1,0:T(8,128)(2,1)S(1)}, u32[]{:S(2)}, u32[]{:S(2)}) %collective-permute-start.3) | collective-permute-done | bytes 69664 | tf_op jit(solution)/shard_map/ppermute | solution.py:40
  95.5 0.4 collective-permute-done.5.refs_5_
  95.9 0.1 collective-permute-start.4
  96.0 0.4 collective-permute-start.6
  96.4 0.3 collective-permute-done.2.refs_2_
  96.7 0.4 collective-permute-done.4.refs_4_
  97.2 0.2 collective-permute-done.6.refs_6_
  97.4 0.8 shard_map.196.refs_0_
  98.2 1.1 collective-permute-start.7
  99.3 1.3 %collective-permute-start.8 = (bf16[304,512]{1,0:T(8,128)(2,1)S(1)}, bf16[304,512]{1,0:T(8,128)(2,1)S(1)}, u32[]{:S(2)}, u32[]{:S(2)}) collective-permute-start(bf16[304,512]{1,0:T(8,128)(2,1)S(1)} %shard_map.196.refs_0_), channel_id=1, source_target_pairs={{0,2},{1,3},{2,0},{3,1},{4,6},{5,7},{6,4},{7,5},{8,10},{9,11},{10,... | collective-permute-start | bytes 933896 | tf_op jit(solution)/shard_map/ppermute | solution.py:40
  100.5 1.2 %collective-permute-start.9 = (bf16[304,512]{1,0:T(8,128)(2,1)S(1)}, bf16[304,512]{1,0:T(8,128)(2,1)S(1)}, u32[]{:S(2)}, u32[]{:S(2)}) collective-permute-start(bf16[304,512]{1,0:T(8,128)(2,1)S(1)} %shard_map.196.refs_0_), channel_id=1, source_target_pairs={{0,3},{1,2},{2,1},{3,0},{4,7},{5,6},{6,5},{7,4},{8,11},{9,10},{10,... | collective-permute-start | bytes 933896 | tf_op jit(solution)/shard_map/ppermute | solution.py:40
  101.7 0.4 shard_map.204
  102.1 0.2 fusion.5
  102.3 2.9 %collective-permute-start.33 = (bf16[96,512]{1,0:T(8,128)(2,1)S(1)}, bf16[96,512]{1,0:T(8,128)(2,1)S(1)}, u32[]{:S(2)}, u32[]{:S(2)}) collective-permute-start(bf16[96,512]{1,0:T(8,128)(2,1)S(1)} %get-tuple-element.64), channel_id=1, source_target_pairs={{0,24},{1,25},{2,26},{3,27},{4,28},{5,29},{6,30},{7,31},{8,0},{9,1... | collective-permute-start | bytes 294920 | tf_op jit(solution)/shard_map/ppermute | solution.py:40
  105.3 0.1 collective-permute-start.34
  105.3 3.1 %collective-permute-done.7.refs_1_ = bf16[304,512]{1,0:T(8,128)(2,1)S(1)} collective-permute-done((bf16[304,512]{1,0:T(8,128)(2,1)S(1)}, bf16[304,512]{1,0:T(8,128)(2,1)S(1)}, u32[]{:S(2)}, u32[]{:S(2)}) %collective-permute-start.7) | collective-permute-done | bytes 311328 | tf_op jit(solution)/shard_map/ppermute | solution.py:40
  108.5 1.5 %collective-permute-start.35 = (bf16[96,512]{1,0:T(8,128)(2,1)S(1)}, bf16[96,512]{1,0:T(8,128)(2,1)S(1)}, u32[]{:S(2)}, u32[]{:S(2)}) collective-permute-start(bf16[96,512]{1,0:T(8,128)(2,1)S(1)} %get-tuple-element.65), channel_id=1, source_target_pairs={{0,8},{1,9},{2,10},{3,11},{4,12},{5,13},{6,14},{7,15},{8,16},{9,17... | collective-permute-start | bytes 294920 | tf_op jit(solution)/shard_map/ppermute | solution.py:40
  110.0 5.3 %collective-permute-done.8.refs_2_ = bf16[304,512]{1,0:T(8,128)(2,1)S(1)} collective-permute-done((bf16[304,512]{1,0:T(8,128)(2,1)S(1)}, bf16[304,512]{1,0:T(8,128)(2,1)S(1)}, u32[]{:S(2)}, u32[]{:S(2)}) %collective-permute-start.8) | collective-permute-done | bytes 311328 | tf_op jit(solution)/shard_map/ppermute | solution.py:40
  115.3 0.9 shard_map.197
  116.2 0.7 copy.21
  116.9 0.7 fusion.4
  (57 shorter events, 0.2 us)
Async XLA Ops:
  0.6 31.9 %copy-start.1 = (bf16[1,2048,1024]{2,1,0:T(8,128)(2,1)S(1)}, bf16[1,2048,1024]{2,1,0:T(8,128)(2,1)}, u32[]{:S(2)}) copy-start(bf16[1,2048,1024]{2,1,0:T(8,128)(2,1)} %param.32) | copy-start | bytes 12582916
  2.2 22.4 %collective-permute-start.16 = (bf16[96,2048]{1,0:T(8,128)(2,1)S(1)}, bf16[96,2048]{1,0:T(8,128)(2,1)S(1)}, u32[]{:S(2)}, u32[]{:S(2)}) collective-permute-start(bf16[96,2048]{1,0:T(8,128)(2,1)S(1)} %get-tuple-element.34.normed_ref.refs_0_), channel_id=1, source_target_pairs={{0,4},{1,5},{2,6},{3,7},{4,0},{5,1},{6,2},{7,3},{8,12},{9,13},{10,... | collective-permute-start | bytes 1179656 | tf_op jit(solution)/shard_map/ppermute | solution.py:40
  2.7 10.9 %collective-permute-start.10 = (bf16[104,1024]{1,0:T(8,128)(2,1)S(1)}, bf16[104,1024]{1,0:T(8,128)(2,1)S(1)}, u32[]{:S(2)}, u32[]{:S(2)}) collective-permute-start(bf16[104,1024]{1,0:T(8,128)(2,1)S(1)} %get-tuple-element.37.refs_1_), channel_id=1, source_target_pairs={{0,8},{1,9},{2,10},{3,11},{4,12},{5,13},{6,14},{7,15},{8,16},{9,17... | collective-permute-start | bytes 638984 | tf_op jit(solution)/shard_map/ppermute | solution.py:40
  5.4 17.1 %collective-permute-start.12 = (bf16[104,1024]{1,0:T(8,128)(2,1)S(1)}, bf16[104,1024]{1,0:T(8,128)(2,1)S(1)}, u32[]{:S(2)}, u32[]{:S(2)}) collective-permute-start(bf16[104,1024]{1,0:T(8,128)(2,1)S(1)} %get-tuple-element.37.refs_1_), channel_id=1, source_target_pairs={{0,16},{1,17},{2,18},{3,19},{4,20},{5,21},{6,22},{7,23},{8,24},{9,... | collective-permute-start | bytes 638984 | tf_op jit(solution)/shard_map/ppermute | solution.py:40
  7.9 16.0 %collective-permute-start.14 = (bf16[104,1024]{1,0:T(8,128)(2,1)S(1)}, bf16[104,1024]{1,0:T(8,128)(2,1)S(1)}, u32[]{:S(2)}, u32[]{:S(2)}) collective-permute-start(bf16[104,1024]{1,0:T(8,128)(2,1)S(1)} %get-tuple-element.37.refs_1_), channel_id=1, source_target_pairs={{0,24},{1,25},{2,26},{3,27},{4,28},{5,29},{6,30},{7,31},{8,0},{9,1... | collective-permute-start | bytes 638984 | tf_op jit(solution)/shard_map/ppermute | solution.py:40
  9.3 15.2 %collective-permute-start.17 = (bf16[104,1024]{1,0:T(8,128)(2,1)S(1)}, bf16[104,1024]{1,0:T(8,128)(2,1)S(1)}, u32[]{:S(2)}, u32[]{:S(2)}) collective-permute-start(bf16[104,1024]{1,0:T(8,128)(2,1)S(1)} %get-tuple-element.37.refs_1_), channel_id=1, source_target_pairs={{0,4},{1,5},{2,6},{3,7},{4,0},{5,1},{6,2},{7,3},{8,12},{9,13},{10,... | collective-permute-start | bytes 638984 | tf_op jit(solution)/shard_map/ppermute | solution.py:40
  13.6 13.0 %collective-permute-start.11 = (bf16[104,1024]{1,0:T(8,128)(2,1)S(1)}, bf16[104,1024]{1,0:T(8,128)(2,1)S(1)}, u32[]{:S(2)}, u32[]{:S(2)}) collective-permute-start(bf16[104,1024]{1,0:T(8,128)(2,1)S(1)} %collective-permute-done.10.refs_2_), channel_id=1, source_target_pairs={{0,1},{1,0},{2,3},{3,2},{4,6},{5,7},{6,4},{7,5},{8,9},{9,8},{10,11... | collective-permute-start | bytes 638984 | tf_op jit(solution)/shard_map/ppermute | solution.py:40
  22.5 5.8 %collective-permute-start.13 = (bf16[104,1024]{1,0:T(8,128)(2,1)S(1)}, bf16[104,1024]{1,0:T(8,128)(2,1)S(1)}, u32[]{:S(2)}, u32[]{:S(2)}) collective-permute-start(bf16[104,1024]{1,0:T(8,128)(2,1)S(1)} %collective-permute-done.12.refs_4_), channel_id=1, source_target_pairs={{0,1},{1,0},{2,3},{3,2},{4,6},{5,7},{6,4},{7,5},{8,9},{9,8},{10,11... | collective-permute-start | bytes 638984 | tf_op jit(solution)/shard_map/ppermute | solution.py:40
  24.0 7.9 %collective-permute-start.15 = (bf16[104,1024]{1,0:T(8,128)(2,1)S(1)}, bf16[104,1024]{1,0:T(8,128)(2,1)S(1)}, u32[]{:S(2)}, u32[]{:S(2)}) collective-permute-start(bf16[104,1024]{1,0:T(8,128)(2,1)S(1)} %collective-permute-done.14.refs_6_), channel_id=1, source_target_pairs={{0,1},{1,0},{2,3},{3,2},{4,6},{5,7},{6,4},{7,5},{8,9},{9,8},{10,11... | collective-permute-start | bytes 638984 | tf_op jit(solution)/shard_map/ppermute | solution.py:40
  24.5 7.4 %collective-permute-start.18 = (bf16[104,1024]{1,0:T(8,128)(2,1)S(1)}, bf16[104,1024]{1,0:T(8,128)(2,1)S(1)}, u32[]{:S(2)}, u32[]{:S(2)}) collective-permute-start(bf16[104,1024]{1,0:T(8,128)(2,1)S(1)} %collective-permute-done.10.refs_2_), channel_id=1, source_target_pairs={{0,4},{1,5},{2,6},{3,7},{4,0},{5,1},{6,2},{7,3},{8,12},{9,13},{10,... | collective-permute-start | bytes 638984 | tf_op jit(solution)/shard_map/ppermute | solution.py:40
  24.5 7.9 %collective-permute-start.20 = (bf16[104,1024]{1,0:T(8,128)(2,1)S(1)}, bf16[104,1024]{1,0:T(8,128)(2,1)S(1)}, u32[]{:S(2)}, u32[]{:S(2)}) collective-permute-start(bf16[104,1024]{1,0:T(8,128)(2,1)S(1)} %collective-permute-done.12.refs_4_), channel_id=1, source_target_pairs={{0,4},{1,5},{2,6},{3,7},{4,0},{5,1},{6,2},{7,3},{8,12},{9,13},{10,... | collective-permute-start | bytes 638984 | tf_op jit(solution)/shard_map/ppermute | solution.py:40
  26.6 18.6 %collective-permute-start.24 = (bf16[512,512]{1,0:T(8,128)(2,1)S(1)}, bf16[512,512]{1,0:T(8,128)(2,1)S(1)}, u32[]{:S(2)}, u32[]{:S(2)}) collective-permute-start(bf16[512,512]{1,0:T(8,128)(2,1)S(1)} %get-tuple-element.48), channel_id=1, source_target_pairs={{0,2},{1,3},{2,0},{3,1},{4,5},{5,4},{6,7},{7,6},{8,10},{9,11},{10,... | collective-permute-start | bytes 1572872 | tf_op jit(solution)/shard_map/ppermute | solution.py:40
  28.3 9.5 %collective-permute-start.22 = (bf16[104,1024]{1,0:T(8,128)(2,1)S(1)}, bf16[104,1024]{1,0:T(8,128)(2,1)S(1)}, u32[]{:S(2)}, u32[]{:S(2)}) collective-permute-start(bf16[104,1024]{1,0:T(8,128)(2,1)S(1)} %collective-permute-done.14.refs_6_), channel_id=1, source_target_pairs={{0,4},{1,5},{2,6},{3,7},{4,0},{5,1},{6,2},{7,3},{8,12},{9,13},{10,... | collective-permute-start | bytes 638984 | tf_op jit(solution)/shard_map/ppermute | solution.py:40
  31.9 7.5 %collective-permute-start.19 = (bf16[104,1024]{1,0:T(8,128)(2,1)S(1)}, bf16[104,1024]{1,0:T(8,128)(2,1)S(1)}, u32[]{:S(2)}, u32[]{:S(2)}) collective-permute-start(bf16[104,1024]{1,0:T(8,128)(2,1)S(1)} %collective-permute-done.11.refs_3_), channel_id=1, source_target_pairs={{0,4},{1,5},{2,6},{3,7},{4,0},{5,1},{6,2},{7,3},{8,12},{9,13},{10,... | collective-permute-start | bytes 638984 | tf_op jit(solution)/shard_map/ppermute | solution.py:40
  31.9 9.0 %collective-permute-start.21 = (bf16[104,1024]{1,0:T(8,128)(2,1)S(1)}, bf16[104,1024]{1,0:T(8,128)(2,1)S(1)}, u32[]{:S(2)}, u32[]{:S(2)}) collective-permute-start(bf16[104,1024]{1,0:T(8,128)(2,1)S(1)} %collective-permute-done.13.refs_5_), channel_id=1, source_target_pairs={{0,4},{1,5},{2,6},{3,7},{4,0},{5,1},{6,2},{7,3},{8,12},{9,13},{10,... | collective-permute-start | bytes 638984 | tf_op jit(solution)/shard_map/ppermute | solution.py:40
  32.4 8.5 %collective-permute-start.23 = (bf16[104,1024]{1,0:T(8,128)(2,1)S(1)}, bf16[104,1024]{1,0:T(8,128)(2,1)S(1)}, u32[]{:S(2)}, u32[]{:S(2)}) collective-permute-start(bf16[104,1024]{1,0:T(8,128)(2,1)S(1)} %collective-permute-done.15.refs_7_), channel_id=1, source_target_pairs={{0,4},{1,5},{2,6},{3,7},{4,0},{5,1},{6,2},{7,3},{8,12},{9,13},{10,... | collective-permute-start | bytes 638984 | tf_op jit(solution)/shard_map/ppermute | solution.py:40
  32.5 2.2 %copy-start.2 = (bf16[1,2048,1024]{2,1,0:T(8,128)(2,1)S(1)}, bf16[1,2048,1024]{2,1,0:T(8,128)(2,1)}, u32[]{:S(2)}) copy-start(bf16[1,2048,1024]{2,1,0:T(8,128)(2,1)} %param.33) | copy-start | bytes 12582916
  34.7 6.3 %copy-start.3 = (bf16[1,2048,1024]{2,1,0:T(8,128)(2,1)S(1)}, bf16[1,2048,1024]{2,1,0:T(8,128)(2,1)}, u32[]{:S(2)}) copy-start(bf16[1,2048,1024]{2,1,0:T(8,128)(2,1)} %param.33) | copy-start | bytes 12582916
  37.8 14.2 %collective-permute-start.25 = (bf16[512,512]{1,0:T(8,128)(2,1)S(1)}, bf16[512,512]{1,0:T(8,128)(2,1)S(1)}, u32[]{:S(2)}, u32[]{:S(2)}) collective-permute-start(bf16[512,512]{1,0:T(8,128)(2,1)S(1)} %get-tuple-element.49), channel_id=1, source_target_pairs={{0,2},{1,3},{2,0},{3,1},{4,5},{5,4},{6,7},{7,6},{8,10},{9,11},{10,... | collective-permute-start | bytes 1572872 | tf_op jit(solution)/shard_map/ppermute | solution.py:40
  39.4 12.6 %copy-start = (bf16[1,4096,512]{2,1,0:T(8,128)(2,1)S(1)}, bf16[1,4096,512]{2,1,0:T(8,128)(2,1)}, u32[]{:S(2)}) copy-start(bf16[1,4096,512]{2,1,0:T(8,128)(2,1)} %param.34) | copy-start | bytes 12582916
  39.4 31.5 %collective-permute-start.26 = (bf16[288,1024]{1,0:T(8,128)(2,1)S(1)}, bf16[288,1024]{1,0:T(8,128)(2,1)S(1)}, u32[]{:S(2)}, u32[]{:S(2)}) collective-permute-start(bf16[288,1024]{1,0:T(8,128)(2,1)S(1)} %get-tuple-element.38.refs_0_), channel_id=1, source_target_pairs={{0,1},{1,0},{2,3},{3,2},{4,6},{5,7},{6,4},{7,5},{8,9},{9,8},{10,11... | collective-permute-start | bytes 1769480 | tf_op jit(solution)/shard_map/ppermute | solution.py:40
  44.1 27.4 %collective-permute-start.27 = (bf16[288,1024]{1,0:T(8,128)(2,1)S(1)}, bf16[288,1024]{1,0:T(8,128)(2,1)S(1)}, u32[]{:S(2)}, u32[]{:S(2)}) collective-permute-start(bf16[288,1024]{1,0:T(8,128)(2,1)S(1)} %get-tuple-element.47.refs_1_), channel_id=1, source_target_pairs={{0,1},{1,0},{2,3},{3,2},{4,6},{5,7},{6,4},{7,5},{8,9},{9,8},{10,11... | collective-permute-start | bytes 1769480 | tf_op jit(solution)/shard_map/ppermute | solution.py:40
  44.7 18.6 %collective-permute-start.28 = (bf16[512,512]{1,0:T(8,128)(2,1)S(1)}, bf16[512,512]{1,0:T(8,128)(2,1)S(1)}, u32[]{:S(2)}, u32[]{:S(2)}) collective-permute-start(bf16[512,512]{1,0:T(8,128)(2,1)S(1)} %get-tuple-element.53), channel_id=1, source_target_pairs={{0,2},{1,3},{2,0},{3,1},{4,5},{5,4},{6,7},{7,6},{8,10},{9,11},{10,... | collective-permute-start | bytes 1572872 | tf_op jit(solution)/shard_map/ppermute | solution.py:40
  45.2 25.8 %collective-permute-start.29 = (bf16[512,512]{1,0:T(8,128)(2,1)S(1)}, bf16[512,512]{1,0:T(8,128)(2,1)S(1)}, u32[]{:S(2)}, u32[]{:S(2)}) collective-permute-start(bf16[512,512]{1,0:T(8,128)(2,1)S(1)} %get-tuple-element.54), channel_id=1, source_target_pairs={{0,2},{1,3},{2,0},{3,1},{4,5},{5,4},{6,7},{7,6},{8,10},{9,11},{10,... | collective-permute-start | bytes 1572872 | tf_op jit(solution)/shard_map/ppermute | solution.py:40
  71.9 8.9 %copy-start.8 = (bf16[256,512]{1,0:T(8,128)(2,1)S(1)}, bf16[256,512]{1,0:T(8,128)(2,1)}, u32[]{:S(2)}) copy-start(bf16[256,512]{1,0:T(8,128)(2,1)} %v_ref.1) | copy-start | bytes 786436
  72.0 8.9 %copy-start.10 = (bf16[256,256]{1,0:T(8,128)(2,1)S(1)}, bf16[256,256]{1,0:T(8,128)(2,1)}, u32[]{:S(2)}) copy-start(bf16[256,256]{1,0:T(8,128)(2,1)} %q_ref.1) | copy-start | bytes 393220
  72.0 8.9 %copy-start.11 = (bf16[256,256]{1,0:T(8,128)(2,1)S(1)}, bf16[256,256]{1,0:T(8,128)(2,1)}, u32[]{:S(2)}) copy-start(bf16[256,256]{1,0:T(8,128)(2,1)} %k_ref.1) | copy-start | bytes 393220
  72.0 8.9 %copy-start.12 = (bf16[256,256]{1,0:T(8,128)(2,1)S(1)}, bf16[256,256]{1,0:T(8,128)(2,1)}, u32[]{:S(2)}) copy-start(bf16[256,256]{1,0:T(8,128)(2,1)} %d_ref.1) | copy-start | bytes 393220
  72.0 8.8 %copy-start.13 = (f32[4,256]{1,0:T(4,128)S(1)}, f32[4,256]{1,0:T(4,128)}, u32[]{:S(2)}) copy-start(f32[4,256]{1,0:T(4,128)} %added_ref.1) | copy-start | bytes 12292
  72.0 8.8 %copy-start.15 = (f32[256]{0:T(256)S(1)}, f32[256]{0:T(256)}, u32[]{:S(2)}) copy-start(f32[256]{0:T(256)} %param.24) | copy-start | bytes 3076
  72.0 6.8 %collective-permute-start.31 = (bf16[288,512]{1,0:T(8,128)(2,1)S(1)}, bf16[288,512]{1,0:T(8,128)(2,1)S(1)}, u32[]{:S(2)}, u32[]{:S(2)}) collective-permute-start(bf16[288,512]{1,0:T(8,128)(2,1)S(1)} %shard_map.205), channel_id=1, source_target_pairs={{0,2},{1,3},{2,0},{3,1},{4,5},{5,4},{6,7},{7,6},{8,10},{9,11},{10,... | collective-permute-start | bytes 884744 | tf_op jit(solution)/shard_map/ppermute | solution.py:40
  73.6 23.7 %copy-start.5 = (bf16[2048,256]{1,0:T(8,128)(2,1)S(1)}, bf16[2048,256]{1,0:T(8,128)(2,1)}, u32[]{:S(2)}) copy-start(bf16[2048,256]{1,0:T(8,128)(2,1)} %sg_ref.1) | copy-start | bytes 3145732
  73.6 23.7 %copy-start.6 = (bf16[2048,256]{1,0:T(8,128)(2,1)S(1)}, bf16[2048,256]{1,0:T(8,128)(2,1)}, u32[]{:S(2)}) copy-start(bf16[2048,256]{1,0:T(8,128)(2,1)} %su_ref.1) | copy-start | bytes 3145732
  73.6 23.7 %copy-start.9 = (bf16[256,512]{1,0:T(8,128)(2,1)S(1)}, bf16[256,512]{1,0:T(8,128)(2,1)}, u32[]{:S(2)}) copy-start(bf16[256,512]{1,0:T(8,128)(2,1)} %gate_ref.1) | copy-start | bytes 786436
  73.6 23.7 %copy-start.14 = (f32[512]{0:T(512)S(1)}, f32[512]{0:T(512)}, u32[]{:S(2)}) copy-start(f32[512]{0:T(512)} %param.26) | copy-start | bytes 6148
  79.2 23.0 %collective-permute-start.32 = (bf16[4,96,512]{2,1,0:T(8,128)(2,1)S(1)}, bf16[4,96,512]{2,1,0:T(8,128)(2,1)S(1)}, u32[]{:S(2)}, u32[]{:S(2)}) collective-permute-start(bf16[4,96,512]{2,1,0:T(8,128)(2,1)S(1)} %shard_map.206), channel_id=1, source_target_pairs={{0,4},{1,5},{2,6},{3,7},{4,0},{5,1},{6,2},{7,3},{8,12},{9,13},{10,... | collective-permute-start | bytes 1179656 | tf_op jit(solution)/shard_map/ppermute | solution.py:40
  79.2 22.5 %collective-permute-start.30 = (bf16[288,512]{1,0:T(8,128)(2,1)S(1)}, bf16[288,512]{1,0:T(8,128)(2,1)S(1)}, u32[]{:S(2)}, u32[]{:S(2)}) collective-permute-start(bf16[288,512]{1,0:T(8,128)(2,1)S(1)} %shard_map.202), channel_id=1, source_target_pairs={{0,2},{1,3},{2,0},{3,1},{4,5},{5,4},{6,7},{7,6},{8,10},{9,11},{10,... | collective-permute-start | bytes 884744 | tf_op jit(solution)/shard_map/ppermute | solution.py:40
  84.1 9.3 %collective-permute-start.1 = (bf16[136,256]{1,0:T(8,128)(2,1)S(1)}, bf16[136,256]{1,0:T(8,128)(2,1)S(1)}, u32[]{:S(2)}, u32[]{:S(2)}) collective-permute-start(bf16[136,256]{1,0:T(8,128)(2,1)S(1)} %get-tuple-element.35), channel_id=1, source_target_pairs={{0,8},{1,9},{2,10},{3,11},{4,12},{5,13},{6,14},{7,15},{8,16},{9,17... | collective-permute-start | bytes 208904 | tf_op jit(solution)/shard_map/ppermute | solution.py:40
  86.1 9.3 %collective-permute-start.3 = (bf16[136,256]{1,0:T(8,128)(2,1)S(1)}, bf16[136,256]{1,0:T(8,128)(2,1)S(1)}, u32[]{:S(2)}, u32[]{:S(2)}) collective-permute-start(bf16[136,256]{1,0:T(8,128)(2,1)S(1)} %get-tuple-element.35), channel_id=1, source_target_pairs={{0,16},{1,17},{2,18},{3,19},{4,20},{5,21},{6,22},{7,23},{8,24},{9,... | collective-permute-start | bytes 208904 | tf_op jit(solution)/shard_map/ppermute | solution.py:40
  90.8 5.1 %collective-permute-start.5 = (bf16[136,256]{1,0:T(8,128)(2,1)S(1)}, bf16[136,256]{1,0:T(8,128)(2,1)S(1)}, u32[]{:S(2)}, u32[]{:S(2)}) collective-permute-start(bf16[136,256]{1,0:T(8,128)(2,1)S(1)} %get-tuple-element.35), channel_id=1, source_target_pairs={{0,24},{1,25},{2,26},{3,27},{4,28},{5,29},{6,30},{7,31},{8,0},{9,1... | collective-permute-start | bytes 208904 | tf_op jit(solution)/shard_map/ppermute | solution.py:40
  93.4 2.6 %collective-permute-start = (bf16[136,256]{1,0:T(8,128)(2,1)S(1)}, bf16[136,256]{1,0:T(8,128)(2,1)S(1)}, u32[]{:S(2)}, u32[]{:S(2)}) collective-permute-start(bf16[136,256]{1,0:T(8,128)(2,1)S(1)} %get-tuple-element.35), channel_id=1, source_target_pairs={{0,4},{1,5},{2,6},{3,7},{4,0},{5,1},{6,2},{7,3},{8,12},{9,13},{10,... | collective-permute-start | bytes 208904 | tf_op jit(solution)/shard_map/ppermute | solution.py:40
  95.5 1.3 %collective-permute-start.2 = (bf16[136,256]{1,0:T(8,128)(2,1)S(1)}, bf16[136,256]{1,0:T(8,128)(2,1)S(1)}, u32[]{:S(2)}, u32[]{:S(2)}) collective-permute-start(bf16[136,256]{1,0:T(8,128)(2,1)S(1)} %collective-permute-done.1.refs_1_), channel_id=1, source_target_pairs={{0,4},{1,5},{2,6},{3,7},{4,0},{5,1},{6,2},{7,3},{8,12},{9,13},{10,... | collective-permute-start | bytes 208904 | tf_op jit(solution)/shard_map/ppermute | solution.py:40
  95.9 1.3 %collective-permute-start.4 = (bf16[136,256]{1,0:T(8,128)(2,1)S(1)}, bf16[136,256]{1,0:T(8,128)(2,1)S(1)}, u32[]{:S(2)}, u32[]{:S(2)}) collective-permute-start(bf16[136,256]{1,0:T(8,128)(2,1)S(1)} %collective-permute-done.3.refs_3_), channel_id=1, source_target_pairs={{0,4},{1,5},{2,6},{3,7},{4,0},{5,1},{6,2},{7,3},{8,12},{9,13},{10,... | collective-permute-start | bytes 208904 | tf_op jit(solution)/shard_map/ppermute | solution.py:40
  96.0 1.3 %collective-permute-start.6 = (bf16[136,256]{1,0:T(8,128)(2,1)S(1)}, bf16[136,256]{1,0:T(8,128)(2,1)S(1)}, u32[]{:S(2)}, u32[]{:S(2)}) collective-permute-start(bf16[136,256]{1,0:T(8,128)(2,1)S(1)} %collective-permute-done.5.refs_5_), channel_id=1, source_target_pairs={{0,4},{1,5},{2,6},{3,7},{4,0},{5,1},{6,2},{7,3},{8,12},{9,13},{10,... | collective-permute-start | bytes 208904 | tf_op jit(solution)/shard_map/ppermute | solution.py:40
  97.3 17.9 %copy-start.4 = (bf16[2048,512]{1,0:T(8,128)(2,1)S(1)}, bf16[2048,512]{1,0:T(8,128)(2,1)}, u32[]{:S(2)}) copy-start(bf16[2048,512]{1,0:T(8,128)(2,1)} %refs_4_.1) | copy-start | bytes 6291460
  97.3 17.9 %copy-start.7 = (bf16[1024,512]{1,0:T(8,128)(2,1)S(1)}, bf16[1024,512]{1,0:T(8,128)(2,1)}, u32[]{:S(2)}) copy-start(bf16[1024,512]{1,0:T(8,128)(2,1)} %refs_5_.1) | copy-start | bytes 3145732
  98.2 10.3 %collective-permute-start.7 = (bf16[304,512]{1,0:T(8,128)(2,1)S(1)}, bf16[304,512]{1,0:T(8,128)(2,1)S(1)}, u32[]{:S(2)}, u32[]{:S(2)}) collective-permute-start(bf16[304,512]{1,0:T(8,128)(2,1)S(1)} %shard_map.196.refs_0_), channel_id=1, source_target_pairs={{0,1},{1,0},{2,3},{3,2},{4,5},{5,4},{6,7},{7,6},{8,9},{9,8},{10,11... | collective-permute-start | bytes 933896 | tf_op jit(solution)/shard_map/ppermute | solution.py:40
  99.3 16.0 %collective-permute-start.8 = (bf16[304,512]{1,0:T(8,128)(2,1)S(1)}, bf16[304,512]{1,0:T(8,128)(2,1)S(1)}, u32[]{:S(2)}, u32[]{:S(2)}) collective-permute-start(bf16[304,512]{1,0:T(8,128)(2,1)S(1)} %shard_map.196.refs_0_), channel_id=1, source_target_pairs={{0,2},{1,3},{2,0},{3,1},{4,6},{5,7},{6,4},{7,5},{8,10},{9,11},{10,... | collective-permute-start | bytes 933896 | tf_op jit(solution)/shard_map/ppermute | solution.py:40
  100.5 14.8 %collective-permute-start.9 = (bf16[304,512]{1,0:T(8,128)(2,1)S(1)}, bf16[304,512]{1,0:T(8,128)(2,1)S(1)}, u32[]{:S(2)}, u32[]{:S(2)}) collective-permute-start(bf16[304,512]{1,0:T(8,128)(2,1)S(1)} %shard_map.196.refs_0_), channel_id=1, source_target_pairs={{0,3},{1,2},{2,1},{3,0},{4,7},{5,6},{6,5},{7,4},{8,11},{9,10},{10,... | collective-permute-start | bytes 933896 | tf_op jit(solution)/shard_map/ppermute | solution.py:40
  102.3 14.6 %collective-permute-start.33 = (bf16[96,512]{1,0:T(8,128)(2,1)S(1)}, bf16[96,512]{1,0:T(8,128)(2,1)S(1)}, u32[]{:S(2)}, u32[]{:S(2)}) collective-permute-start(bf16[96,512]{1,0:T(8,128)(2,1)S(1)} %get-tuple-element.64), channel_id=1, source_target_pairs={{0,24},{1,25},{2,26},{3,27},{4,28},{5,29},{6,30},{7,31},{8,0},{9,1... | collective-permute-start | bytes 294920 | tf_op jit(solution)/shard_map/ppermute | solution.py:40
  105.3 11.6 %collective-permute-start.34 = (bf16[96,512]{1,0:T(8,128)(2,1)S(1)}, bf16[96,512]{1,0:T(8,128)(2,1)S(1)}, u32[]{:S(2)}, u32[]{:S(2)}) collective-permute-start(bf16[96,512]{1,0:T(8,128)(2,1)S(1)} %get-tuple-element.66), channel_id=1, source_target_pairs={{0,16},{1,17},{2,18},{3,19},{4,20},{5,21},{6,22},{7,23},{8,24},{9,... | collective-permute-start | bytes 294920 | tf_op jit(solution)/shard_map/ppermute | solution.py:40
  108.5 8.4 %collective-permute-start.35 = (bf16[96,512]{1,0:T(8,128)(2,1)S(1)}, bf16[96,512]{1,0:T(8,128)(2,1)S(1)}, u32[]{:S(2)}, u32[]{:S(2)}) collective-permute-start(bf16[96,512]{1,0:T(8,128)(2,1)S(1)} %get-tuple-element.65), channel_id=1, source_target_pairs={{0,8},{1,9},{2,10},{3,11},{4,12},{5,13},{6,14},{7,15},{8,16},{9,17... | collective-permute-start | bytes 294920 | tf_op jit(solution)/shard_map/ppermute | solution.py:40

commit v5 on v4

--- a/solution.py
+++ b/solution.py
@@ -257,26 +257,36 @@
     return call(body, outs, operands, 2 * folded * width * columns * count)
 
 
-def prepare_rows(places, parts, rows, gain, index, scores, experts):
+def prepare_rows(places, parts, rows, gain, index, scores, experts, weight, wanted, hidden):
+    size = hidden // PIECES
     tokens, width = rows.shape
     top = index.shape[1]
-    piece = width // parts
+    part = width // parts
     pad = -(-tokens // 128) * 128
     extra = -(-experts // 8) * 8
 
-    def body(rows_hbm, gain_hbm, index_hbm, score_hbm, normed_ref, packed_ref, *scratch):
-        rows_ref, gain_ref, index_ref, score_ref, done = scratch
+    def body(rows_hbm, gain_hbm, index_hbm, score_hbm, weight_hbm, normed_ref, packed_ref, *refs):
+        pieces, scratch = refs[: len(wanted)], refs[len(wanted) :]
+        rows_ref, gain_ref, index_ref, score_ref, done, taken = scratch
+        here = Here(places)
         copies = [
             pltpu.make_async_copy(source, target, done.at[i])
             for i, (source, target) in enumerate(
                 zip((rows_hbm, gain_hbm, index_hbm, score_hbm), scratch[:4])
             )
         ]
-        for copy in copies:
+        takes = []
+        for i, (du, dv, piece) in enumerate(wanted):
+            start = pl.multiple_of(here.column(du, dv) * hidden + piece * size, size)
+            takes.append(
+                pltpu.make_async_copy(
+                    weight_hbm.at[pl.ds(start, size), :], pieces[i], taken.at[i]
+                )
+            )
+        for copy in copies + takes:
             copy.start()
         for copy in copies:
             copy.wait()
-        here = Here(places)
         value = rows_ref[...].astype(f32)
         mean_square = jnp.mean(value * value, axis=1, keepdims=True)
         normed = (value * lax.rsqrt(mean_square + epsilon) * gain_ref[...]).astype(bf16)
@@ -285,34 +295,38 @@
 
             @pl.when(here.part == q)
             def _():
-                packed_ref[0:tokens, :] = normed[:, q * piece : (q + 1) * piece]
+                packed_ref[0:tokens, :] = normed[:, q * part : (q + 1) * part]
 
         scores = score_ref[...]
         weights = routed_scale * scores / jnp.sum(scores, axis=0, keepdims=True)
         expert = lax.broadcasted_iota(jnp.int32, (extra, tokens), 0)
         named = jnp.zeros((extra, tokens), f32)
-        weight = jnp.zeros((extra, tokens), f32)
+        share = jnp.zeros((extra, tokens), f32)
         for k in range(top):
             hit = index_ref[k : k + 1, :] == expert
             named = jnp.where(hit, 1.0, named)
-            weight = jnp.where(hit, weights[k : k + 1, :], weight)
+            share = jnp.where(hit, weights[k : k + 1, :], share)
         strict = (
             lax.broadcasted_iota(jnp.int32, (tokens, tokens), 0)
             < lax.broadcasted_iota(jnp.int32, (tokens, tokens), 1)
         ).astype(bf16)
         ranks = jnp.where(named > 0, dot(named.astype(bf16), strict), -1.0)
-        packed_ref[tokens : tokens + extra, :] = jnp.full((extra, piece), -1.0, bf16)
+        packed_ref[tokens : tokens + extra, :] = jnp.full((extra, part), -1.0, bf16)
         packed_ref[tokens : tokens + extra, 0:tokens] = ranks.astype(bf16)
-        packed_ref[tokens : tokens + extra, pad : pad + tokens] = weight.astype(bf16)
-
-    outs = (
+        packed_ref[tokens : tokens + extra, pad : pad + tokens] = share.astype(bf16)
+        for copy in takes:
+            copy.wait()
+
+    outs = [
         jax.ShapeDtypeStruct((tokens, width), bf16),
-        jax.ShapeDtypeStruct((tokens + extra, piece), bf16),
-    )
-    operands = (rows, gain[None, :], index.T, scores.T)
-    scratch = [pltpu.VMEM(v.shape, v.dtype) for v in operands]
-    scratch.append(pltpu.SemaphoreType.DMA((4,)))
-    return call(body, outs, operands, 1 << 22, scratch=scratch, far=4)
+        jax.ShapeDtypeStruct((tokens + extra, part), bf16),
+    ]
+    outs += [jax.ShapeDtypeStruct((size, weight.shape[1]), weight.dtype) for _ in wanted]
+    operands = (rows, gain[None, :], index.T, scores.T, weight)
+    scratch = [pltpu.VMEM(v.shape, v.dtype) for v in operands[:4]]
+    scratch += [pltpu.SemaphoreType.DMA((4,)), pltpu.SemaphoreType.DMA((len(wanted),))]
+    normed, packed, *taken = call(body, outs, operands, 1 << 22, scratch=scratch, far=5)
+    return normed, packed, taken
 
 
 def group_of(sources, capacity):
@@ -385,26 +399,22 @@
     return call(body, outs, operands, 4 * slots * width * hidden, scratch=scratch)
 
 
-def take_pieces(places, weight, wanted, hidden):
-    size = hidden // PIECES
-
-    def body(in_ref, *refs):
-        outs, done = refs[:-1], refs[-1]
-        here = Here(places)
-        copies = []
-        for i, (du, dv, piece) in enumerate(wanted):
-            start = pl.multiple_of(here.column(du, dv) * hidden + piece * size, size)
-            copies.append(
-                pltpu.make_async_copy(in_ref.at[pl.ds(start, size), :], outs[i], done.at[i])
-            )
+def load(weights):
+    count = len(weights)
+
+    def body(*refs):
+        done = refs[-1]
+        copies = [
+            pltpu.make_async_copy(refs[i], refs[count + i], done.at[i]) for i in range(count)
+        ]
         for copy in copies:
             copy.start()
         for copy in copies:
             copy.wait()
 
-    outs = [jax.ShapeDtypeStruct((size, weight.shape[1]), weight.dtype) for _ in wanted]
-    scratch = (pltpu.SemaphoreType.DMA((len(wanted),)),)
-    return call(body, outs, (weight,), 1 << 20, scratch=scratch, far=1)
+    outs = [jax.ShapeDtypeStruct(w.shape, w.dtype) for w in weights]
+    scratch = (pltpu.SemaphoreType.DMA((count,)),)
+    return call(body, outs, weights, 1 << 20, scratch=scratch, far=count)
 
 
 def dot_pieces(ref, pieces):
@@ -535,7 +545,6 @@
     traded = [[[] for _ in range(n)] for _ in range(1, n)]
     lacking = [(i, piece) for i in range(n) for piece in range(PIECES)]
     wanted = [(i, k, piece) for i, piece in lacking for k in range(1, n)]
-    taken = take_pieces(at, down_weight, [(-i, k, p) for i, k, p in wanted], hidden)
     quarter = len(wanted) // 4
 
     def trade(number):
@@ -543,7 +552,7 @@
             i, k, _ = wanted[at_piece]
             traded[k - 1][i].append(at.along_v(taken[at_piece], k))
 
-    normed, packed = prepare_rows(
+    normed, packed, taken = prepare_rows(
         at,
         n,
         second_batch_rows,
@@ -551,6 +560,9 @@
         routed_expert_index,
         router_chosen_scores,
         experts,
+        down_weight,
+        [(-i, k, piece) for i, k, piece in wanted],
+        hidden,
     )
     middle = chips // 2
     far = {middle: at.along_z(packed, middle)}
@@ -576,6 +588,7 @@
     for pieces, others in zip(far, other[1]):
         others += [at.to_sibling(p) for p in pieces[1:]]
     trade(3)
+    gate_weight, up_weight = load((gate_weight, up_weight))
     ups = [expert_up(at, (normed, packed), far, capacity, gate_weight, up_weight)]
     gathered_first = [at.along_u(ups[0][0], i) for i in range(1, n)]
     _, other = hold((ups[0][0], other))
@@ -603,7 +616,7 @@
 
     partial = partials(0, gathered_first)
     back = [[at.along_v(partial[k - 1], -k) for k in range(1, n)]]
-    gathered_second, _ = hold((gathered_second, partial))
+    gathered_second, both, _ = hold((gathered_second, both, partial))
     partial = partials(1, gathered_second)
     back.append([at.along_v(partial[k - 1], -k) for k in range(1, n)])
     gathered = [list(pair) for pair in zip(gathered_first, gathered_second)]

time: 118 us -> 120 us (1.017)
  local copies, waits for them, and re-layouts: 2.99 us -> 5.79 us
  Pallas kernels: 18.2 us -> 20.5 us
  starting transfers between devices: 37.8 us -> 36 us
    unnamed x33 -> x27, local copies, waits for them, and re-layouts: 2.97 us -> 5.77 us
    pallas_call x13, Pallas kernels: 18.2 us -> 20.5 us  [call(): pl.pallas_call(body, out_shape=jax.tree.map(lambda o: pltpu.VMEM(o.shape,...]
    ppermute x36, starting transfers between devices: 37.8 us -> 36 us  [send(): return lax.ppermute(value, AXES, self.pairs(move))]
  transfers between devices with their start and end apart: 36 -> 36, of which waited for: 16 -> 10; matrix products, arithmetic and copies ran while one was open for 1% -> 1% of each run, Pallas kernels for 13% -> 14%
where the time goes in v5:
time: 120 us
  waiting for transfers between devices  55.9 us (47%)
  starting transfers between devices  36 us (30%)
  Pallas kernels  20.5 us (17%)
  local copies, waits for them, and re-layouts  5.79 us (5%)
    ppermute x36, waiting for transfers between devices, send(): return lax.ppermute(value, AXES, self.pairs(move))  55.9 us
    ppermute x36, starting transfers between devices, send(): return lax.ppermute(value, AXES, self.pairs(move))  36 us
    pallas_call x13, Pallas kernels, call(): pl.pallas_call(body, out_shape=jax.tree.map(lambda o: pltpu.VMEM(o.shape,...  20.5 us
    unnamed x27, local copies, waits for them, and re-layouts  5.77 us
  transfers between devices with their start and end apart: 36, of which 10 were waited for; matrix products, arithmetic and copies ran while one was open for 1% of the time, Pallas kernels for 14%

profile of v5, /device:TPU:0, one launch (start us, length us, event | category | flops | bytes accessed | tf_op | source)
XLA Modules:
  0.0 120.0 jit_solution(18214772416769602673)
XLA Ops:
  0.6 0.9 copy-done.5
  1.6 0.9 copy-done.7
  2.5 0.9 copy-done.8
  3.4 0.9 copy-done.9
  4.3 0.7 copy-done.10
  5.0 0.7 copy-done.12
  5.7 3.3 %shard_map.198 = (f32[256,512]{1,0:T(8,128)S(1)}, bf16[256,256]{1,0:T(8,128)(2,1)S(1)}, bf16[136,256]{1,0:T(8,128)(2,1)S(1)}) custom-call(bf16[256,256]{1,0:T(8,128)(2,1)S(1)} %copy-done.7, bf16[256,256]{1,0:T(8,128)(2,1)S(1)} %copy-done.8, bf16[256,512]{1,0:T(8,128)(2,1)S(1)} %copy-done.5, bf16[256,256]{1,0:T(8,128)(2,1)S(1)} %copy-done.9, ...), custom_call_target="tpu_custom_call" | custom-call | flops 33554432 | tf_op jit(solution)/shard_map/pallas_call | solution.py:107
  8.9 3.1 %collective-permute-start.16 = (bf16[136,256]{1,0:T(8,128)(2,1)S(1)}, bf16[136,256]{1,0:T(8,128)(2,1)S(1)}, u32[]{:S(2)}, u32[]{:S(2)}) collective-permute-start(bf16[136,256]{1,0:T(8,128)(2,1)S(1)} %get-tuple-element.51), channel_id=1, source_target_pairs={{0,8},{1,9},{2,10},{3,11},{4,12},{5,13},{6,14},{7,15},{8,16},{9,17... | collective-permute-start | bytes 208904 | tf_op jit(solution)/shard_map/ppermute | solution.py:40
  12.0 1.8 %shard_map.194 = (bf16[96,2048]{1,0:T(8,128)(2,1)S(1)}, bf16[104,1024]{1,0:T(8,128)(2,1)S(1)}, bf16[512,512]{1,0:T(8,128)(2,1)S(1)}, bf16[512,512]{1,0:T(8,128)(...) custom-call(bf16[96,2048]{1,0:T(8,128)(2,1)} %rows_hbm.1, f32[1,2048]{1,0:T(1,128)} %bitcast.33, ...), custom_call_target="tpu_custom_call" | custom-call | flops 4194304 | tf_op jit(solution)/shard_map/pallas_call | solution.py:107
  13.7 0.1 collective-permute-start.6
  13.8 1.6 %collective-permute-start = (bf16[104,1024]{1,0:T(8,128)(2,1)S(1)}, bf16[104,1024]{1,0:T(8,128)(2,1)S(1)}, u32[]{:S(2)}, u32[]{:S(2)}) collective-permute-start(bf16[104,1024]{1,0:T(8,128)(2,1)S(1)} %get-tuple-element.36.refs_1_), channel_id=1, source_target_pairs={{0,8},{1,9},{2,10},{3,11},{4,12},{5,13},{6,14},{7,15},{8,16},{9,17... | collective-permute-start | bytes 638984 | tf_op jit(solution)/shard_map/ppermute | solution.py:40
  15.4 1.1 collective-permute-start.2
  16.5 2.8 %collective-permute-start.4 = (bf16[104,1024]{1,0:T(8,128)(2,1)S(1)}, bf16[104,1024]{1,0:T(8,128)(2,1)S(1)}, u32[]{:S(2)}, u32[]{:S(2)}) collective-permute-start(bf16[104,1024]{1,0:T(8,128)(2,1)S(1)} %get-tuple-element.36.refs_1_), channel_id=1, source_target_pairs={{0,24},{1,25},{2,26},{3,27},{4,28},{5,29},{6,30},{7,31},{8,0},{9,1... | collective-permute-start | bytes 638984 | tf_op jit(solution)/shard_map/ppermute | solution.py:40
  19.4 4.5 %collective-permute-done.refs_2_ = bf16[104,1024]{1,0:T(8,128)(2,1)S(1)} collective-permute-done((bf16[104,1024]{1,0:T(8,128)(2,1)S(1)}, bf16[104,1024]{1,0:T(8,128)(2,1)S(1)}, u32[]{:S(2)}, u32[]{:S(2)}) %collective-permute-start) | collective-permute-done | bytes 213024 | tf_op jit(solution)/shard_map/ppermute | solution.py:40
  23.9 1.5 %collective-permute-start.1 = (bf16[104,1024]{1,0:T(8,128)(2,1)S(1)}, bf16[104,1024]{1,0:T(8,128)(2,1)S(1)}, u32[]{:S(2)}, u32[]{:S(2)}) collective-permute-start(bf16[104,1024]{1,0:T(8,128)(2,1)S(1)} %collective-permute-done.refs_2_), channel_id=1, source_target_pairs={{0,1},{1,0},{2,3},{3,2},{4,6},{5,7},{6,4},{7,5},{8,9},{9,8},{10,11... | collective-permute-start | bytes 638984 | tf_op jit(solution)/shard_map/ppermute | solution.py:40
  25.4 7.1 %collective-permute-done.2.refs_4_ = bf16[104,1024]{1,0:T(8,128)(2,1)S(1)} collective-permute-done((bf16[104,1024]{1,0:T(8,128)(2,1)S(1)}, bf16[104,1024]{1,0:T(8,128)(2,1)S(1)}, u32[]{:S(2)}, u32[]{:S(2)}) %collective-permute-start.2) | collective-permute-done | bytes 213024 | tf_op jit(solution)/shard_map/ppermute | solution.py:40
  32.5 1.5 %collective-permute-start.3 = (bf16[104,1024]{1,0:T(8,128)(2,1)S(1)}, bf16[104,1024]{1,0:T(8,128)(2,1)S(1)}, u32[]{:S(2)}, u32[]{:S(2)}) collective-permute-start(bf16[104,1024]{1,0:T(8,128)(2,1)S(1)} %collective-permute-done.2.refs_4_), channel_id=1, source_target_pairs={{0,1},{1,0},{2,3},{3,2},{4,6},{5,7},{6,4},{7,5},{8,9},{9,8},{10,11... | collective-permute-start | bytes 638984 | tf_op jit(solution)/shard_map/ppermute | solution.py:40
  34.0 0.5 collective-permute-start.5
  34.5 0.5 collective-permute-start.12
  35.1 0.1 collective-permute-start.8
  35.1 3.2 %collective-permute-done.3.refs_5_ = bf16[104,1024]{1,0:T(8,128)(2,1)S(1)} collective-permute-done((bf16[104,1024]{1,0:T(8,128)(2,1)S(1)}, bf16[104,1024]{1,0:T(8,128)(2,1)S(1)}, u32[]{:S(2)}, u32[]{:S(2)}) %collective-permute-start.3) | collective-permute-done | bytes 213024 | tf_op jit(solution)/shard_map/ppermute | solution.py:40
  38.4 2.3 %collective-permute-done.5.refs_7_ = bf16[104,1024]{1,0:T(8,128)(2,1)S(1)} collective-permute-done((bf16[104,1024]{1,0:T(8,128)(2,1)S(1)}, bf16[104,1024]{1,0:T(8,128)(2,1)S(1)}, u32[]{:S(2)}, u32[]{:S(2)}) %collective-permute-start.5) | collective-permute-done | bytes 213024 | tf_op jit(solution)/shard_map/ppermute | solution.py:40
  40.6 0.5 collective-permute-start.9
  41.2 1.5 %collective-permute-start.22 = (bf16[512,512]{1,0:T(8,128)(2,1)S(1)}, bf16[512,512]{1,0:T(8,128)(2,1)S(1)}, u32[]{:S(2)}, u32[]{:S(2)}) collective-permute-start(bf16[512,512]{1,0:T(8,128)(2,1)S(1)} %get-tuple-element.52), channel_id=1, source_target_pairs={{0,2},{1,3},{2,0},{3,1},{4,5},{5,4},{6,7},{7,6},{8,10},{9,11},{10,... | collective-permute-start | bytes 1572872 | tf_op jit(solution)/shard_map/ppermute | solution.py:40
  42.7 3.5 %shard_map.195 = (bf16[2048,1024]{1,0:T(8,128)(2,1)S(1)}, bf16[2048,1024]{1,0:T(8,128)(2,1)S(1)}) custom-call(bf16[2048,1024]{1,0:T(8,128)(2,1)} %bitcast.31, bf16[2048,1024]{1,0:T(8,128)(2,1)} %bitcast.32), custom_call_target="tpu_custom_call" | custom-call | flops 1048576 | tf_op jit(solution)/shard_map/pallas_call | solution.py:107
  46.2 3.5 %collective-permute-start.18 = (bf16[136,256]{1,0:T(8,128)(2,1)S(1)}, bf16[136,256]{1,0:T(8,128)(2,1)S(1)}, u32[]{:S(2)}, u32[]{:S(2)}) collective-permute-start(bf16[136,256]{1,0:T(8,128)(2,1)S(1)} %get-tuple-element.51), channel_id=1, source_target_pairs={{0,16},{1,17},{2,18},{3,19},{4,20},{5,21},{6,22},{7,23},{8,24},{9,... | collective-permute-start | bytes 208904 | tf_op jit(solution)/shard_map/ppermute | solution.py:40
  49.7 2.7 %collective-permute-start.20 = (bf16[136,256]{1,0:T(8,128)(2,1)S(1)}, bf16[136,256]{1,0:T(8,128)(2,1)S(1)}, u32[]{:S(2)}, u32[]{:S(2)}) collective-permute-start(bf16[136,256]{1,0:T(8,128)(2,1)S(1)} %get-tuple-element.51), channel_id=1, source_target_pairs={{0,24},{1,25},{2,26},{3,27},{4,28},{5,29},{6,30},{7,31},{8,0},{9,1... | collective-permute-start | bytes 208904 | tf_op jit(solution)/shard_map/ppermute | solution.py:40
  52.5 0.5 collective-permute-start.17
  53.0 3.2 %shard_map.196 = (bf16[288,1024]{1,0:T(8,128)(2,1)S(1)}, f32[4,256]{1,0:T(4,128)S(1)}) custom-call(bf16[96,2048]{1,0:T(8,128)(2,1)S(1)} %get-tuple-element.35.refs_0_.normed_ref, bf16[104,1024]{1,0:T(8,128)(2,1)S(1)} %get-tuple-element.36.refs_1_, bf16[104,1024]{1,0:T(8,128)(2,1)S(1)} %collective-permute-done.refs_2_, ...), custom_call_target="tpu_custom_call" | custom-call | flops 2415919104 | tf_op jit(solution)/shard_map/pallas_call | solution.py:107
  56.2 0.0 copy-start.2
  56.2 0.0 copy-start.11
  56.2 0.6 collective-permute-start.23
  56.8 0.7 collective-permute-start.19
  57.5 0.1 collective-permute-start.21
  57.6 1.2 collective-permute-start.24
  58.8 3.3 %shard_map.197 = (bf16[288,1024]{1,0:T(8,128)(2,1)S(1)}, f32[4,256]{1,0:T(4,128)S(1)}) custom-call(bf16[96,2048]{1,0:T(8,128)(2,1)S(1)} %collective-permute-done.6.refs_0_, bf16[104,1024]{1,0:T(8,128)(2,1)S(1)} %collective-permute-done.7.refs_1_, bf16[104,1024]{1,0:T(8,128)(2,1)S(1)} %collective-permute-done.8.refs_2_, ...), custom_call_target="tpu_custom_call" | custom-call | flops 2415919104 | tf_op jit(solution)/shard_map/pallas_call | solution.py:107
  62.2 0.9 collective-permute-start.14
  63.1 1.2 collective-permute-start.25
  64.3 0.8 collective-permute-start.26
  65.1 0.8 shard_map.199.refs_0_
  65.9 4.3 %collective-permute-done.23.refs_4_ = bf16[512,512]{1,0:T(8,128)(2,1)S(1)} collective-permute-done((bf16[512,512]{1,0:T(8,128)(2,1)S(1)}, bf16[512,512]{1,0:T(8,128)(2,1)S(1)}, u32[]{:S(2)}, u32[]{:S(2)}) %collective-permute-start.23) | collective-permute-done | bytes 524320 | tf_op jit(solution)/shard_map/ppermute | solution.py:40
  70.2 1.5 %shard_map.200 = (f32[288,512]{1,0:T(8,128)S(1)}, f32[288,512]{1,0:T(8,128)S(1)}, f32[288,512]{1,0:T(8,128)S(1)}, f32[288,512]{1,0:T(8,128)S(1)}) custom-call(bf16[288,1024]{1,0:T(8,128)(2,1)S(1)} %get-tuple-element.39.refs_0_, bf16[288,1024]{1,0:T(8,128)(2,1)S(1)} %get-tuple-element.48.refs_1_, bf16[4096,512]{1,0:T(8,128)(2,1)S(1)} %bitcast.27, ...), custom_call_target="tpu_custom_call" | custom-call | flops 1207959552 | tf_op jit(solution)/shard_map/pallas_call | solution.py:107
  71.7 9.8 %collective-permute-done.25.refs_1_ = bf16[512,512]{1,0:T(8,128)(2,1)S(1)} collective-permute-done((bf16[512,512]{1,0:T(8,128)(2,1)S(1)}, bf16[512,512]{1,0:T(8,128)(2,1)S(1)}, u32[]{:S(2)}, u32[]{:S(2)}) %collective-permute-start.25) | collective-permute-done | bytes 524320 | tf_op jit(solution)/shard_map/ppermute | solution.py:40
  81.5 7.8 %collective-permute-done.26.refs_2_ = bf16[512,512]{1,0:T(8,128)(2,1)S(1)} collective-permute-done((bf16[512,512]{1,0:T(8,128)(2,1)S(1)}, bf16[512,512]{1,0:T(8,128)(2,1)S(1)}, u32[]{:S(2)}, u32[]{:S(2)}) %collective-permute-start.26) | collective-permute-done | bytes 524320 | tf_op jit(solution)/shard_map/ppermute | solution.py:40
  89.3 0.5 shard_map.201
  89.8 0.5 shard_map.205
  90.3 0.6 collective-permute-start.31
  90.9 0.8 shard_map.203
  91.7 5.3 %collective-permute-done.31.refs_0_ = bf16[288,512]{1,0:T(8,128)(2,1)S(1)} collective-permute-done((bf16[288,512]{1,0:T(8,128)(2,1)S(1)}, bf16[288,512]{1,0:T(8,128)(2,1)S(1)}, u32[]{:S(2)}, u32[]{:S(2)}) %collective-permute-start.31) | collective-permute-done | bytes 294944 | tf_op jit(solution)/shard_map/ppermute | solution.py:40
  97.1 0.3 shard_map.206
  97.4 0.1 collective-permute-start.32
  97.5 0.6 collective-permute-start.30
  98.1 1.4 %collective-permute-start.27 = (bf16[304,512]{1,0:T(8,128)(2,1)S(1)}, bf16[304,512]{1,0:T(8,128)(2,1)S(1)}, u32[]{:S(2)}, u32[]{:S(2)}) collective-permute-start(bf16[304,512]{1,0:T(8,128)(2,1)S(1)} %shard_map.199.refs_0_), channel_id=1, source_target_pairs={{0,1},{1,0},{2,3},{3,2},{4,5},{5,4},{6,7},{7,6},{8,9},{9,8},{10,11... | collective-permute-start | bytes 933896 | tf_op jit(solution)/shard_map/ppermute | solution.py:40
  99.6 1.5 %collective-permute-start.28 = (bf16[304,512]{1,0:T(8,128)(2,1)S(1)}, bf16[304,512]{1,0:T(8,128)(2,1)S(1)}, u32[]{:S(2)}, u32[]{:S(2)}) collective-permute-start(bf16[304,512]{1,0:T(8,128)(2,1)S(1)} %shard_map.199.refs_0_), channel_id=1, source_target_pairs={{0,2},{1,3},{2,0},{3,1},{4,6},{5,7},{6,4},{7,5},{8,10},{9,11},{10,... | collective-permute-start | bytes 933896 | tf_op jit(solution)/shard_map/ppermute | solution.py:40
  101.1 0.5 collective-permute-start.29
  101.6 4.9 %collective-permute-done.30.refs_0_ = bf16[288,512]{1,0:T(8,128)(2,1)S(1)} collective-permute-done((bf16[288,512]{1,0:T(8,128)(2,1)S(1)}, bf16[288,512]{1,0:T(8,128)(2,1)S(1)}, u32[]{:S(2)}, u32[]{:S(2)}) %collective-permute-start.30) | collective-permute-done | bytes 294944 | tf_op jit(solution)/shard_map/ppermute | solution.py:40
  106.5 0.3 shard_map.204
  106.9 0.1 fusion.5
  107.1 2.7 %collective-permute-start.33 = (bf16[96,512]{1,0:T(8,128)(2,1)S(1)}, bf16[96,512]{1,0:T(8,128)(2,1)S(1)}, u32[]{:S(2)}, u32[]{:S(2)}) collective-permute-start(bf16[96,512]{1,0:T(8,128)(2,1)S(1)} %get-tuple-element.70), channel_id=1, source_target_pairs={{0,24},{1,25},{2,26},{3,27},{4,28},{5,29},{6,30},{7,31},{8,0},{9,1... | collective-permute-start | bytes 294920 | tf_op jit(solution)/shard_map/ppermute | solution.py:40
  109.8 1.3 %collective-permute-start.35 = (bf16[96,512]{1,0:T(8,128)(2,1)S(1)}, bf16[96,512]{1,0:T(8,128)(2,1)S(1)}, u32[]{:S(2)}, u32[]{:S(2)}) collective-permute-start(bf16[96,512]{1,0:T(8,128)(2,1)S(1)} %get-tuple-element.71), channel_id=1, source_target_pairs={{0,8},{1,9},{2,10},{3,11},{4,12},{5,13},{6,14},{7,15},{8,16},{9,17... | collective-permute-start | bytes 294920 | tf_op jit(solution)/shard_map/ppermute | solution.py:40
  111.1 6.5 %collective-permute-done.28.refs_2_ = bf16[304,512]{1,0:T(8,128)(2,1)S(1)} collective-permute-done((bf16[304,512]{1,0:T(8,128)(2,1)S(1)}, bf16[304,512]{1,0:T(8,128)(2,1)S(1)}, u32[]{:S(2)}, u32[]{:S(2)}) %collective-permute-start.28) | collective-permute-done | bytes 311328 | tf_op jit(solution)/shard_map/ppermute | solution.py:40
  117.7 0.9 shard_map.202
  118.5 0.7 copy.21
  119.2 0.7 fusion.4
  (51 shorter events, 0.2 us)
Async XLA Ops:
  0.6 1.0 copy-start.5
  1.6 0.9 copy-start.7
  2.5 0.9 copy-start.8
  3.4 0.9 copy-start.9
  4.3 0.7 copy-start.10
  5.0 0.7 copy-start.12
  8.9 10.5 %collective-permute-start.16 = (bf16[136,256]{1,0:T(8,128)(2,1)S(1)}, bf16[136,256]{1,0:T(8,128)(2,1)S(1)}, u32[]{:S(2)}, u32[]{:S(2)}) collective-permute-start(bf16[136,256]{1,0:T(8,128)(2,1)S(1)} %get-tuple-element.51), channel_id=1, source_target_pairs={{0,8},{1,9},{2,10},{3,11},{4,12},{5,13},{6,14},{7,15},{8,16},{9,17... | collective-permute-start | bytes 208904 | tf_op jit(solution)/shard_map/ppermute | solution.py:40
  13.7 20.8 %collective-permute-start.6 = (bf16[96,2048]{1,0:T(8,128)(2,1)S(1)}, bf16[96,2048]{1,0:T(8,128)(2,1)S(1)}, u32[]{:S(2)}, u32[]{:S(2)}) collective-permute-start(bf16[96,2048]{1,0:T(8,128)(2,1)S(1)} %get-tuple-element.35.refs_0_.normed_ref), channel_id=1, source_target_pairs={{0,4},{1,5},{2,6},{3,7},{4,0},{5,1},{6,2},{7,3},{8,12},{9,13},{10,... | collective-permute-start | bytes 1179656 | tf_op jit(solution)/shard_map/ppermute | solution.py:40
  13.8 10.1 %collective-permute-start = (bf16[104,1024]{1,0:T(8,128)(2,1)S(1)}, bf16[104,1024]{1,0:T(8,128)(2,1)S(1)}, u32[]{:S(2)}, u32[]{:S(2)}) collective-permute-start(bf16[104,1024]{1,0:T(8,128)(2,1)S(1)} %get-tuple-element.36.refs_1_), channel_id=1, source_target_pairs={{0,8},{1,9},{2,10},{3,11},{4,12},{5,13},{6,14},{7,15},{8,16},{9,17... | collective-permute-start | bytes 638984 | tf_op jit(solution)/shard_map/ppermute | solution.py:40
  15.4 17.1 %collective-permute-start.2 = (bf16[104,1024]{1,0:T(8,128)(2,1)S(1)}, bf16[104,1024]{1,0:T(8,128)(2,1)S(1)}, u32[]{:S(2)}, u32[]{:S(2)}) collective-permute-start(bf16[104,1024]{1,0:T(8,128)(2,1)S(1)} %get-tuple-element.36.refs_1_), channel_id=1, source_target_pairs={{0,16},{1,17},{2,18},{3,19},{4,20},{5,21},{6,22},{7,23},{8,24},{9,... | collective-permute-start | bytes 638984 | tf_op jit(solution)/shard_map/ppermute | solution.py:40
  16.5 17.5 %collective-permute-start.4 = (bf16[104,1024]{1,0:T(8,128)(2,1)S(1)}, bf16[104,1024]{1,0:T(8,128)(2,1)S(1)}, u32[]{:S(2)}, u32[]{:S(2)}) collective-permute-start(bf16[104,1024]{1,0:T(8,128)(2,1)S(1)} %get-tuple-element.36.refs_1_), channel_id=1, source_target_pairs={{0,24},{1,25},{2,26},{3,27},{4,28},{5,29},{6,30},{7,31},{8,0},{9,1... | collective-permute-start | bytes 638984 | tf_op jit(solution)/shard_map/ppermute | solution.py:40
  19.4 15.2 %collective-permute-start.7 = (bf16[104,1024]{1,0:T(8,128)(2,1)S(1)}, bf16[104,1024]{1,0:T(8,128)(2,1)S(1)}, u32[]{:S(2)}, u32[]{:S(2)}) collective-permute-start(bf16[104,1024]{1,0:T(8,128)(2,1)S(1)} %get-tuple-element.36.refs_1_), channel_id=1, source_target_pairs={{0,4},{1,5},{2,6},{3,7},{4,0},{5,1},{6,2},{7,3},{8,12},{9,13},{10,... | collective-permute-start | bytes 638984 | tf_op jit(solution)/shard_map/ppermute | solution.py:40
  23.9 11.1 %collective-permute-start.1 = (bf16[104,1024]{1,0:T(8,128)(2,1)S(1)}, bf16[104,1024]{1,0:T(8,128)(2,1)S(1)}, u32[]{:S(2)}, u32[]{:S(2)}) collective-permute-start(bf16[104,1024]{1,0:T(8,128)(2,1)S(1)} %collective-permute-done.refs_2_), channel_id=1, source_target_pairs={{0,1},{1,0},{2,3},{3,2},{4,6},{5,7},{6,4},{7,5},{8,9},{9,8},{10,11... | collective-permute-start | bytes 638984 | tf_op jit(solution)/shard_map/ppermute | solution.py:40
  32.5 5.8 %collective-permute-start.3 = (bf16[104,1024]{1,0:T(8,128)(2,1)S(1)}, bf16[104,1024]{1,0:T(8,128)(2,1)S(1)}, u32[]{:S(2)}, u32[]{:S(2)}) collective-permute-start(bf16[104,1024]{1,0:T(8,128)(2,1)S(1)} %collective-permute-done.2.refs_4_), channel_id=1, source_target_pairs={{0,1},{1,0},{2,3},{3,2},{4,6},{5,7},{6,4},{7,5},{8,9},{9,8},{10,11... | collective-permute-start | bytes 638984 | tf_op jit(solution)/shard_map/ppermute | solution.py:40
  34.0 6.6 %collective-permute-start.5 = (bf16[104,1024]{1,0:T(8,128)(2,1)S(1)}, bf16[104,1024]{1,0:T(8,128)(2,1)S(1)}, u32[]{:S(2)}, u32[]{:S(2)}) collective-permute-start(bf16[104,1024]{1,0:T(8,128)(2,1)S(1)} %collective-permute-done.4.refs_6_), channel_id=1, source_target_pairs={{0,1},{1,0},{2,3},{3,2},{4,6},{5,7},{6,4},{7,5},{8,9},{9,8},{10,11... | collective-permute-start | bytes 638984 | tf_op jit(solution)/shard_map/ppermute | solution.py:40
  34.5 6.1 %collective-permute-start.10 = (bf16[104,1024]{1,0:T(8,128)(2,1)S(1)}, bf16[104,1024]{1,0:T(8,128)(2,1)S(1)}, u32[]{:S(2)}, u32[]{:S(2)}) collective-permute-start(bf16[104,1024]{1,0:T(8,128)(2,1)S(1)} %collective-permute-done.2.refs_4_), channel_id=1, source_target_pairs={{0,4},{1,5},{2,6},{3,7},{4,0},{5,1},{6,2},{7,3},{8,12},{9,13},{10,... | collective-permute-start | bytes 638984 | tf_op jit(solution)/shard_map/ppermute | solution.py:40
  34.5 6.6 %collective-permute-start.12 = (bf16[104,1024]{1,0:T(8,128)(2,1)S(1)}, bf16[104,1024]{1,0:T(8,128)(2,1)S(1)}, u32[]{:S(2)}, u32[]{:S(2)}) collective-permute-start(bf16[104,1024]{1,0:T(8,128)(2,1)S(1)} %collective-permute-done.4.refs_6_), channel_id=1, source_target_pairs={{0,4},{1,5},{2,6},{3,7},{4,0},{5,1},{6,2},{7,3},{8,12},{9,13},{10,... | collective-permute-start | bytes 638984 | tf_op jit(solution)/shard_map/ppermute | solution.py:40
  35.1 11.1 %collective-permute-start.8 = (bf16[104,1024]{1,0:T(8,128)(2,1)S(1)}, bf16[104,1024]{1,0:T(8,128)(2,1)S(1)}, u32[]{:S(2)}, u32[]{:S(2)}) collective-permute-start(bf16[104,1024]{1,0:T(8,128)(2,1)S(1)} %collective-permute-done.refs_2_), channel_id=1, source_target_pairs={{0,4},{1,5},{2,6},{3,7},{4,0},{5,1},{6,2},{7,3},{8,12},{9,13},{10,... | collective-permute-start | bytes 638984 | tf_op jit(solution)/shard_map/ppermute | solution.py:40
  38.4 11.4 %collective-permute-start.11 = (bf16[104,1024]{1,0:T(8,128)(2,1)S(1)}, bf16[104,1024]{1,0:T(8,128)(2,1)S(1)}, u32[]{:S(2)}, u32[]{:S(2)}) collective-permute-start(bf16[104,1024]{1,0:T(8,128)(2,1)S(1)} %collective-permute-done.3.refs_5_), channel_id=1, source_target_pairs={{0,4},{1,5},{2,6},{3,7},{4,0},{5,1},{6,2},{7,3},{8,12},{9,13},{10,... | collective-permute-start | bytes 638984 | tf_op jit(solution)/shard_map/ppermute | solution.py:40
  40.6 11.8 %collective-permute-start.13 = (bf16[104,1024]{1,0:T(8,128)(2,1)S(1)}, bf16[104,1024]{1,0:T(8,128)(2,1)S(1)}, u32[]{:S(2)}, u32[]{:S(2)}) collective-permute-start(bf16[104,1024]{1,0:T(8,128)(2,1)S(1)} %collective-permute-done.5.refs_7_), channel_id=1, source_target_pairs={{0,4},{1,5},{2,6},{3,7},{4,0},{5,1},{6,2},{7,3},{8,12},{9,13},{10,... | collective-permute-start | bytes 638984 | tf_op jit(solution)/shard_map/ppermute | solution.py:40
  40.6 11.8 %collective-permute-start.9 = (bf16[104,1024]{1,0:T(8,128)(2,1)S(1)}, bf16[104,1024]{1,0:T(8,128)(2,1)S(1)}, u32[]{:S(2)}, u32[]{:S(2)}) collective-permute-start(bf16[104,1024]{1,0:T(8,128)(2,1)S(1)} %collective-permute-done.1.refs_3_), channel_id=1, source_target_pairs={{0,4},{1,5},{2,6},{3,7},{4,0},{5,1},{6,2},{7,3},{8,12},{9,13},{10,... | collective-permute-start | bytes 638984 | tf_op jit(solution)/shard_map/ppermute | solution.py:40
  41.2 23.1 %collective-permute-start.22 = (bf16[512,512]{1,0:T(8,128)(2,1)S(1)}, bf16[512,512]{1,0:T(8,128)(2,1)S(1)}, u32[]{:S(2)}, u32[]{:S(2)}) collective-permute-start(bf16[512,512]{1,0:T(8,128)(2,1)S(1)} %get-tuple-element.52), channel_id=1, source_target_pairs={{0,2},{1,3},{2,0},{3,1},{4,5},{5,4},{6,7},{7,6},{8,10},{9,11},{10,... | collective-permute-start | bytes 1572872 | tf_op jit(solution)/shard_map/ppermute | solution.py:40
  46.2 10.0 %collective-permute-start.18 = (bf16[136,256]{1,0:T(8,128)(2,1)S(1)}, bf16[136,256]{1,0:T(8,128)(2,1)S(1)}, u32[]{:S(2)}, u32[]{:S(2)}) collective-permute-start(bf16[136,256]{1,0:T(8,128)(2,1)S(1)} %get-tuple-element.51), channel_id=1, source_target_pairs={{0,16},{1,17},{2,18},{3,19},{4,20},{5,21},{6,22},{7,23},{8,24},{9,... | collective-permute-start | bytes 208904 | tf_op jit(solution)/shard_map/ppermute | solution.py:40
  49.7 7.1 %collective-permute-start.20 = (bf16[136,256]{1,0:T(8,128)(2,1)S(1)}, bf16[136,256]{1,0:T(8,128)(2,1)S(1)}, u32[]{:S(2)}, u32[]{:S(2)}) collective-permute-start(bf16[136,256]{1,0:T(8,128)(2,1)S(1)} %get-tuple-element.51), channel_id=1, source_target_pairs={{0,24},{1,25},{2,26},{3,27},{4,28},{5,29},{6,30},{7,31},{8,0},{9,1... | collective-permute-start | bytes 208904 | tf_op jit(solution)/shard_map/ppermute | solution.py:40
  52.5 5.1 %collective-permute-start.15 = (bf16[136,256]{1,0:T(8,128)(2,1)S(1)}, bf16[136,256]{1,0:T(8,128)(2,1)S(1)}, u32[]{:S(2)}, u32[]{:S(2)}) collective-permute-start(bf16[136,256]{1,0:T(8,128)(2,1)S(1)} %get-tuple-element.51), channel_id=1, source_target_pairs={{0,4},{1,5},{2,6},{3,7},{4,0},{5,1},{6,2},{7,3},{8,12},{9,13},{10,... | collective-permute-start | bytes 208904 | tf_op jit(solution)/shard_map/ppermute | solution.py:40
  52.5 5.2 %collective-permute-start.17 = (bf16[136,256]{1,0:T(8,128)(2,1)S(1)}, bf16[136,256]{1,0:T(8,128)(2,1)S(1)}, u32[]{:S(2)}, u32[]{:S(2)}) collective-permute-start(bf16[136,256]{1,0:T(8,128)(2,1)S(1)} %collective-permute-done.16.refs_1_), channel_id=1, source_target_pairs={{0,4},{1,5},{2,6},{3,7},{4,0},{5,1},{6,2},{7,3},{8,12},{9,13},{10,... | collective-permute-start | bytes 208904 | tf_op jit(solution)/shard_map/ppermute | solution.py:40
  56.2 9.0 %copy-start.2 = (bf16[2048,256]{1,0:T(8,128)(2,1)S(1)}, bf16[2048,256]{1,0:T(8,128)(2,1)}, u32[]{:S(2)}) copy-start(bf16[2048,256]{1,0:T(8,128)(2,1)} %sg_ref.1) | copy-start | bytes 3145732
  56.2 9.0 %copy-start.3 = (bf16[2048,256]{1,0:T(8,128)(2,1)S(1)}, bf16[2048,256]{1,0:T(8,128)(2,1)}, u32[]{:S(2)}) copy-start(bf16[2048,256]{1,0:T(8,128)(2,1)} %su_ref.1) | copy-start | bytes 3145732
  56.2 8.9 %copy-start.6 = (bf16[256,512]{1,0:T(8,128)(2,1)S(1)}, bf16[256,512]{1,0:T(8,128)(2,1)}, u32[]{:S(2)}) copy-start(bf16[256,512]{1,0:T(8,128)(2,1)} %gate_ref.1) | copy-start | bytes 786436
  56.2 8.9 %copy-start.11 = (f32[512]{0:T(512)S(1)}, f32[512]{0:T(512)}, u32[]{:S(2)}) copy-start(f32[512]{0:T(512)} %param.26) | copy-start | bytes 6148
  56.2 14.0 %collective-permute-start.23 = (bf16[512,512]{1,0:T(8,128)(2,1)S(1)}, bf16[512,512]{1,0:T(8,128)(2,1)S(1)}, u32[]{:S(2)}, u32[]{:S(2)}) collective-permute-start(bf16[512,512]{1,0:T(8,128)(2,1)S(1)} %get-tuple-element.53), channel_id=1, source_target_pairs={{0,2},{1,3},{2,0},{3,1},{4,5},{5,4},{6,7},{7,6},{8,10},{9,11},{10,... | collective-permute-start | bytes 1572872 | tf_op jit(solution)/shard_map/ppermute | solution.py:40
  56.8 5.3 %collective-permute-start.19 = (bf16[136,256]{1,0:T(8,128)(2,1)S(1)}, bf16[136,256]{1,0:T(8,128)(2,1)S(1)}, u32[]{:S(2)}, u32[]{:S(2)}) collective-permute-start(bf16[136,256]{1,0:T(8,128)(2,1)S(1)} %collective-permute-done.18.refs_3_), channel_id=1, source_target_pairs={{0,4},{1,5},{2,6},{3,7},{4,0},{5,1},{6,2},{7,3},{8,12},{9,13},{10,... | collective-permute-start | bytes 208904 | tf_op jit(solution)/shard_map/ppermute | solution.py:40
  57.5 5.5 %collective-permute-start.21 = (bf16[136,256]{1,0:T(8,128)(2,1)S(1)}, bf16[136,256]{1,0:T(8,128)(2,1)S(1)}, u32[]{:S(2)}, u32[]{:S(2)}) collective-permute-start(bf16[136,256]{1,0:T(8,128)(2,1)S(1)} %collective-permute-done.20.refs_5_), channel_id=1, source_target_pairs={{0,4},{1,5},{2,6},{3,7},{4,0},{5,1},{6,2},{7,3},{8,12},{9,13},{10,... | collective-permute-start | bytes 208904 | tf_op jit(solution)/shard_map/ppermute | solution.py:40
  57.6 31.7 %collective-permute-start.24 = (bf16[288,1024]{1,0:T(8,128)(2,1)S(1)}, bf16[288,1024]{1,0:T(8,128)(2,1)S(1)}, u32[]{:S(2)}, u32[]{:S(2)}) collective-permute-start(bf16[288,1024]{1,0:T(8,128)(2,1)S(1)} %get-tuple-element.39.refs_0_), channel_id=1, source_target_pairs={{0,1},{1,0},{2,3},{3,2},{4,6},{5,7},{6,4},{7,5},{8,9},{9,8},{10,11... | collective-permute-start | bytes 1769480 | tf_op jit(solution)/shard_map/ppermute | solution.py:40
  62.1 8.1 %copy-start = (bf16[1,4096,512]{2,1,0:T(8,128)(2,1)S(1)}, bf16[1,4096,512]{2,1,0:T(8,128)(2,1)}, u32[]{:S(2)}) copy-start(bf16[1,4096,512]{2,1,0:T(8,128)(2,1)} %param.34) | copy-start | bytes 12582916
  62.2 27.7 %collective-permute-start.14 = (bf16[288,1024]{1,0:T(8,128)(2,1)S(1)}, bf16[288,1024]{1,0:T(8,128)(2,1)S(1)}, u32[]{:S(2)}, u32[]{:S(2)}) collective-permute-start(bf16[288,1024]{1,0:T(8,128)(2,1)S(1)} %get-tuple-element.48.refs_1_), channel_id=1, source_target_pairs={{0,1},{1,0},{2,3},{3,2},{4,6},{5,7},{6,4},{7,5},{8,9},{9,8},{10,11... | collective-permute-start | bytes 1769480 | tf_op jit(solution)/shard_map/ppermute | solution.py:40
  63.1 18.4 %collective-permute-start.25 = (bf16[512,512]{1,0:T(8,128)(2,1)S(1)}, bf16[512,512]{1,0:T(8,128)(2,1)S(1)}, u32[]{:S(2)}, u32[]{:S(2)}) collective-permute-start(bf16[512,512]{1,0:T(8,128)(2,1)S(1)} %get-tuple-element.55), channel_id=1, source_target_pairs={{0,2},{1,3},{2,0},{3,1},{4,5},{5,4},{6,7},{7,6},{8,10},{9,11},{10,... | collective-permute-start | bytes 1572872 | tf_op jit(solution)/shard_map/ppermute | solution.py:40
  64.3 25.0 %collective-permute-start.26 = (bf16[512,512]{1,0:T(8,128)(2,1)S(1)}, bf16[512,512]{1,0:T(8,128)(2,1)S(1)}, u32[]{:S(2)}, u32[]{:S(2)}) collective-permute-start(bf16[512,512]{1,0:T(8,128)(2,1)S(1)} %get-tuple-element.56), channel_id=1, source_target_pairs={{0,2},{1,3},{2,0},{3,1},{4,5},{5,4},{6,7},{7,6},{8,10},{9,11},{10,... | collective-permute-start | bytes 1572872 | tf_op jit(solution)/shard_map/ppermute | solution.py:40
  90.3 6.8 %collective-permute-start.31 = (bf16[288,512]{1,0:T(8,128)(2,1)S(1)}, bf16[288,512]{1,0:T(8,128)(2,1)S(1)}, u32[]{:S(2)}, u32[]{:S(2)}) collective-permute-start(bf16[288,512]{1,0:T(8,128)(2,1)S(1)} %shard_map.205), channel_id=1, source_target_pairs={{0,2},{1,3},{2,0},{3,1},{4,5},{5,4},{6,7},{7,6},{8,10},{9,11},{10,... | collective-permute-start | bytes 884744 | tf_op jit(solution)/shard_map/ppermute | solution.py:40
  91.7 25.9 %copy-start.1 = (bf16[2048,512]{1,0:T(8,128)(2,1)S(1)}, bf16[2048,512]{1,0:T(8,128)(2,1)}, u32[]{:S(2)}) copy-start(bf16[2048,512]{1,0:T(8,128)(2,1)} %refs_4_.1) | copy-start | bytes 6291460
  91.7 25.9 %copy-start.4 = (bf16[1024,512]{1,0:T(8,128)(2,1)S(1)}, bf16[1024,512]{1,0:T(8,128)(2,1)}, u32[]{:S(2)}) copy-start(bf16[1024,512]{1,0:T(8,128)(2,1)} %refs_5_.1) | copy-start | bytes 3145732
  97.4 9.4 %collective-permute-start.32 = (bf16[4,96,512]{2,1,0:T(8,128)(2,1)S(1)}, bf16[4,96,512]{2,1,0:T(8,128)(2,1)S(1)}, u32[]{:S(2)}, u32[]{:S(2)}) collective-permute-start(bf16[4,96,512]{2,1,0:T(8,128)(2,1)S(1)} %shard_map.206), channel_id=1, source_target_pairs={{0,4},{1,5},{2,6},{3,7},{4,0},{5,1},{6,2},{7,3},{8,12},{9,13},{10,... | collective-permute-start | bytes 1179656 | tf_op jit(solution)/shard_map/ppermute | solution.py:40
  97.5 9.0 %collective-permute-start.30 = (bf16[288,512]{1,0:T(8,128)(2,1)S(1)}, bf16[288,512]{1,0:T(8,128)(2,1)S(1)}, u32[]{:S(2)}, u32[]{:S(2)}) collective-permute-start(bf16[288,512]{1,0:T(8,128)(2,1)S(1)} %shard_map.201), channel_id=1, source_target_pairs={{0,2},{1,3},{2,0},{3,1},{4,5},{5,4},{6,7},{7,6},{8,10},{9,11},{10,... | collective-permute-start | bytes 884744 | tf_op jit(solution)/shard_map/ppermute | solution.py:40
  98.1 11.7 %collective-permute-start.27 = (bf16[304,512]{1,0:T(8,128)(2,1)S(1)}, bf16[304,512]{1,0:T(8,128)(2,1)S(1)}, u32[]{:S(2)}, u32[]{:S(2)}) collective-permute-start(bf16[304,512]{1,0:T(8,128)(2,1)S(1)} %shard_map.199.refs_0_), channel_id=1, source_target_pairs={{0,1},{1,0},{2,3},{3,2},{4,5},{5,4},{6,7},{7,6},{8,9},{9,8},{10,11... | collective-permute-start | bytes 933896 | tf_op jit(solution)/shard_map/ppermute | solution.py:40
  99.6 18.1 %collective-permute-start.28 = (bf16[304,512]{1,0:T(8,128)(2,1)S(1)}, bf16[304,512]{1,0:T(8,128)(2,1)S(1)}, u32[]{:S(2)}, u32[]{:S(2)}) collective-permute-start(bf16[304,512]{1,0:T(8,128)(2,1)S(1)} %shard_map.199.refs_0_), channel_id=1, source_target_pairs={{0,2},{1,3},{2,0},{3,1},{4,6},{5,7},{6,4},{7,5},{8,10},{9,11},{10,... | collective-permute-start | bytes 933896 | tf_op jit(solution)/shard_map/ppermute | solution.py:40
  101.1 16.6 %collective-permute-start.29 = (bf16[304,512]{1,0:T(8,128)(2,1)S(1)}, bf16[304,512]{1,0:T(8,128)(2,1)S(1)}, u32[]{:S(2)}, u32[]{:S(2)}) collective-permute-start(bf16[304,512]{1,0:T(8,128)(2,1)S(1)} %shard_map.199.refs_0_), channel_id=1, source_target_pairs={{0,3},{1,2},{2,1},{3,0},{4,7},{5,6},{6,5},{7,4},{8,11},{9,10},{10,... | collective-permute-start | bytes 933896 | tf_op jit(solution)/shard_map/ppermute | solution.py:40
  107.1 12.2 %collective-permute-start.33 = (bf16[96,512]{1,0:T(8,128)(2,1)S(1)}, bf16[96,512]{1,0:T(8,128)(2,1)S(1)}, u32[]{:S(2)}, u32[]{:S(2)}) collective-permute-start(bf16[96,512]{1,0:T(8,128)(2,1)S(1)} %get-tuple-element.70), channel_id=1, source_target_pairs={{0,24},{1,25},{2,26},{3,27},{4,28},{5,29},{6,30},{7,31},{8,0},{9,1... | collective-permute-start | bytes 294920 | tf_op jit(solution)/shard_map/ppermute | solution.py:40
  109.8 9.4 %collective-permute-start.34 = (bf16[96,512]{1,0:T(8,128)(2,1)S(1)}, bf16[96,512]{1,0:T(8,128)(2,1)S(1)}, u32[]{:S(2)}, u32[]{:S(2)}) collective-permute-start(bf16[96,512]{1,0:T(8,128)(2,1)S(1)} %get-tuple-element.72), channel_id=1, source_target_pairs={{0,16},{1,17},{2,18},{3,19},{4,20},{5,21},{6,22},{7,23},{8,24},{9,... | collective-permute-start | bytes 294920 | tf_op jit(solution)/shard_map/ppermute | solution.py:40
  109.8 9.4 %collective-permute-start.35 = (bf16[96,512]{1,0:T(8,128)(2,1)S(1)}, bf16[96,512]{1,0:T(8,128)(2,1)S(1)}, u32[]{:S(2)}, u32[]{:S(2)}) collective-permute-start(bf16[96,512]{1,0:T(8,128)(2,1)S(1)} %get-tuple-element.71), channel_id=1, source_target_pairs={{0,8},{1,9},{2,10},{3,11},{4,12},{5,13},{6,14},{7,15},{8,16},{9,17... | collective-permute-start | bytes 294920 | tf_op jit(solution)/shard_map/ppermute | solution.py:40
